TPU v7x, 32 devices: a whole 2x2x4 slice. The times are simulated.
32 devices in a mesh: fs: 8 (over z, x), tp: 4 (over y, core).
Axes of the slice: x: 2, y: 2, z: 4, core: 2. Of those that a mesh axis runs over, the one named last changes fastest.
Arguments:
- tokens: bfloat16 [6144, 2048], P('fs', 'tp'), may hold values from -6 to 6
- ffn_one_gain: float32 [2048], replicated, may hold values from 0.1 to 1.9
- ffn_one_gate: bfloat16 [2048, 5632], P('fs', 'tp'), may hold values from -0.125 to 0.125
- ffn_one_up: bfloat16 [2048, 5632], P('fs', 'tp'), may hold values from -0.125 to 0.125
- ffn_one_down: bfloat16 [5632, 2048], P('tp', 'fs'), may hold values from -0.078125 to 0.078125
- mix_gain: float32 [2048], replicated, may hold values from 0.1 to 1.9
- conv_value: bfloat16 [2048, 1024], P('fs', 'tp'), may hold values from -0.125 to 0.125
- conv_gate: bfloat16 [2048, 1024], P('fs', 'tp'), may hold values from -0.125 to 0.125
- conv_kernel: float32 [31, 1024], P(None, 'tp'), may hold values from -15 to 15
- conv_ln_gain: float32 [1024], P('tp'), may hold values from 0.1 to 1.9
- conv_out: bfloat16 [1024, 2048], P('tp', 'fs'), may hold values from -0.1875 to 0.1875
- ffn_two_gain: float32 [2048], replicated, may hold values from 0.1 to 1.9
- ffn_two_gate: bfloat16 [2048, 5632], P('fs', 'tp'), may hold values from -0.125 to 0.125
- ffn_two_up: bfloat16 [2048, 5632], P('fs', 'tp'), may hold values from -0.125 to 0.125
- ffn_two_down: bfloat16 [5632, 2048], P('tp', 'fs'), may hold values from -0.078125 to 0.078125
Outputs:
- layer_out: bfloat16 [6144, 2048], P('fs', 'tp')
All inputs are finite; a program needn't handle non-finite values.
Results may differ from a plain program's by a relative error of at most 0.017.
Values may be sent and summed in bfloat16 or wider, within the bound.
No kernel may reach another device: no remote copies, remote signals or barrier semaphores. Data moves between devices by JAX's collectives and lax.ppermute only.
A program may use at most 128 MiB of HBM per device.

v0:
```python
import jax
import jax.numpy as jnp
import numpy as np
from jax import lax
from jax.experimental import pallas as pl
from jax.experimental.pallas import tpu as pltpu
from jax.sharding import PartitionSpec as P


def spots_of(devices):
    return [tuple(getattr(device, "coords", (0, 0, place))) for place, device in enumerate(devices)]


def grid_ring(mesh):
    count = mesh.shape["fs"]
    spots = spots_of(mesh.devices.reshape(count, -1)[:, 0])
    xs = sorted({spot[0] for spot in spots})
    zs = sorted({spot[2] for spot in spots})
    if len(xs) < 2 or len(zs) % 2 or len(xs) * len(zs) != count:
        return list(range(count))
    where = {(spot[0], spot[2]): index for index, spot in enumerate(spots)}
    walk = [(xs[0], z) for z in zs]
    for turn, z in enumerate(reversed(zs)):
        inner = xs[1:] if turn % 2 == 0 else xs[:0:-1]
        walk += [(x, z) for x in inner]
    return [where[spot] for spot in walk]


def cores_of(mesh):
    spots = spots_of(mesh.devices.reshape(-1, mesh.shape["tp"])[0])
    cores = sum(spot == spots[0] for spot in spots)
    return cores if mesh.shape["tp"] % cores == 0 else 1


def tie(*values):
    return lax.optimization_barrier(values)


def spec(space):
    return pl.BlockSpec(memory_space=space)


def hidden_kernel(blocks, rows, sides, lanes, act, spots, turn, gain, *refs):
    tokens = refs[:blocks]
    shards = [refs[blocks + i * rows : blocks + (i + 1) * rows] for i in range(sides)]
    out, normed, left, right, sems = refs[blocks + sides * rows :]
    depth = shards[0][0].shape[0]
    width = left.shape[1]
    copies = []
    for which, whole in enumerate((left, right)):
        source = shards[which % sides]
        for slot in range(rows):
            at = pl.multiple_of(spots[slot] * depth, depth)
            copies.append(
                pltpu.make_async_copy(
                    source[slot].at[:, pl.ds(lanes[which], width)],
                    whole.at[pl.ds(at, depth), :],
                    sems.at[which, slot],
                )
            )
    for copy in copies:
        copy.start()

    count, size = tokens[0].shape
    step = 64 if count % 64 == 0 else count

    @pl.loop(0, count // step)
    def _(index):
        here = pl.ds(pl.multiple_of(index * step, step), step)
        parts = [token[here, :].astype(jnp.float32) for token in tokens]
        total = sum(jnp.sum(part * part, axis=1, keepdims=True) for part in parts)
        scale = lax.rsqrt(total / (size * blocks) + 1e-06)
        for place_at, part in enumerate(parts):
            scaled = part * scale * gain[turn[place_at]]
            normed[here, place_at * size : (place_at + 1) * size] = scaled.astype(jnp.bfloat16)

    for copy in copies:
        copy.wait()

    def product(whole, here):
        return jnp.dot(normed[...], whole[:, here], preferred_element_type=jnp.float32)

    tile = 256
    whole_tiles = width // tile

    @pl.loop(0, whole_tiles)
    def _(index):
        here = pl.ds(pl.multiple_of(index * tile, tile), tile)
        out[:, here] = act(product(left, here), product(right, here)).astype(out.dtype)

    rest = width - whole_tiles * tile
    if rest:
        here = pl.ds(whole_tiles * tile, rest)
        if rest % 128 == 0:
            both = jnp.concatenate([left[:, here], right[:, here]], axis=1)
            pair = jnp.dot(normed[...], both, preferred_element_type=jnp.float32)
            out[:, here] = act(pair[:, :rest], pair[:, rest:]).astype(out.dtype)
        else:
            out[:, here] = act(product(left, here), product(right, here)).astype(out.dtype)


def terms_kernel(slots, parts, low, cores, whose, where, inside, hidden, *refs):
    shards = refs[: slots * parts]
    outs = refs[slots * parts : slots * parts + cores]
    columns, sems = refs[slots * parts + cores :]
    width = columns.shape[2]
    copies = [
        pltpu.make_async_copy(
            shards[part * slots + slot].at[:, pl.ds(low, width)],
            columns.at[slot, pl.ds(part * shards[0].shape[0], shards[0].shape[0]), :],
            sems.at[part, slot],
        )
        for slot in range(slots)
        for part in range(parts)
    ]
    for copy in copies:
        copy.start()
    for copy in copies:
        copy.wait()

    @pl.loop(0, slots)
    def _(slot):
        value = jnp.dot(hidden[...], columns[slot], preferred_element_type=jnp.float32)
        value = value.astype(jnp.bfloat16)
        here = pl.ds(pl.multiple_of(inside[slot] * width, width), width)
        for core in range(cores):

            @pl.when(whose[slot] == core)
            def _(core=core):
                outs[core][where[slot], :, here] = value


def silu_times(gate, up):
    return gate / (1.0 + jnp.exp(-gate)) * up


def gate_times(gate, value):
    return value / (1.0 + jnp.exp(-gate))


class Ring:
    def __init__(self, order):
        count = len(order)
        after = {order[i]: order[(i + 1) % count] for i in range(count)}
        self.count = count
        self.forward = sorted(after.items())
        self.backward = sorted((b, a) for a, b in after.items())
        owners = np.zeros((count, count), np.int32)
        for place, index in enumerate(order):
            owners[index] = [order[(place + offset) % count] for offset in range(count)]
        row = lax.dynamic_slice_in_dim(jnp.asarray(owners), lax.axis_index("fs"), 1, axis=0)
        self.owners = row[0]


class Gathered:
    def __init__(self, ring, shard, onward):
        self.ring, self.onward = ring, onward
        self.ahead = self.behind = shard
        self.step = 0
        self.shards = {0: shard}

    def steps(self):
        return self.ring.count // 2

    def complete(self):
        return len(self.shards) == self.ring.count

    def ways(self):
        if self.step < self.ring.count - self.step:
            return (True, False)
        return (self.onward,)

    def sends(self):
        self.step += 1
        return [
            (self.ahead, self.ring.forward) if onward else (self.behind, self.ring.backward)
            for onward in self.ways()
        ]

    def accept(self, landed):
        for onward in self.ways():
            shard = landed.pop(0)
            if onward:
                self.ahead = shard
                self.shards[self.ring.count - self.step] = shard
            else:
                self.behind = shard
                self.shards[self.step] = shard

    def listed(self):
        return [self.shards[offset] for offset in range(self.ring.count)]


class Pump:
    def __init__(self, depth):
        self.depth = depth
        self.waiting = []
        self.flying = []
        self.sent = 0
        self.mark = lax.axis_index("fs")

    def add(self, *groups):
        steps = max(group[0].steps() for group in groups)
        for _ in range(steps):
            self.waiting += [list(group) for group in groups]

    def launch(self, value):
        group = self.waiting.pop(0)
        sends = [send for item in group for send in item.sends()]
        arrays, value = tie([array for array, _ in sends], value)
        landed = [lax.ppermute(a, "fs", way) for a, (_, way) in zip(arrays, sends)]
        self.flying.append((group, landed, self.sent))
        self.sent += 1
        return value

    def fill(self, value):
        while self.waiting and len(self.flying) < self.depth:
            value = self.launch(value)
        return value

    def until(self, items, value):
        while not all(item.complete() for item in items):
            value = self.turn(value)
        return value

    def turn(self, value, times=1):
        for _ in range(times):
            if not self.flying:
                return value
            group, landed, _ = self.flying.pop(0)
            landed, self.mark, value = tie(landed, self.mark, value)
            landed = list(landed)
            for item in group:
                item.accept(landed)
            self.mark, value = self.fill((self.mark, value))
            if len(self.flying) == self.depth:
                self.mark = self.mark + 1
                self.mark, value = tie(self.mark, value)
        return value


class Features:
    def __init__(self, count, cores):
        self.count, self.cores, self.chips = count, cores, count // cores
        index = lax.axis_index("tp")
        self.chip, self.core = index // cores, index % cores

    def across_core(self, value, shift):
        pairs = [
            (y * self.cores + c, y * self.cores + (c + shift) % self.cores)
            for y in range(self.chips)
            for c in range(self.cores)
        ]
        return lax.ppermute(value, "tp", pairs)

    def across_chip(self, value, shift):
        pairs = [
            (y * self.cores + c, (y + shift) % self.chips * self.cores + c)
            for y in range(self.chips)
            for c in range(self.cores)
        ]
        return lax.ppermute(value, "tp", pairs)

    def place_of(self, chip_shift, core_shift):
        chip = (self.chip - chip_shift + self.chips) % self.chips
        core = (self.core - core_shift + self.cores) % self.cores
        return chip * self.cores + core

    def gather_far(self, mine):
        return [mine] + [self.across_chip(mine, shift) for shift in range(1, self.chips)]

    def gather_near(self, far):
        return [
            self.across_core(piece, shift) if shift else piece
            for piece in far
            for shift in range(self.cores)
        ]

    def blocks(self):
        return jnp.stack(
            [
                (self.chip - chip + self.chips) % self.chips * self.cores
                + (self.core - core + self.cores) % self.cores
                for chip in range(self.chips)
                for core in range(self.cores)
            ]
        )

    def spots(self, owners, each):
        holder = owners // each
        chip = (self.chip - holder // self.cores + self.chips) % self.chips
        core = (self.core - holder % self.cores + self.cores) % self.cores
        return (chip * self.cores + core) * each + owners % each

    def targets(self, owners, each):
        holder = owners // each
        chip = (holder // self.cores - self.chip + self.chips) % self.chips
        core = (holder % self.cores - self.core + self.cores) % self.cores
        return core, chip, owners % each

    def scatter_near(self, terms):
        sent = [self.across_core(part, shift) for shift, part in enumerate(terms[1:], 1)]
        total = terms[0].astype(jnp.float32)
        for part in sent:
            total = total + part.astype(jnp.float32)
        return [total[0]] + [total[chip].astype(jnp.bfloat16) for chip in range(1, self.chips)]

    def scatter_far(self, sums):
        return [sums[0]] + [
            self.across_chip(total, shift) for shift, total in enumerate(sums[1:], 1)
        ]


def add_up(current, landed, factor):
    total = landed[0]
    for part in landed[1:]:
        total = total + part.astype(jnp.float32)
    return (current.astype(jnp.float32) + factor * total).astype(jnp.bfloat16)


def solution(mesh):
    order = grid_ring(mesh)
    cores = cores_of(mesh)
    depth = 2

    def per_device(
        tokens,
        ffn_one_gain,
        ffn_one_gate,
        ffn_one_up,
        ffn_one_down,
        mix_gain,
        conv_value,
        conv_gate,
        conv_kernel,
        conv_ln_gain,
        conv_out,
        ffn_two_gain,
        ffn_two_gate,
        ffn_two_up,
        ffn_two_down,
    ):
        ring = Ring(order)
        features = Features(lax.axis_size("tp"), cores)
        channels = conv_ln_gain.shape[0] * lax.axis_size("tp")
        pump = Pump(depth)
        wide = conv_value.shape[1]
        half = ffn_two_down.shape[0] // 2
        one_gate = Gathered(ring, ffn_one_gate, True)
        one_up = Gathered(ring, ffn_one_up, False)
        one_down = Gathered(ring, ffn_one_down, True)
        if conv_value.shape[0] == conv_out.shape[0]:
            mixed = jnp.concatenate([conv_value, conv_gate, conv_out], axis=1)
            mix_in = mix_out = Gathered(ring, mixed, False)
            mixes, out_from = [mix_in], 2 * wide
        else:
            mix_in = Gathered(ring, jnp.concatenate([conv_value, conv_gate], axis=1), False)
            mix_out, out_from = Gathered(ring, conv_out, False), 0
            mixes = [mix_in, mix_out]
        two_gate = Gathered(ring, ffn_two_gate, True)
        two_up = Gathered(ring, ffn_two_up, False)
        two_down = [
            Gathered(ring, ffn_two_down[:half], True),
            Gathered(ring, ffn_two_down[half:], False),
        ]
        pump.add([one_gate], [one_up])
        pump.add([one_down], mixes)
        pump.add([two_gate], [two_up])
        pump.add([two_down[0]], [two_down[1]])

        count = features.count
        each = ring.count // count
        blocks = features.blocks()
        spots = features.spots(ring.owners, each)
        targets = features.targets(ring.owners, each)
        vmem, smem, hbm = pltpu.VMEM, pltpu.SMEM, pltpu.HBM

        def hidden_of(parts, gain_vec, sides, lanes, width, act, dtype):
            length, size = parts[0].shape
            rows = count * size
            arrays = [shard for side in sides for shard in side.listed()]
            return pl.pallas_call(
                lambda *refs: hidden_kernel(
                    count, ring.count, len(sides), lanes, act, *refs
                ),
                out_shape=jax.ShapeDtypeStruct((length, width), dtype),
                in_specs=[spec(smem)] * 2 + [spec(vmem)] * (1 + count) + [spec(hbm)] * len(arrays),
                out_specs=spec(vmem),
                scratch_shapes=[
                    pltpu.VMEM((length, rows), jnp.bfloat16),
                    pltpu.VMEM((rows, width), jnp.bfloat16),
                    pltpu.VMEM((rows, width), jnp.bfloat16),
                    pltpu.SemaphoreType.DMA((2, ring.count)),
                ],
                cost_estimate=pl.CostEstimate(
                    flops=4 * length * rows * width,
                    bytes_accessed=4 * rows * width + 2 * length * rows,
                    transcendentals=length * width,
                ),
                name="hidden",
            )(spots, blocks, gain_vec.reshape(count, 1, size), *parts, *arrays)

        def terms_of(hidden, sides, low, width):
            length, depth_all = hidden.shape
            arrays = [shard for side in sides for shard in side.listed()]
            out = jax.ShapeDtypeStruct((features.chips, length, each * width), jnp.bfloat16)
            return pl.pallas_call(
                lambda *refs: terms_kernel(ring.count, len(sides), low, cores, *refs),
                out_shape=[out] * cores,
                in_specs=[spec(smem)] * 3 + [spec(vmem)] + [spec(hbm)] * len(arrays),
                out_specs=[spec(vmem)] * cores,
                scratch_shapes=[
                    pltpu.VMEM((ring.count, depth_all, width), jnp.bfloat16),
                    pltpu.SemaphoreType.DMA((len(sides), ring.count)),
                ],
                cost_estimate=pl.CostEstimate(
                    flops=2 * length * depth_all * ring.count * width,
                    bytes_accessed=2 * depth_all * ring.count * width,
                    transcendentals=0,
                ),
                name="terms",
            )(*targets, hidden, *arrays)

        tokens = pump.fill(tokens)
        far = features.gather_far(tokens)
        far = pump.turn(far)
        parts = features.gather_near(far)
        parts = pump.until([one_gate, one_up], parts)
        hidden = hidden_of(
            parts, ffn_one_gain, [one_gate, one_up], (0, 0), ffn_one_up.shape[1], silu_times,
            jnp.bfloat16,
        )
        hidden = pump.until([one_down], hidden)
        terms = terms_of(hidden, [one_down], 0, ffn_one_down.shape[1])
        sums = pump.turn(features.scatter_near(terms))
        landed = features.scatter_far(sums)
        pump.turn(())
        stream_one = add_up(tokens, landed, 0.5)

        stream_one = pump.until(mixes, stream_one)
        far = features.gather_far(stream_one)
        pump.turn((), 2)
        parts = pump.turn(features.gather_near(far))
        gated_lin = hidden_of(
            parts, mix_gain, [mix_in], (wide, 0), wide, gate_times, jnp.float32
        )
        half_span = conv_kernel.shape[0] // 2
        convolved = lax.conv_general_dilated(
            gated_lin[None],
            conv_kernel[:, None, :],
            (1,),
            [(half_span, half_span)],
            dimension_numbers=("NWC", "WIO", "NWC"),
            feature_group_count=gated_lin.shape[1],
            precision=lax.Precision.HIGHEST,
        )[0]
        convolved = pump.turn(convolved)
        sum_one, sum_two = lax.psum(
            (jnp.sum(convolved, axis=1), jnp.sum(convolved * convolved, axis=1)), "tp"
        )
        mean_val = (sum_one / channels)[:, None]
        varied = (sum_two / channels)[:, None] - mean_val * mean_val
        active = jax.nn.silu(
            (convolved - mean_val) * lax.rsqrt(varied + 1e-05) * conv_ln_gain
        ).astype(jnp.bfloat16)
        terms = terms_of(active, [mix_out], out_from, conv_out.shape[1])
        sums = pump.turn(features.scatter_near(terms))
        landed = features.scatter_far(sums)
        pump.turn(())
        stream_two = pump.turn(add_up(stream_one, landed, 1.0))

        far = features.gather_far(stream_two)
        pump.turn((), 2)
        parts = features.gather_near(far)
        parts = pump.until([two_gate, two_up], parts)
        hidden = hidden_of(
            parts, ffn_two_gain, [two_gate, two_up], (0, 0), ffn_two_up.shape[1], silu_times,
            jnp.bfloat16,
        )
        hidden = pump.until(two_down, hidden)
        terms = terms_of(hidden, two_down, 0, ffn_two_down.shape[1])
        landed = features.scatter_far(features.scatter_near(terms))
        return jnp.where(pump.mark < 0, stream_two, add_up(stream_two, landed, 0.5))

    in_specs = (
        P("fs", "tp"),
        P(),
        P("fs", "tp"),
        P("fs", "tp"),
        P("tp", "fs"),
        P(),
        P("fs", "tp"),
        P("fs", "tp"),
        P(None, "tp"),
        P("tp"),
        P("tp", "fs"),
        P(),
        P("fs", "tp"),
        P("fs", "tp"),
        P("tp", "fs"),
    )
    return jax.shard_map(
        per_device, mesh=mesh, in_specs=in_specs, out_specs=P("fs", "tp"), check_vma=False
    )
```

profile of v0, /device:TPU:0, one launch (start us, length us, event | category | flops | bytes accessed | tf_op | source)
XLA Modules:
  0.0 508.4 jit_solution(15566622998148802430)
XLA Ops:
  5.0 15.8 %collective-permute-done.2.refs_14_ = bf16[256,1408]{1,0:T(8,128)(2,1)S(1)} collective-permute-done((bf16[256,1408]{1,0:T(8,128)(2,1)}, bf16[256,1408]{1,0:T(8,128)(2,1)S(1)}, u32[]{:S(2)}, u32[]{:S(2)}) %collective-permute-start.2) | collective-permute-done | bytes 720928 | tf_op jit(solution)/shard_map/ppermute | solution.py:211
  26.0 15.9 %collective-permute-done.refs_22_ = bf16[256,1408]{1,0:T(8,128)(2,1)} collective-permute-done((bf16[256,1408]{1,0:T(8,128)(2,1)}, bf16[256,1408]{1,0:T(8,128)(2,1)}, u32[]{:S(2)}, u32[]{:S(2)}) %collective-permute-start) | collective-permute-done | bytes 720928 | tf_op jit(solution)/shard_map/ppermute | solution.py:211
  46.5 13.3 %collective-permute-done.10.refs_9_ = bf16[256,1408]{1,0:T(8,128)(2,1)} collective-permute-done((bf16[256,1408]{1,0:T(8,128)(2,1)}, bf16[256,1408]{1,0:T(8,128)(2,1)}, u32[]{:S(2)}, u32[]{:S(2)}) %collective-permute-start.10) | collective-permute-done | bytes 720928 | tf_op jit(solution)/shard_map/ppermute | solution.py:211
  63.0 13.4 %collective-permute-done.7.refs_21_ = bf16[256,1408]{1,0:T(8,128)(2,1)} collective-permute-done((bf16[256,1408]{1,0:T(8,128)(2,1)}, bf16[256,1408]{1,0:T(8,128)(2,1)}, u32[]{:S(2)}, u32[]{:S(2)}) %collective-permute-start.7) | collective-permute-done | bytes 720928 | tf_op jit(solution)/shard_map/ppermute | solution.py:211
  80.6 11.3 %collective-permute-done.13.refs_12_ = bf16[256,1408]{1,0:T(8,128)(2,1)} collective-permute-done((bf16[256,1408]{1,0:T(8,128)(2,1)}, bf16[256,1408]{1,0:T(8,128)(2,1)}, u32[]{:S(2)}, u32[]{:S(2)}) %collective-permute-start.13) | collective-permute-done | bytes 720928 | tf_op jit(solution)/shard_map/ppermute | solution.py:211
  93.5 13.9 %collective-permute-done.11.refs_20_ = bf16[256,1408]{1,0:T(8,128)(2,1)} collective-permute-done((bf16[256,1408]{1,0:T(8,128)(2,1)}, bf16[256,1408]{1,0:T(8,128)(2,1)}, u32[]{:S(2)}, u32[]{:S(2)}) %collective-permute-start.11) | collective-permute-done | bytes 720928 | tf_op jit(solution)/shard_map/ppermute | solution.py:211
  112.1 8.9 %collective-permute-done.16.refs_11_ = bf16[256,1408]{1,0:T(8,128)(2,1)} collective-permute-done((bf16[256,1408]{1,0:T(8,128)(2,1)}, bf16[256,1408]{1,0:T(8,128)(2,1)}, u32[]{:S(2)}, u32[]{:S(2)}) %collective-permute-start.16) | collective-permute-done | bytes 720928 | tf_op jit(solution)/shard_map/ppermute | solution.py:211
  123.0 17.7 %hidden.3.refs_3_ = bf16[768,1408]{1,0:T(8,128)(2,1)} custom-call(s32[8]{0:T(128)} %get-tuple-element.661.refs_0_, s32[4]{0:T(128)} %pad_add_fusion.refs_1_, f32[4,1,512]{2,1,0:T(1,128)} %bitcast.52, bf16[768,512]{1,0:T(8,128)(2,1)} %refs_3_, bf16[768,512]{1,0:T(8,128)(2,1)} %copy-done.18, bf16[768,512]{1,0:T(8,128)(2,1)} %copy-done.17, ...), custom_call_target="tpu_custom_call" | custom-call | flops 8858370048 | bytes 14680064 | tf_op jit(solution)/shard_map/hidden/pallas_call | solution.py:382
  144.9 20.4 %collective-permute-done.17.refs_14_.refs_11_ = bf16[256,768]{1,0:T(8,128)(2,1)S(1)} collective-permute-done((bf16[256,768]{1,0:T(8,128)(2,1)S(1)}, bf16[256,768]{1,0:T(8,128)(2,1)S(1)}, u32[]{:S(2)}, u32[]{:S(2)}) %collective-permute-start.17) | collective-permute-done | bytes 393248 | tf_op jit(solution)/shard_map/ppermute | solution.py:211
  170.7 19.1 %collective-permute-done.21.refs_13_.refs_10_ = bf16[256,768]{1,0:T(8,128)(2,1)S(1)} collective-permute-done((bf16[256,768]{1,0:T(8,128)(2,1)S(1)}, bf16[256,768]{1,0:T(8,128)(2,1)S(1)}, u32[]{:S(2)}, u32[]{:S(2)}) %collective-permute-start.21) | collective-permute-done | bytes 393248 | tf_op jit(solution)/shard_map/ppermute | solution.py:211
  195.4 18.1 %collective-permute-done.25.refs_12_.refs_9_ = bf16[256,768]{1,0:T(8,128)(2,1)S(1)} collective-permute-done((bf16[256,768]{1,0:T(8,128)(2,1)S(1)}, bf16[256,768]{1,0:T(8,128)(2,1)S(1)}, u32[]{:S(2)}, u32[]{:S(2)}) %collective-permute-start.25) | collective-permute-done | bytes 393248 | tf_op jit(solution)/shard_map/ppermute | solution.py:211
  213.6 12.7 %terms.3 = (bf16[2,768,512]{2,1,0:T(8,128)(2,1)}, bf16[2,768,512]{2,1,0:T(8,128)(2,1)}) custom-call(s32[8]{0:T(128)} %get-tuple-element.660.refs_0_, s32[8]{0:T(128)} %get-tuple-element.653.refs_1_, s32[8]{0:T(128)} %get-tuple-element.651.refs_2_, bf16[768,1408]{1,0:T(8,128)(2,1)} %hidden.3.refs_3_, bf16[1408,256]{1,0:T(8,128)(2,1)} %refs_4_.1, ...), custom_call_target="tpu_custom_call" | custom-call | flops 4429185024 | bytes 5767168 | tf_op jit(solution)/shard_map/terms/pallas_call | solution.py:407
  232.1 6.0 %collective-permute-done.29.refs_11_.refs_8_ = bf16[256,768]{1,0:T(8,128)(2,1)S(1)} collective-permute-done((bf16[256,768]{1,0:T(8,128)(2,1)}, bf16[256,768]{1,0:T(8,128)(2,1)S(1)}, u32[]{:S(2)}, u32[]{:S(2)}) %collective-permute-start.29) | collective-permute-done | bytes 393248 | tf_op jit(solution)/shard_map/ppermute | solution.py:211
  240.7 16.5 %collective-permute-done.40 = bf16[768,512]{1,0:T(8,128)(2,1)S(1)} collective-permute-done((bf16[768,512]{1,0:T(8,128)(2,1)S(1)}, bf16[768,512]{1,0:T(8,128)(2,1)S(1)}, u32[]{:S(2)}, u32[]{:S(2)}) %collective-permute-start.40) | collective-permute-done | bytes 786464 | tf_op jit(solution)/shard_map/ppermute | solution.py:262
  263.3 15.3 %collective-permute-done.32.refs_22_ = bf16[256,1408]{1,0:T(8,128)(2,1)} collective-permute-done((bf16[256,1408]{1,0:T(8,128)(2,1)}, bf16[256,1408]{1,0:T(8,128)(2,1)}, u32[]{:S(2)}, u32[]{:S(2)}) %collective-permute-start.32) | collective-permute-done | bytes 720928 | tf_op jit(solution)/shard_map/ppermute | solution.py:211
  283.0 11.1 %collective-permute-done.38.refs_13_ = bf16[256,1408]{1,0:T(8,128)(2,1)} collective-permute-done((bf16[256,1408]{1,0:T(8,128)(2,1)}, bf16[256,1408]{1,0:T(8,128)(2,1)}, u32[]{:S(2)}, u32[]{:S(2)}) %collective-permute-start.38) | collective-permute-done | bytes 720928 | tf_op jit(solution)/shard_map/ppermute | solution.py:211
  296.1 13.4 %collective-permute-done.36.refs_21_ = bf16[256,1408]{1,0:T(8,128)(2,1)} collective-permute-done((bf16[256,1408]{1,0:T(8,128)(2,1)}, bf16[256,1408]{1,0:T(8,128)(2,1)}, u32[]{:S(2)}, u32[]{:S(2)}) %collective-permute-start.36) | collective-permute-done | bytes 720928 | tf_op jit(solution)/shard_map/ppermute | solution.py:211
  311.1 6.8 %hidden.4 = f32[768,256]{1,0:T(8,128)} custom-call(s32[8]{0:T(128)} %get-tuple-element.661.refs_0_, s32[4]{0:T(128)} %pad_add_fusion.refs_1_, f32[4,1,512]{2,1,0:T(1,128)} %bitcast.51, bf16[768,512]{1,0:T(8,128)(2,1)} %copy-done.2, bf16[768,512]{1,0:T(8,128)(2,1)} %copy-done.13, bf16[768,512]{1,0:T(8,128)(2,1)} %copy-done.12, bf16[768,512]{1,0:T(8,128)(2,1)} %copy-done.14, ...), custom_call_target="tpu_custom_call" | custom-call | flops 1610612736 | bytes 5242880 | tf_op jit(solution)/shard_map/hidden/pallas_call | solution.py:382
  317.9 6.9 %fusion.8 = f32[1,768,256]{2,0,1:T(1,128)S(1)} fusion(f32[1,768,256]{2,1,0:T(8,128)} %bitcast.50, f32[31,1,256]{2,0,1:T(8,128)S(1)} %bitcast.47), kind=kOutput, calls=%fused_computation.20 | convolution fusion | flops 72400896 | bytes 1604608 | tf_op jit(solution)/shard_map/conv_general_dilated | solution.py:448
  325.2 6.0 %all-reduce = (f32[768]{0:T(1024)S(1)}, f32[768]{0:T(1024)S(1)}) all-reduce(f32[768]{0:T(1024)S(1)} %get-tuple-element.648, f32[768]{0:T(1024)S(1)} %get-tuple-element.647), channel_id=1, replica_groups=mesh['fs'=8,'tp'=4] {'tp'}, use_global_device_ids=true, to_apply=%region_3.4 | all-reduce | flops 1536 | bytes 12288 | tf_op jit(solution)/shard_map/psum | solution.py:458
  332.3 6.5 %terms.4 = (bf16[2,768,512]{2,1,0:T(8,128)(2,1)}, bf16[2,768,512]{2,1,0:T(8,128)(2,1)}) custom-call(s32[8]{0:T(128)} %get-tuple-element.660.refs_0_, s32[8]{0:T(128)} %get-tuple-element.653.refs_1_, s32[8]{0:T(128)} %get-tuple-element.651.refs_2_, bf16[768,256]{1,0:T(8,128)(2,1)} %multiply_convert_fusion.refs_3_, bf16[256,768]{1,0:T(8,128)(2,1)} %copy-done.5, ...), custom_call_target="tpu_custom_call" | custom-call | flops 805306368 | bytes 1048576 | tf_op jit(solution)/shard_map/terms/pallas_call | solution.py:407
  344.6 13.1 %collective-permute-done.44.refs_20_ = bf16[256,1408]{1,0:T(8,128)(2,1)} collective-permute-done((bf16[256,1408]{1,0:T(8,128)(2,1)}, bf16[256,1408]{1,0:T(8,128)(2,1)}, u32[]{:S(2)}, u32[]{:S(2)}) %collective-permute-start.44) | collective-permute-done | bytes 720928 | tf_op jit(solution)/shard_map/ppermute | solution.py:211
  364.6 13.5 %collective-permute-done.50.refs_11_ = bf16[256,1408]{1,0:T(8,128)(2,1)} collective-permute-done((bf16[256,1408]{1,0:T(8,128)(2,1)}, bf16[256,1408]{1,0:T(8,128)(2,1)}, u32[]{:S(2)}, u32[]{:S(2)}) %collective-permute-start.50) | collective-permute-done | bytes 720928 | tf_op jit(solution)/shard_map/ppermute | solution.py:211
  381.1 16.2 %collective-permute-done.61.refs_5_ = bf16[768,512]{1,0:T(8,128)(2,1)S(1)} collective-permute-done((bf16[768,512]{1,0:T(8,128)(2,1)S(1)}, bf16[768,512]{1,0:T(8,128)(2,1)S(1)}, u32[]{:S(2)}, u32[]{:S(2)}) %collective-permute-start.61) | collective-permute-done | bytes 786464 | tf_op jit(solution)/shard_map/ppermute | solution.py:262
  400.9 7.8 %collective-permute-done.54.refs_11_ = bf16[704,256]{1,0:T(8,128)(2,1)} collective-permute-done((bf16[704,256]{1,0:T(8,128)(2,1)S(1)}, bf16[704,256]{1,0:T(8,128)(2,1)}, u32[]{:S(2)}, u32[]{:S(2)}) %collective-permute-start.54) | collective-permute-done | bytes 360480 | tf_op jit(solution)/shard_map/ppermute | solution.py:211
  411.7 4.7 collective-permute-done.52.refs_19_
  421.5 17.7 %hidden.5.refs_3_ = bf16[768,1408]{1,0:T(8,128)(2,1)} custom-call(s32[8]{0:T(128)} %get-tuple-element.661.refs_0_, s32[4]{0:T(128)} %pad_add_fusion.refs_1_, f32[4,1,512]{2,1,0:T(1,128)} %bitcast.53, bf16[768,512]{1,0:T(8,128)(2,1)} %copy-done.4, bf16[768,512]{1,0:T(8,128)(2,1)} %copy-done.21, bf16[768,512]{1,0:T(8,128)(2,1)} %copy-done.20, ...), custom_call_target="tpu_custom_call" | custom-call | flops 8858370048 | bytes 14680064 | tf_op jit(solution)/shard_map/hidden/pallas_call | solution.py:382
  443.4 7.2 %collective-permute-done.65.refs_9_ = bf16[704,256]{1,0:T(8,128)(2,1)S(1)} collective-permute-done((bf16[704,256]{1,0:T(8,128)(2,1)S(1)}, bf16[704,256]{1,0:T(8,128)(2,1)S(1)}, u32[]{:S(2)}, u32[]{:S(2)}) %collective-permute-start.65) | collective-permute-done | bytes 360480 | tf_op jit(solution)/shard_map/ppermute | solution.py:211
  458.7 5.4 %collective-permute-done.68.refs_8_ = bf16[704,256]{1,0:T(8,128)(2,1)S(1)} collective-permute-done((bf16[704,256]{1,0:T(8,128)(2,1)S(1)}, bf16[704,256]{1,0:T(8,128)(2,1)S(1)}, u32[]{:S(2)}, u32[]{:S(2)}) %collective-permute-start.68) | collective-permute-done | bytes 360480 | tf_op jit(solution)/shard_map/ppermute | solution.py:211
  466.5 12.6 %terms.5 = (bf16[2,768,512]{2,1,0:T(8,128)(2,1)}, bf16[2,768,512]{2,1,0:T(8,128)(2,1)}) custom-call(s32[8]{0:T(128)} %get-tuple-element.660.refs_0_, s32[8]{0:T(128)} %get-tuple-element.653.refs_1_, s32[8]{0:T(128)} %get-tuple-element.651.refs_2_, bf16[768,1408]{1,0:T(8,128)(2,1)} %hidden.5.refs_3_, bf16[704,256]{1,0:T(8,128)(2,1)} %copy-done.15, ...), custom_call_target="tpu_custom_call" | custom-call | flops 4429185024 | bytes 5767168 | tf_op jit(solution)/shard_map/terms/pallas_call | solution.py:407
  479.1 3.6 collective-permute-done.69
  487.3 18.2 %collective-permute-done.70 = bf16[768,512]{1,0:T(8,128)(2,1)} collective-permute-done((bf16[768,512]{1,0:T(8,128)(2,1)}, bf16[768,512]{1,0:T(8,128)(2,1)}, u32[]{:S(2)}, u32[]{:S(2)}) %collective-permute-start.70) | collective-permute-done | bytes 786464 | tf_op jit(solution)/shard_map/ppermute | solution.py:262
  (213 shorter events, 119.0 us)
Async XLA Ops:
  0.0 22.1 %collective-permute-start.4 = (bf16[768,512]{1,0:T(8,128)(2,1)}, bf16[768,512]{1,0:T(8,128)(2,1)S(1)}, u32[]{:S(2)}, u32[]{:S(2)}) collective-permute-start(bf16[768,512]{1,0:T(8,128)(2,1)} %refs_3_), channel_id=1, source_target_pairs={{0,2},{1,3},{2,0},{3,1},{4,6},{5,7},{6,4},{7,5},{8,10},{9,11},{10,... | collective-permute-start | bytes 2359304 | tf_op jit(solution)/shard_map/ppermute | solution.py:262
  23.0 21.4 %collective-permute-start.5 = (bf16[768,512]{1,0:T(8,128)(2,1)}, bf16[768,512]{1,0:T(8,128)(2,1)S(1)}, u32[]{:S(2)}, u32[]{:S(2)}) collective-permute-start(bf16[768,512]{1,0:T(8,128)(2,1)} %refs_3_), channel_id=1, source_target_pairs={{0,1},{1,0},{2,3},{3,2},{4,5},{5,4},{6,7},{7,6},{8,9},{9,8},{10,11... | collective-permute-start | bytes 2359304 | tf_op jit(solution)/shard_map/ppermute | solution.py:254
  23.0 21.4 %collective-permute-start.6 = (bf16[768,512]{1,0:T(8,128)(2,1)S(1)}, bf16[768,512]{1,0:T(8,128)(2,1)S(1)}, u32[]{:S(2)}, u32[]{:S(2)}) collective-permute-start(bf16[768,512]{1,0:T(8,128)(2,1)S(1)} %collective-permute-done.4.refs_5_), channel_id=1, source_target_pairs={{0,1},{1,0},{2,3},{3,2},{4,5},{5,4},{6,7},{7,6},{8,9},{9,8},{10,11... | collective-permute-start | bytes 2359304 | tf_op jit(solution)/shard_map/ppermute | solution.py:254
  25.6 34.3 %collective-permute-start.10 = (bf16[256,1408]{1,0:T(8,128)(2,1)}, bf16[256,1408]{1,0:T(8,128)(2,1)}, u32[]{:S(2)}, u32[]{:S(2)}) collective-permute-start(bf16[256,1408]{1,0:T(8,128)(2,1)} %copy-done.25), channel_id=1, source_target_pairs={{0,4},{4,12},{8,0},{12,20},{16,8},{20,28},{24,16},{28,24},{1,5},{5... | collective-permute-start | bytes 2162696 | tf_op jit(solution)/shard_map/ppermute | solution.py:211
  44.5 32.0 %collective-permute-start.7 = (bf16[256,1408]{1,0:T(8,128)(2,1)}, bf16[256,1408]{1,0:T(8,128)(2,1)}, u32[]{:S(2)}, u32[]{:S(2)}) collective-permute-start(bf16[256,1408]{1,0:T(8,128)(2,1)} %collective-permute-done.refs_22_), channel_id=1, source_target_pairs={{0,8},{4,0},{8,16},{12,4},{16,24},{20,12},{24,28},{28,20},{1,9},{5... | collective-permute-start | bytes 2162696 | tf_op jit(solution)/shard_map/ppermute | solution.py:211
  46.1 30.4 %collective-permute-start.8 = (bf16[256,1408]{1,0:T(8,128)(2,1)}, bf16[256,1408]{1,0:T(8,128)(2,1)}, u32[]{:S(2)}, u32[]{:S(2)}) collective-permute-start(bf16[256,1408]{1,0:T(8,128)(2,1)} %collective-permute-done.1.refs_16_), channel_id=1, source_target_pairs={{0,4},{4,12},{8,0},{12,20},{16,8},{20,28},{24,16},{28,24},{1,5},{5... | collective-permute-start | bytes 2162696 | tf_op jit(solution)/shard_map/ppermute | solution.py:211
  61.0 30.9 %collective-permute-start.13 = (bf16[256,1408]{1,0:T(8,128)(2,1)}, bf16[256,1408]{1,0:T(8,128)(2,1)}, u32[]{:S(2)}, u32[]{:S(2)}) collective-permute-start(bf16[256,1408]{1,0:T(8,128)(2,1)} %collective-permute-done.9.refs_13_), channel_id=1, source_target_pairs={{0,8},{4,0},{8,16},{12,4},{16,24},{20,12},{24,28},{28,20},{1,9},{5... | collective-permute-start | bytes 2162696 | tf_op jit(solution)/shard_map/ppermute | solution.py:211
  62.6 29.3 %collective-permute-start.14 = (bf16[256,1408]{1,0:T(8,128)(2,1)}, bf16[256,1408]{1,0:T(8,128)(2,1)}, u32[]{:S(2)}, u32[]{:S(2)}) collective-permute-start(bf16[256,1408]{1,0:T(8,128)(2,1)} %collective-permute-done.10.refs_9_), channel_id=1, source_target_pairs={{0,4},{4,12},{8,0},{12,20},{16,8},{20,28},{24,16},{28,24},{1,5},{5... | collective-permute-start | bytes 2162696 | tf_op jit(solution)/shard_map/ppermute | solution.py:211
  76.5 30.9 %collective-permute-start.11 = (bf16[256,1408]{1,0:T(8,128)(2,1)}, bf16[256,1408]{1,0:T(8,128)(2,1)}, u32[]{:S(2)}, u32[]{:S(2)}) collective-permute-start(bf16[256,1408]{1,0:T(8,128)(2,1)} %collective-permute-done.7.refs_21_), channel_id=1, source_target_pairs={{0,8},{4,0},{8,16},{12,4},{16,24},{20,12},{24,28},{28,20},{1,9},{5... | collective-permute-start | bytes 2162696 | tf_op jit(solution)/shard_map/ppermute | solution.py:211
  78.0 29.3 %collective-permute-start.12 = (bf16[256,1408]{1,0:T(8,128)(2,1)}, bf16[256,1408]{1,0:T(8,128)(2,1)}, u32[]{:S(2)}, u32[]{:S(2)}) collective-permute-start(bf16[256,1408]{1,0:T(8,128)(2,1)} %collective-permute-done.8.refs_17_), channel_id=1, source_target_pairs={{0,4},{4,12},{8,0},{12,20},{16,8},{20,28},{24,16},{28,24},{1,5},{5... | collective-permute-start | bytes 2162696 | tf_op jit(solution)/shard_map/ppermute | solution.py:211
  91.9 29.1 %collective-permute-start.16 = (bf16[256,1408]{1,0:T(8,128)(2,1)}, bf16[256,1408]{1,0:T(8,128)(2,1)}, u32[]{:S(2)}, u32[]{:S(2)}) collective-permute-start(bf16[256,1408]{1,0:T(8,128)(2,1)} %collective-permute-done.13.refs_12_), channel_id=1, source_target_pairs={{0,8},{4,0},{8,16},{12,4},{16,24},{20,12},{24,28},{28,20},{1,9},{5... | collective-permute-start | bytes 2162696 | tf_op jit(solution)/shard_map/ppermute | solution.py:211
  140.8 25.8 %collective-permute-start.23 = (bf16[1408,256]{1,0:T(8,128)(2,1)}, bf16[1408,256]{1,0:T(8,128)(2,1)S(1)}, u32[]{:S(2)}, u32[]{:S(2)}) collective-permute-start(bf16[1408,256]{1,0:T(8,128)(2,1)} %collective-permute-done.19.refs_11_), channel_id=1, source_target_pairs={{0,8},{4,0},{8,16},{12,4},{16,24},{20,12},{24,28},{28,20},{1,9},{5... | collective-permute-start | bytes 2162696 | tf_op jit(solution)/shard_map/ppermute | solution.py:211
  142.4 24.1 %collective-permute-start.24 = (bf16[1408,256]{1,0:T(8,128)(2,1)}, bf16[1408,256]{1,0:T(8,128)(2,1)}, u32[]{:S(2)}, u32[]{:S(2)}) collective-permute-start(bf16[1408,256]{1,0:T(8,128)(2,1)} %collective-permute-done.20.refs_5_), channel_id=1, source_target_pairs={{0,4},{4,12},{8,0},{12,20},{16,8},{20,28},{24,16},{28,24},{1,5},{5... | collective-permute-start | bytes 2162696 | tf_op jit(solution)/shard_map/ppermute | solution.py:211
  142.9 22.4 %collective-permute-start.17 = (bf16[256,768]{1,0:T(8,128)(2,1)S(1)}, bf16[256,768]{1,0:T(8,128)(2,1)S(1)}, u32[]{:S(2)}, u32[]{:S(2)}) collective-permute-start(bf16[256,768]{1,0:T(8,128)(2,1)S(1)} %constant_dynamic-update-slice_fusion.refs_7_.refs_4_), channel_id=1, source_target_pairs={{0,8},{4,0},{8,16},{12,4},{16,24},{20,12},{24,28},{28,20},{1,9},{5... | collective-permute-start | bytes 1179656 | tf_op jit(solution)/shard_map/ppermute | solution.py:211
  144.5 22.1 %collective-permute-start.18 = (bf16[256,768]{1,0:T(8,128)(2,1)S(1)}, bf16[256,768]{1,0:T(8,128)(2,1)S(1)}, u32[]{:S(2)}, u32[]{:S(2)}) collective-permute-start(bf16[256,768]{1,0:T(8,128)(2,1)S(1)} %constant_dynamic-update-slice_fusion.refs_7_.refs_4_), channel_id=1, source_target_pairs={{0,4},{4,12},{8,0},{12,20},{16,8},{20,28},{24,16},{28,24},{1,5},{5... | collective-permute-start | bytes 1179656 | tf_op jit(solution)/shard_map/ppermute | solution.py:211
  166.6 24.6 %collective-permute-start.27 = (bf16[1408,256]{1,0:T(8,128)(2,1)S(1)}, bf16[1408,256]{1,0:T(8,128)(2,1)}, u32[]{:S(2)}, u32[]{:S(2)}) collective-permute-start(bf16[1408,256]{1,0:T(8,128)(2,1)S(1)} %collective-permute-done.23.refs_10_), channel_id=1, source_target_pairs={{0,8},{4,0},{8,16},{12,4},{16,24},{20,12},{24,28},{28,20},{1,9},{5... | collective-permute-start | bytes 2162696 | tf_op jit(solution)/shard_map/ppermute | solution.py:211
  168.2 23.0 %collective-permute-start.28 = (bf16[1408,256]{1,0:T(8,128)(2,1)}, bf16[1408,256]{1,0:T(8,128)(2,1)}, u32[]{:S(2)}, u32[]{:S(2)}) collective-permute-start(bf16[1408,256]{1,0:T(8,128)(2,1)} %collective-permute-done.24.refs_6_), channel_id=1, source_target_pairs={{0,4},{4,12},{8,0},{12,20},{16,8},{20,28},{24,16},{28,24},{1,5},{5... | collective-permute-start | bytes 2162696 | tf_op jit(solution)/shard_map/ppermute | solution.py:211
  191.2 22.4 %collective-permute-start.30 = (bf16[1408,256]{1,0:T(8,128)(2,1)}, bf16[1408,256]{1,0:T(8,128)(2,1)}, u32[]{:S(2)}, u32[]{:S(2)}) collective-permute-start(bf16[1408,256]{1,0:T(8,128)(2,1)} %collective-permute-done.27.refs_9_), channel_id=1, source_target_pairs={{0,8},{4,0},{8,16},{12,4},{16,24},{20,12},{24,28},{28,20},{1,9},{5... | collective-permute-start | bytes 2162696 | tf_op jit(solution)/shard_map/ppermute | solution.py:211
  238.6 22.7 %collective-permute-start.34 = (bf16[256,1408]{1,0:T(8,128)(2,1)S(1)}, bf16[256,1408]{1,0:T(8,128)(2,1)}, u32[]{:S(2)}, u32[]{:S(2)}) collective-permute-start(bf16[256,1408]{1,0:T(8,128)(2,1)S(1)} %copy-done.23), channel_id=1, source_target_pairs={{0,8},{4,0},{8,16},{12,4},{16,24},{20,12},{24,28},{28,20},{1,9},{5... | collective-permute-start | bytes 2162696 | tf_op jit(solution)/shard_map/ppermute | solution.py:211
  258.7 23.8 %collective-permute-start.42 = (bf16[768,512]{1,0:T(8,128)(2,1)S(1)}, bf16[768,512]{1,0:T(8,128)(2,1)S(1)}, u32[]{:S(2)}, u32[]{:S(2)}) collective-permute-start(bf16[768,512]{1,0:T(8,128)(2,1)S(1)} %add_convert_fusion.1.refs_3_), channel_id=1, source_target_pairs={{0,2},{1,3},{2,0},{3,1},{4,6},{5,7},{6,4},{7,5},{8,10},{9,11},{10,... | collective-permute-start | bytes 2359304 | tf_op jit(solution)/shard_map/ppermute | solution.py:262
  261.3 32.7 %collective-permute-start.38 = (bf16[256,1408]{1,0:T(8,128)(2,1)}, bf16[256,1408]{1,0:T(8,128)(2,1)}, u32[]{:S(2)}, u32[]{:S(2)}) collective-permute-start(bf16[256,1408]{1,0:T(8,128)(2,1)} %collective-permute-done.34.refs_14_), channel_id=1, source_target_pairs={{0,8},{4,0},{8,16},{12,4},{16,24},{20,12},{24,28},{28,20},{1,9},{5... | collective-permute-start | bytes 2162696 | tf_op jit(solution)/shard_map/ppermute | solution.py:211
  262.9 31.6 %collective-permute-start.39 = (bf16[256,1408]{1,0:T(8,128)(2,1)}, bf16[256,1408]{1,0:T(8,128)(2,1)}, u32[]{:S(2)}, u32[]{:S(2)}) collective-permute-start(bf16[256,1408]{1,0:T(8,128)(2,1)} %collective-permute-done.35.refs_8_), channel_id=1, source_target_pairs={{0,4},{4,12},{8,0},{12,20},{16,8},{20,28},{24,16},{28,24},{1,5},{5... | collective-permute-start | bytes 2162696 | tf_op jit(solution)/shard_map/ppermute | solution.py:211
  281.0 28.5 %collective-permute-start.36 = (bf16[256,1408]{1,0:T(8,128)(2,1)}, bf16[256,1408]{1,0:T(8,128)(2,1)}, u32[]{:S(2)}, u32[]{:S(2)}) collective-permute-start(bf16[256,1408]{1,0:T(8,128)(2,1)} %collective-permute-done.32.refs_22_), channel_id=1, source_target_pairs={{0,8},{4,0},{8,16},{12,4},{16,24},{20,12},{24,28},{28,20},{1,9},{5... | collective-permute-start | bytes 2162696 | tf_op jit(solution)/shard_map/ppermute | solution.py:211
  282.5 27.5 %collective-permute-start.41 = (bf16[768,512]{1,0:T(8,128)(2,1)S(1)}, bf16[768,512]{1,0:T(8,128)(2,1)S(1)}, u32[]{:S(2)}, u32[]{:S(2)}) collective-permute-start(bf16[768,512]{1,0:T(8,128)(2,1)S(1)} %add_convert_fusion.1.refs_3_), channel_id=1, source_target_pairs={{0,1},{1,0},{2,3},{3,2},{4,5},{5,4},{6,7},{7,6},{8,9},{9,8},{10,11... | collective-permute-start | bytes 2359304 | tf_op jit(solution)/shard_map/ppermute | solution.py:254
  282.5 27.5 %collective-permute-start.43 = (bf16[768,512]{1,0:T(8,128)(2,1)S(1)}, bf16[768,512]{1,0:T(8,128)(2,1)S(1)}, u32[]{:S(2)}, u32[]{:S(2)}) collective-permute-start(bf16[768,512]{1,0:T(8,128)(2,1)S(1)} %collective-permute-done.42.refs_5_), channel_id=1, source_target_pairs={{0,1},{1,0},{2,3},{3,2},{4,5},{5,4},{6,7},{7,6},{8,9},{9,8},{10,11... | collective-permute-start | bytes 2359304 | tf_op jit(solution)/shard_map/ppermute | solution.py:254
  294.5 30.4 %collective-permute-start.46 = (bf16[256,1408]{1,0:T(8,128)(2,1)}, bf16[256,1408]{1,0:T(8,128)(2,1)}, u32[]{:S(2)}, u32[]{:S(2)}) collective-permute-start(bf16[256,1408]{1,0:T(8,128)(2,1)} %collective-permute-done.38.refs_13_), channel_id=1, source_target_pairs={{0,8},{4,0},{8,16},{12,4},{16,24},{20,12},{24,28},{28,20},{1,9},{5... | collective-permute-start | bytes 2162696 | tf_op jit(solution)/shard_map/ppermute | solution.py:211
  381.1 39.0 %collective-permute-start.60 = (bf16[768,512]{1,0:T(8,128)(2,1)S(1)}, bf16[768,512]{1,0:T(8,128)(2,1)S(1)}, u32[]{:S(2)}, u32[]{:S(2)}) collective-permute-start(bf16[768,512]{1,0:T(8,128)(2,1)S(1)} %add_convert_fusion.refs_3_), channel_id=1, source_target_pairs={{0,1},{1,0},{2,3},{3,2},{4,5},{5,4},{6,7},{7,6},{8,9},{9,8},{10,11... | collective-permute-start | bytes 2359304 | tf_op jit(solution)/shard_map/ppermute | solution.py:254
  397.3 23.3 %collective-permute-start.62 = (bf16[768,512]{1,0:T(8,128)(2,1)S(1)}, bf16[768,512]{1,0:T(8,128)(2,1)S(1)}, u32[]{:S(2)}, u32[]{:S(2)}) collective-permute-start(bf16[768,512]{1,0:T(8,128)(2,1)S(1)} %collective-permute-done.61.refs_5_), channel_id=1, source_target_pairs={{0,1},{1,0},{2,3},{3,2},{4,5},{5,4},{6,7},{7,6},{8,9},{9,8},{10,11... | collective-permute-start | bytes 2359304 | tf_op jit(solution)/shard_map/ppermute | solution.py:254
  410.2 29.0 %collective-permute-start.58 = (bf16[704,256]{1,0:T(8,128)(2,1)}, bf16[704,256]{1,0:T(8,128)(2,1)S(1)}, u32[]{:S(2)}, u32[]{:S(2)}) collective-permute-start(bf16[704,256]{1,0:T(8,128)(2,1)} %collective-permute-done.54.refs_11_), channel_id=1, source_target_pairs={{0,8},{4,0},{8,16},{12,4},{16,24},{20,12},{24,28},{28,20},{1,9},{5... | collective-permute-start | bytes 1081352 | tf_op jit(solution)/shard_map/ppermute | solution.py:211
  416.4 22.8 %collective-permute-start.59 = (bf16[704,256]{1,0:T(8,128)(2,1)}, bf16[704,256]{1,0:T(8,128)(2,1)}, u32[]{:S(2)}, u32[]{:S(2)}) collective-permute-start(bf16[704,256]{1,0:T(8,128)(2,1)} %copy-done.28), channel_id=1, source_target_pairs={{0,4},{4,12},{8,0},{12,20},{16,8},{20,28},{24,16},{28,24},{1,5},{5... | collective-permute-start | bytes 1081352 | tf_op jit(solution)/shard_map/ppermute | solution.py:211
  418.5 22.8 %collective-permute-start.56 = (bf16[704,256]{1,0:T(8,128)(2,1)}, bf16[704,256]{1,0:T(8,128)(2,1)}, u32[]{:S(2)}, u32[]{:S(2)}) collective-permute-start(bf16[704,256]{1,0:T(8,128)(2,1)} %collective-permute-done.52.refs_19_), channel_id=1, source_target_pairs={{0,8},{4,0},{8,16},{12,4},{16,24},{20,12},{24,28},{28,20},{1,9},{5... | collective-permute-start | bytes 1081352 | tf_op jit(solution)/shard_map/ppermute | solution.py:211
  420.1 21.2 %collective-permute-start.57 = (bf16[704,256]{1,0:T(8,128)(2,1)}, bf16[704,256]{1,0:T(8,128)(2,1)}, u32[]{:S(2)}, u32[]{:S(2)}) collective-permute-start(bf16[704,256]{1,0:T(8,128)(2,1)} %collective-permute-done.53.refs_13_), channel_id=1, source_target_pairs={{0,4},{4,12},{8,0},{12,20},{16,8},{20,28},{24,16},{28,24},{1,5},{5... | collective-permute-start | bytes 1081352 | tf_op jit(solution)/shard_map/ppermute | solution.py:211
  (75 other events, 1915.0 us)
where the time goes:
time: 509 us; the launch traced here: 508 us
  waiting for transfers between devices  325 us (64%)
  Pallas kernels  74 us (15%)
  starting transfers between devices  67.8 us (13%)
  other arithmetic  16.5 us (3%)
  local copies, waits for them, and re-layouts  11.6 us (2%)
  matrix products  6.93 us (1%)
  blocking collectives  5.95 us (1%)
    ppermute x56, waiting for transfers between devices, launch(): landed = [lax.ppermute(a, 'fs', way) for a, (_, way) in zip(arrays, sends)]  266 us
    ppermute x56, starting transfers between devices, launch(): landed = [lax.ppermute(a, 'fs', way) for a, (_, way) in zip(arrays, sends)]  57.6 us
    ppermute x6, waiting for transfers between devices, across_chip(): return lax.ppermute(value, 'tp', pairs)  50.9 us
    pallas_call x3, Pallas kernels, hidden_of(): pl.pallas_call(lambda *refs: hidden_kernel(count, ring.count, len(sides),...  42.2 us
    pallas_call x3, Pallas kernels, terms_of(): pl.pallas_call(lambda *refs: terms_kernel(ring.count, len(sides), low, co...  31.7 us
  transfers between devices with their start and end apart: 71, of which 39 were waited for; matrix products, arithmetic and copies ran while one was open for 4% of the time, Pallas kernels for 8%

commit v1 on v0

--- a/solution.py
+++ b/solution.py
@@ -99,35 +99,42 @@
             out[:, here] = act(product(left, here), product(right, here)).astype(out.dtype)
 
 
-def terms_kernel(slots, parts, low, cores, whose, where, inside, hidden, *refs):
+def terms_kernel(slots, parts, low, cores, far, whose, where, inside, hidden, *refs):
     shards = refs[: slots * parts]
     outs = refs[slots * parts : slots * parts + cores]
     columns, sems = refs[slots * parts + cores :]
-    width = columns.shape[2]
-    copies = [
-        pltpu.make_async_copy(
-            shards[part * slots + slot].at[:, pl.ds(low, width)],
-            columns.at[slot, pl.ds(part * shards[0].shape[0], shards[0].shape[0]), :],
-            sems.at[part, slot],
-        )
-        for slot in range(slots)
-        for part in range(parts)
-    ]
-    for copy in copies:
-        copy.start()
-    for copy in copies:
-        copy.wait()
+    depth, width = shards[0].shape[0], columns.shape[2]
+
+    def wanted(slot):
+        return where[slot] > 0 if far else where[slot] == 0
+
+    for slot in range(slots):
+
+        @pl.when(wanted(slot))
+        def _(slot=slot):
+            for part in range(parts):
+                pltpu.make_async_copy(
+                    shards[part * slots + slot].at[:, pl.ds(low, width)],
+                    columns.at[slot, pl.ds(part * depth, depth), :],
+                    sems.at[part, slot],
+                ).start()
 
     @pl.loop(0, slots)
     def _(slot):
-        value = jnp.dot(hidden[...], columns[slot], preferred_element_type=jnp.float32)
-        value = value.astype(jnp.bfloat16)
-        here = pl.ds(pl.multiple_of(inside[slot] * width, width), width)
-        for core in range(cores):
-
-            @pl.when(whose[slot] == core)
-            def _(core=core):
-                outs[core][where[slot], :, here] = value
+        @pl.when(wanted(slot))
+        def _():
+            for part in range(parts):
+                landing = columns.at[slot, pl.ds(part * depth, depth), :]
+                pltpu.make_async_copy(landing, landing, sems.at[part, slot]).wait()
+            value = jnp.dot(hidden[...], columns[slot], preferred_element_type=jnp.float32)
+            value = value.astype(jnp.bfloat16)
+            here = pl.ds(pl.multiple_of(inside[slot] * width, width), width)
+            to = where[slot] - 1 if far else 0
+            for core in range(cores):
+
+                @pl.when(whose[slot] == core)
+                def _(core=core):
+                    outs[core][to, :, here] = value
 
 
 def silu_times(gate, up):
@@ -267,7 +274,7 @@
         return chip * self.cores + core
 
     def gather_far(self, mine):
-        return [mine] + [self.across_chip(mine, shift) for shift in range(1, self.chips)]
+        return [self.across_chip(mine, shift) for shift in range(1, self.chips)]
 
     def gather_near(self, far):
         return [
@@ -298,22 +305,21 @@
         core = (holder % self.cores - self.core + self.cores) % self.cores
         return core, chip, owners % each
 
-    def scatter_near(self, terms):
+    def over_cores(self, terms):
         sent = [self.across_core(part, shift) for shift, part in enumerate(terms[1:], 1)]
         total = terms[0].astype(jnp.float32)
         for part in sent:
             total = total + part.astype(jnp.float32)
-        return [total[0]] + [total[chip].astype(jnp.bfloat16) for chip in range(1, self.chips)]
-
-    def scatter_far(self, sums):
-        return [sums[0]] + [
-            self.across_chip(total, shift) for shift, total in enumerate(sums[1:], 1)
-        ]
-
-
-def add_up(current, landed, factor):
-    total = landed[0]
-    for part in landed[1:]:
+        return total
+
+    def over_chips(self, sums):
+        sums = sums.astype(jnp.bfloat16)
+        return [self.across_chip(sums[shift - 1], shift) for shift in range(1, self.chips)]
+
+
+def add_up(current, own, landed, factor):
+    total = own[0]
+    for part in landed:
         total = total + part.astype(jnp.float32)
     return (current.astype(jnp.float32) + factor * total).astype(jnp.bfloat16)
 
@@ -400,12 +406,13 @@
                 name="hidden",
             )(spots, blocks, gain_vec.reshape(count, 1, size), *parts, *arrays)
 
-        def terms_of(hidden, sides, low, width):
+        def terms_of(hidden, sides, low, width, far):
             length, depth_all = hidden.shape
             arrays = [shard for side in sides for shard in side.listed()]
-            out = jax.ShapeDtypeStruct((features.chips, length, each * width), jnp.bfloat16)
+            chips = features.chips - 1 if far else 1
+            out = jax.ShapeDtypeStruct((chips, length, each * width), jnp.bfloat16)
             return pl.pallas_call(
-                lambda *refs: terms_kernel(ring.count, len(sides), low, cores, *refs),
+                lambda *refs: terms_kernel(ring.count, len(sides), low, cores, far, *refs),
                 out_shape=[out] * cores,
                 in_specs=[spec(smem)] * 3 + [spec(vmem)] + [spec(hbm)] * len(arrays),
                 out_specs=[spec(vmem)] * cores,
@@ -414,33 +421,39 @@
                     pltpu.SemaphoreType.DMA((len(sides), ring.count)),
                 ],
                 cost_estimate=pl.CostEstimate(
-                    flops=2 * length * depth_all * ring.count * width,
-                    bytes_accessed=2 * depth_all * ring.count * width,
+                    flops=2 * length * depth_all * chips * cores * each * width,
+                    bytes_accessed=2 * depth_all * chips * cores * each * width,
                     transcendentals=0,
                 ),
-                name="terms",
+                name="far_terms" if far else "near_terms",
             )(*targets, hidden, *arrays)
+
+        def scatter(hidden, sides, low, width, turns):
+            landed = []
+            if features.chips > 1:
+                sums = features.over_cores(terms_of(hidden, sides, low, width, True))
+                hidden, sums = tie(hidden, sums)
+                landed = features.over_chips(sums)
+            terms = terms_of(hidden, sides, low, width, False)
+            own = features.over_cores(terms)
+            return pump.turn(own, turns), landed
 
         tokens = pump.fill(tokens)
         far = features.gather_far(tokens)
         far = pump.turn(far)
-        parts = features.gather_near(far)
+        parts = features.gather_near([tokens] + far)
         parts = pump.until([one_gate, one_up], parts)
         hidden = hidden_of(
             parts, ffn_one_gain, [one_gate, one_up], (0, 0), ffn_one_up.shape[1], silu_times,
             jnp.bfloat16,
         )
-        hidden = pump.until([one_down], hidden)
-        terms = terms_of(hidden, [one_down], 0, ffn_one_down.shape[1])
-        sums = pump.turn(features.scatter_near(terms))
-        landed = features.scatter_far(sums)
-        pump.turn(())
-        stream_one = add_up(tokens, landed, 0.5)
-
-        stream_one = pump.until(mixes, stream_one)
+        hidden = pump.until([one_down] + mixes, hidden)
+        own, landed = scatter(hidden, [one_down], 0, ffn_one_down.shape[1], 1)
+        stream_one = add_up(tokens, own, landed, 0.5)
+
         far = features.gather_far(stream_one)
-        pump.turn((), 2)
-        parts = pump.turn(features.gather_near(far))
+        stream_one = pump.turn(stream_one, 2)
+        parts = features.gather_near([stream_one] + far)
         gated_lin = hidden_of(
             parts, mix_gain, [mix_in], (wide, 0), wide, gate_times, jnp.float32
         )
@@ -463,24 +476,21 @@
         active = jax.nn.silu(
             (convolved - mean_val) * lax.rsqrt(varied + 1e-05) * conv_ln_gain
         ).astype(jnp.bfloat16)
-        terms = terms_of(active, [mix_out], out_from, conv_out.shape[1])
-        sums = pump.turn(features.scatter_near(terms))
-        landed = features.scatter_far(sums)
-        pump.turn(())
-        stream_two = pump.turn(add_up(stream_one, landed, 1.0))
+        active = pump.turn(active)
+        own, landed = scatter(active, [mix_out], out_from, conv_out.shape[1], 1)
+        stream_two = add_up(stream_one, own, landed, 1.0)
 
         far = features.gather_far(stream_two)
-        pump.turn((), 2)
-        parts = features.gather_near(far)
-        parts = pump.until([two_gate, two_up], parts)
+        stream_two = pump.turn(stream_two, 3)
+        parts = features.gather_near([stream_two] + far)
+        parts = pump.until([two_gate, two_up], pump.turn(parts))
         hidden = hidden_of(
             parts, ffn_two_gain, [two_gate, two_up], (0, 0), ffn_two_up.shape[1], silu_times,
             jnp.bfloat16,
         )
         hidden = pump.until(two_down, hidden)
-        terms = terms_of(hidden, two_down, 0, ffn_two_down.shape[1])
-        landed = features.scatter_far(features.scatter_near(terms))
-        return jnp.where(pump.mark < 0, stream_two, add_up(stream_two, landed, 0.5))
+        own, landed = scatter(hidden, two_down, 0, ffn_two_down.shape[1], 0)
+        return jnp.where(pump.mark < 0, stream_two, add_up(stream_two, own, landed, 0.5))
 
     in_specs = (
         P("fs", "tp"),

time: 509 us -> 490 us (0.963)
  waiting for transfers between devices: 325 us -> 304 us
  Pallas kernels: 74 us -> 80.5 us
  local copies, waits for them, and re-layouts: 11.6 us -> 6.22 us
    ppermute x6, waiting for transfers between devices: 50.9 us -> 17.5 us  [across_chip(): return lax.ppermute(value, 'tp', pairs)]
    ppermute x56, waiting for transfers between devices: 266 us -> 278 us  [launch(): landed = [lax.ppermute(a, 'fs', way) for a, (_, way) in zip(arrays, sends)]]
    pallas_call x3 -> x6, Pallas kernels: 31.7 us -> 38.3 us  [terms_of(): pl.pallas_call(lambda *refs: terms_kernel(ring.count, len(sides), low, co...]
  transfers between devices with their start and end apart: 71 -> 74, of which waited for: 39 -> 43; matrix products, arithmetic and copies ran while one was open for 4% -> 4% of each run, Pallas kernels for 8% -> 9%
where the time goes in v1:
time: 490 us; the launch traced here: 489 us
  waiting for transfers between devices  304 us (62%)
  Pallas kernels  80.5 us (16%)
  starting transfers between devices  66.2 us (14%)
  other arithmetic  17.7 us (4%)
  matrix products  6.93 us (1%)
  blocking collectives  6.35 us (1%)
  local copies, waits for them, and re-layouts  6.22 us (1%)
    ppermute x56, waiting for transfers between devices, launch(): landed = [lax.ppermute(a, 'fs', way) for a, (_, way) in zip(arrays, sends)]  278 us
    ppermute x56, starting transfers between devices, launch(): landed = [lax.ppermute(a, 'fs', way) for a, (_, way) in zip(arrays, sends)]  55.8 us
    pallas_call x3, Pallas kernels, hidden_of(): pl.pallas_call(lambda *refs: hidden_kernel(count, ring.count, len(sides),...  42.2 us
    pallas_call x6, Pallas kernels, terms_of(): pl.pallas_call(lambda *refs: terms_kernel(ring.count, len(sides), low, co...  38.3 us
    ppermute x6, waiting for transfers between devices, across_chip(): return lax.ppermute(value, 'tp', pairs)  17.5 us
  transfers between devices with their start and end apart: 74, of which 43 were waited for; matrix products, arithmetic and copies ran while one was open for 4% of the time, Pallas kernels for 9%

profile of v1, /device:TPU:0, one launch (start us, length us, event | category | flops | bytes accessed | tf_op | source)
XLA Modules:
  0.0 488.7 jit_solution(5518942484620384074)
XLA Ops:
  5.0 15.8 %collective-permute-done.2.refs_14_ = bf16[256,1408]{1,0:T(8,128)(2,1)S(1)} collective-permute-done((bf16[256,1408]{1,0:T(8,128)(2,1)}, bf16[256,1408]{1,0:T(8,128)(2,1)S(1)}, u32[]{:S(2)}, u32[]{:S(2)}) %collective-permute-start.2) | collective-permute-done | bytes 720928 | tf_op jit(solution)/shard_map/ppermute | solution.py:218
  25.4 16.4 %collective-permute-done.refs_22_ = bf16[256,1408]{1,0:T(8,128)(2,1)} collective-permute-done((bf16[256,1408]{1,0:T(8,128)(2,1)}, bf16[256,1408]{1,0:T(8,128)(2,1)}, u32[]{:S(2)}, u32[]{:S(2)}) %collective-permute-start) | collective-permute-done | bytes 720928 | tf_op jit(solution)/shard_map/ppermute | solution.py:218
  46.0 13.3 %collective-permute-done.10.refs_9_ = bf16[256,1408]{1,0:T(8,128)(2,1)} collective-permute-done((bf16[256,1408]{1,0:T(8,128)(2,1)}, bf16[256,1408]{1,0:T(8,128)(2,1)}, u32[]{:S(2)}, u32[]{:S(2)}) %collective-permute-start.10) | collective-permute-done | bytes 720928 | tf_op jit(solution)/shard_map/ppermute | solution.py:218
  63.0 13.4 %collective-permute-done.7.refs_21_ = bf16[256,1408]{1,0:T(8,128)(2,1)} collective-permute-done((bf16[256,1408]{1,0:T(8,128)(2,1)}, bf16[256,1408]{1,0:T(8,128)(2,1)}, u32[]{:S(2)}, u32[]{:S(2)}) %collective-permute-start.7) | collective-permute-done | bytes 720928 | tf_op jit(solution)/shard_map/ppermute | solution.py:218
  80.6 11.2 %collective-permute-done.13.refs_12_ = bf16[256,1408]{1,0:T(8,128)(2,1)} collective-permute-done((bf16[256,1408]{1,0:T(8,128)(2,1)}, bf16[256,1408]{1,0:T(8,128)(2,1)}, u32[]{:S(2)}, u32[]{:S(2)}) %collective-permute-start.13) | collective-permute-done | bytes 720928 | tf_op jit(solution)/shard_map/ppermute | solution.py:218
  93.4 13.9 %collective-permute-done.11.refs_20_ = bf16[256,1408]{1,0:T(8,128)(2,1)} collective-permute-done((bf16[256,1408]{1,0:T(8,128)(2,1)}, bf16[256,1408]{1,0:T(8,128)(2,1)}, u32[]{:S(2)}, u32[]{:S(2)}) %collective-permute-start.11) | collective-permute-done | bytes 720928 | tf_op jit(solution)/shard_map/ppermute | solution.py:218
  112.1 9.3 %collective-permute-done.16.refs_11_ = bf16[256,1408]{1,0:T(8,128)(2,1)} collective-permute-done((bf16[256,1408]{1,0:T(8,128)(2,1)}, bf16[256,1408]{1,0:T(8,128)(2,1)}, u32[]{:S(2)}, u32[]{:S(2)}) %collective-permute-start.16) | collective-permute-done | bytes 720928 | tf_op jit(solution)/shard_map/ppermute | solution.py:218
  123.5 17.7 %hidden.3.refs_3_ = bf16[768,1408]{1,0:T(8,128)(2,1)} custom-call(s32[8]{0:T(128)} %get-tuple-element.707.refs_0_, s32[4]{0:T(128)} %pad_add_fusion.refs_1_, f32[4,1,512]{2,1,0:T(1,128)} %bitcast.66, bf16[768,512]{1,0:T(8,128)(2,1)} %refs_3_, bf16[768,512]{1,0:T(8,128)(2,1)} %copy-done.23, bf16[768,512]{1,0:T(8,128)(2,1)} %copy-done.22, ...), custom_call_target="tpu_custom_call" | custom-call | flops 8858370048 | bytes 14680064 | tf_op jit(solution)/shard_map/hidden/pallas_call | solution.py:388
  145.3 20.9 %collective-permute-done.17.refs_14_.refs_11_ = bf16[256,768]{1,0:T(8,128)(2,1)S(1)} collective-permute-done((bf16[256,768]{1,0:T(8,128)(2,1)S(1)}, bf16[256,768]{1,0:T(8,128)(2,1)S(1)}, u32[]{:S(2)}, u32[]{:S(2)}) %collective-permute-start.17) | collective-permute-done | bytes 393248 | tf_op jit(solution)/shard_map/ppermute | solution.py:218
  171.6 19.5 %collective-permute-done.21.refs_13_.refs_10_ = bf16[256,768]{1,0:T(8,128)(2,1)S(1)} collective-permute-done((bf16[256,768]{1,0:T(8,128)(2,1)S(1)}, bf16[256,768]{1,0:T(8,128)(2,1)S(1)}, u32[]{:S(2)}, u32[]{:S(2)}) %collective-permute-start.21) | collective-permute-done | bytes 393248 | tf_op jit(solution)/shard_map/ppermute | solution.py:218
  197.2 7.6 %collective-permute-done.25.refs_12_.refs_9_ = bf16[256,768]{1,0:T(8,128)(2,1)S(1)} collective-permute-done((bf16[256,768]{1,0:T(8,128)(2,1)S(1)}, bf16[256,768]{1,0:T(8,128)(2,1)S(1)}, u32[]{:S(2)}, u32[]{:S(2)}) %collective-permute-start.25) | collective-permute-done | bytes 393248 | tf_op jit(solution)/shard_map/ppermute | solution.py:218
  206.4 8.7 %collective-permute-done.30.refs_8_ = bf16[1408,256]{1,0:T(8,128)(2,1)} collective-permute-done((bf16[1408,256]{1,0:T(8,128)(2,1)}, bf16[1408,256]{1,0:T(8,128)(2,1)}, u32[]{:S(2)}, u32[]{:S(2)}) %collective-permute-start.30) | collective-permute-done | bytes 720928 | tf_op jit(solution)/shard_map/ppermute | solution.py:218
  215.2 7.4 %far_terms.3 = (bf16[1,768,512]{2,1,0:T(8,128)(2,1)}, bf16[1,768,512]{2,1,0:T(8,128)(2,1)}) custom-call(s32[8]{0:T(128)} %get-tuple-element.706.refs_0_, s32[8]{0:T(128)} %get-tuple-element.699.refs_1_, s32[8]{0:T(128)} %get-tuple-element.697.refs_2_, bf16[768,1408]{1,0:T(8,128)(2,1)} %hidden.3.refs_3_, bf16[1408,256]{1,0:T(8,128)(2,1)} %refs_4_.3, ...), custom_call_target="tpu_custom_call" | custom-call | flops 2214592512 | bytes 2883584 | tf_op jit(solution)/shard_map/far_terms/pallas_call | solution.py:414
  226.6 7.3 %near_terms.3 = (bf16[1,768,512]{2,1,0:T(8,128)(2,1)}, bf16[1,768,512]{2,1,0:T(8,128)(2,1)}) custom-call(s32[8]{0:T(128)} %get-tuple-element.706.refs_0_, s32[8]{0:T(128)} %get-tuple-element.699.refs_1_, s32[8]{0:T(128)} %get-tuple-element.697.refs_2_, bf16[768,1408]{1,0:T(8,128)(2,1)} %hidden.3.refs_3_, bf16[1408,256]{1,0:T(8,128)(2,1)} %refs_4_.3, ...), custom_call_target="tpu_custom_call" | custom-call | flops 2214592512 | bytes 2883584 | tf_op jit(solution)/shard_map/near_terms/pallas_call | solution.py:414
  238.0 15.0 %collective-permute-done.33.refs_14_ = bf16[256,1408]{1,0:T(8,128)(2,1)} collective-permute-done((bf16[256,1408]{1,0:T(8,128)(2,1)}, bf16[256,1408]{1,0:T(8,128)(2,1)}, u32[]{:S(2)}, u32[]{:S(2)}) %collective-permute-start.33) | collective-permute-done | bytes 720928 | tf_op jit(solution)/shard_map/ppermute | solution.py:218
  261.5 15.0 %collective-permute-done.31.refs_22_ = bf16[256,1408]{1,0:T(8,128)(2,1)S(1)} collective-permute-done((bf16[256,1408]{1,0:T(8,128)(2,1)S(1)}, bf16[256,1408]{1,0:T(8,128)(2,1)S(1)}, u32[]{:S(2)}, u32[]{:S(2)}) %collective-permute-start.31) | collective-permute-done | bytes 720928 | tf_op jit(solution)/shard_map/ppermute | solution.py:218
  277.9 11.8 %collective-permute-done.40.refs_13_ = bf16[256,1408]{1,0:T(8,128)(2,1)} collective-permute-done((bf16[256,1408]{1,0:T(8,128)(2,1)}, bf16[256,1408]{1,0:T(8,128)(2,1)}, u32[]{:S(2)}, u32[]{:S(2)}) %collective-permute-start.40) | collective-permute-done | bytes 720928 | tf_op jit(solution)/shard_map/ppermute | solution.py:218
  296.4 6.8 %hidden.4 = f32[768,256]{1,0:T(8,128)} custom-call(s32[8]{0:T(128)} %get-tuple-element.707.refs_0_, s32[4]{0:T(128)} %pad_add_fusion.refs_1_, f32[4,1,512]{2,1,0:T(1,128)} %bitcast.65, bf16[768,512]{1,0:T(8,128)(2,1)} %copy-done.2, bf16[768,512]{1,0:T(8,128)(2,1)} %copy-done.15, bf16[768,512]{1,0:T(8,128)(2,1)} %copy-done.14, bf16[768,512]{1,0:T(8,128)(2,1)} %copy-done.16, ...), custom_call_target="tpu_custom_call" | custom-call | flops 1610612736 | bytes 5242880 | tf_op jit(solution)/shard_map/hidden/pallas_call | solution.py:388
  303.2 6.9 %fusion.9 = f32[1,768,256]{2,0,1:T(1,128)S(1)} fusion(f32[1,768,256]{2,1,0:T(8,128)} %bitcast.61, f32[31,1,256]{2,0,1:T(8,128)S(1)} %bitcast.58), kind=kOutput, calls=%fused_computation.18 | convolution fusion | flops 72400896 | bytes 1604608 | tf_op jit(solution)/shard_map/conv_general_dilated | solution.py:461
  311.7 6.4 %all-reduce = (f32[768]{0:T(1024)S(1)}, f32[768]{0:T(1024)S(1)}) all-reduce(f32[768]{0:T(1024)S(1)} %get-tuple-element.694, f32[768]{0:T(1024)S(1)} %get-tuple-element.693), channel_id=1, replica_groups=mesh['fs'=8,'tp'=4] {'tp'}, use_global_device_ids=true, to_apply=%region_3.4 | all-reduce | flops 1536 | bytes 12288 | tf_op jit(solution)/shard_map/psum | solution.py:471
  319.2 5.9 %collective-permute-done.47.refs_12_ = bf16[256,1408]{1,0:T(8,128)(2,1)} collective-permute-done((bf16[256,1408]{1,0:T(8,128)(2,1)}, bf16[256,1408]{1,0:T(8,128)(2,1)}, u32[]{:S(2)}, u32[]{:S(2)}) %collective-permute-start.47) | collective-permute-done | bytes 720928 | tf_op jit(solution)/shard_map/ppermute | solution.py:218
  334.0 4.4 near_terms.4
  344.2 15.3 %collective-permute-done.45.refs_20_ = bf16[256,1408]{1,0:T(8,128)(2,1)} collective-permute-done((bf16[256,1408]{1,0:T(8,128)(2,1)}, bf16[256,1408]{1,0:T(8,128)(2,1)}, u32[]{:S(2)}, u32[]{:S(2)}) %collective-permute-start.45) | collective-permute-done | bytes 720928 | tf_op jit(solution)/shard_map/ppermute | solution.py:218
  363.0 11.1 %collective-permute-done.52.refs_11_ = bf16[256,1408]{1,0:T(8,128)(2,1)} collective-permute-done((bf16[256,1408]{1,0:T(8,128)(2,1)}, bf16[256,1408]{1,0:T(8,128)(2,1)}, u32[]{:S(2)}, u32[]{:S(2)}) %collective-permute-start.52) | collective-permute-done | bytes 720928 | tf_op jit(solution)/shard_map/ppermute | solution.py:218
  376.1 4.8 collective-permute-done.51.refs_19_
  390.1 8.7 %collective-permute-done.54.refs_19_ = bf16[704,256]{1,0:T(8,128)(2,1)S(1)} collective-permute-done((bf16[704,256]{1,0:T(8,128)(2,1)S(1)}, bf16[704,256]{1,0:T(8,128)(2,1)S(1)}, u32[]{:S(2)}, u32[]{:S(2)}) %collective-permute-start.54) | collective-permute-done | bytes 360480 | tf_op jit(solution)/shard_map/ppermute | solution.py:218
  402.1 17.7 %hidden.5.refs_3_ = bf16[768,1408]{1,0:T(8,128)(2,1)} custom-call(s32[8]{0:T(128)} %get-tuple-element.707.refs_0_, s32[4]{0:T(128)} %pad_add_fusion.refs_1_, f32[4,1,512]{2,1,0:T(1,128)} %bitcast.67, bf16[768,512]{1,0:T(8,128)(2,1)} %copy-done.12, bf16[768,512]{1,0:T(8,128)(2,1)} %copy-done.26, bf16[768,512]{1,0:T(8,128)(2,1)} %copy-done.25, ...), custom_call_target="tpu_custom_call" | custom-call | flops 8858370048 | bytes 14680064 | tf_op jit(solution)/shard_map/hidden/pallas_call | solution.py:388
  424.0 7.4 %collective-permute-done.67.refs_9_ = bf16[704,256]{1,0:T(8,128)(2,1)S(1)} collective-permute-done((bf16[704,256]{1,0:T(8,128)(2,1)}, bf16[704,256]{1,0:T(8,128)(2,1)S(1)}, u32[]{:S(2)}, u32[]{:S(2)}) %collective-permute-start.67) | collective-permute-done | bytes 360480 | tf_op jit(solution)/shard_map/ppermute | solution.py:218
  433.5 5.7 %collective-permute-done.65.refs_17_ = bf16[704,256]{1,0:T(8,128)(2,1)S(1)} collective-permute-done((bf16[704,256]{1,0:T(8,128)(2,1)}, bf16[704,256]{1,0:T(8,128)(2,1)S(1)}, u32[]{:S(2)}, u32[]{:S(2)}) %collective-permute-start.65) | collective-permute-done | bytes 360480 | tf_op jit(solution)/shard_map/ppermute | solution.py:218
  447.4 7.4 %far_terms.5 = (bf16[1,768,512]{2,1,0:T(8,128)(2,1)}, bf16[1,768,512]{2,1,0:T(8,128)(2,1)}) custom-call(s32[8]{0:T(128)} %get-tuple-element.706.refs_0_, s32[8]{0:T(128)} %get-tuple-element.699.refs_1_, s32[8]{0:T(128)} %get-tuple-element.697.refs_2_, bf16[768,1408]{1,0:T(8,128)(2,1)} %hidden.5.refs_3_, bf16[704,256]{1,0:T(8,128)(2,1)} %copy-done.20, ...), custom_call_target="tpu_custom_call" | custom-call | flops 2214592512 | bytes 2883584 | tf_op jit(solution)/shard_map/far_terms/pallas_call | solution.py:414
  458.7 7.5 %near_terms.5 = (bf16[1,768,512]{2,1,0:T(8,128)(2,1)}, bf16[1,768,512]{2,1,0:T(8,128)(2,1)}) custom-call(s32[8]{0:T(128)} %get-tuple-element.706.refs_0_, s32[8]{0:T(128)} %get-tuple-element.699.refs_1_, s32[8]{0:T(128)} %get-tuple-element.697.refs_2_, bf16[768,1408]{1,0:T(8,128)(2,1)} %hidden.5.refs_3_, bf16[704,256]{1,0:T(8,128)(2,1)} %copy-done.20, ...), custom_call_target="tpu_custom_call" | custom-call | flops 2214592512 | bytes 2883584 | tf_op jit(solution)/shard_map/near_terms/pallas_call | solution.py:414
  468.7 17.5 %collective-permute-done.73 = bf16[768,512]{1,0:T(8,128)(2,1)S(1)} collective-permute-done((bf16[768,512]{1,0:T(8,128)(2,1)S(1)}, bf16[768,512]{1,0:T(8,128)(2,1)S(1)}, u32[]{:S(2)}, u32[]{:S(2)}) %collective-permute-start.73) | collective-permute-done | bytes 786464 | tf_op jit(solution)/shard_map/ppermute | solution.py:269
  (233 shorter events, 130.7 us)
Async XLA Ops:
  0.0 22.1 %collective-permute-start.4 = (bf16[768,512]{1,0:T(8,128)(2,1)}, bf16[768,512]{1,0:T(8,128)(2,1)S(1)}, u32[]{:S(2)}, u32[]{:S(2)}) collective-permute-start(bf16[768,512]{1,0:T(8,128)(2,1)} %refs_3_), channel_id=1, source_target_pairs={{0,2},{1,3},{2,0},{3,1},{4,6},{5,7},{6,4},{7,5},{8,10},{9,11},{10,... | collective-permute-start | bytes 2359304 | tf_op jit(solution)/shard_map/ppermute | solution.py:269
  5.0 38.8 %collective-permute-start.5 = (bf16[768,512]{1,0:T(8,128)(2,1)}, bf16[768,512]{1,0:T(8,128)(2,1)S(1)}, u32[]{:S(2)}, u32[]{:S(2)}) collective-permute-start(bf16[768,512]{1,0:T(8,128)(2,1)} %refs_3_), channel_id=1, source_target_pairs={{0,1},{1,0},{2,3},{3,2},{4,5},{5,4},{6,7},{7,6},{8,9},{9,8},{10,11... | collective-permute-start | bytes 2359304 | tf_op jit(solution)/shard_map/ppermute | solution.py:261
  23.0 20.9 %collective-permute-start.6 = (bf16[768,512]{1,0:T(8,128)(2,1)S(1)}, bf16[768,512]{1,0:T(8,128)(2,1)S(1)}, u32[]{:S(2)}, u32[]{:S(2)}) collective-permute-start(bf16[768,512]{1,0:T(8,128)(2,1)S(1)} %collective-permute-done.4.refs_5_), channel_id=1, source_target_pairs={{0,1},{1,0},{2,3},{3,2},{4,5},{5,4},{6,7},{7,6},{8,9},{9,8},{10,11... | collective-permute-start | bytes 2359304 | tf_op jit(solution)/shard_map/ppermute | solution.py:261
  25.0 34.3 %collective-permute-start.10 = (bf16[256,1408]{1,0:T(8,128)(2,1)}, bf16[256,1408]{1,0:T(8,128)(2,1)}, u32[]{:S(2)}, u32[]{:S(2)}) collective-permute-start(bf16[256,1408]{1,0:T(8,128)(2,1)} %copy-done.29), channel_id=1, source_target_pairs={{0,4},{4,12},{8,0},{12,20},{16,8},{20,28},{24,16},{28,24},{1,5},{5... | collective-permute-start | bytes 2162696 | tf_op jit(solution)/shard_map/ppermute | solution.py:218
  43.9 32.5 %collective-permute-start.7 = (bf16[256,1408]{1,0:T(8,128)(2,1)}, bf16[256,1408]{1,0:T(8,128)(2,1)}, u32[]{:S(2)}, u32[]{:S(2)}) collective-permute-start(bf16[256,1408]{1,0:T(8,128)(2,1)} %collective-permute-done.refs_22_), channel_id=1, source_target_pairs={{0,8},{4,0},{8,16},{12,4},{16,24},{20,12},{24,28},{28,20},{1,9},{5... | collective-permute-start | bytes 2162696 | tf_op jit(solution)/shard_map/ppermute | solution.py:218
  45.5 30.9 %collective-permute-start.8 = (bf16[256,1408]{1,0:T(8,128)(2,1)}, bf16[256,1408]{1,0:T(8,128)(2,1)}, u32[]{:S(2)}, u32[]{:S(2)}) collective-permute-start(bf16[256,1408]{1,0:T(8,128)(2,1)} %collective-permute-done.1.refs_16_), channel_id=1, source_target_pairs={{0,4},{4,12},{8,0},{12,20},{16,8},{20,28},{24,16},{28,24},{1,5},{5... | collective-permute-start | bytes 2162696 | tf_op jit(solution)/shard_map/ppermute | solution.py:218
  60.9 30.9 %collective-permute-start.13 = (bf16[256,1408]{1,0:T(8,128)(2,1)}, bf16[256,1408]{1,0:T(8,128)(2,1)}, u32[]{:S(2)}, u32[]{:S(2)}) collective-permute-start(bf16[256,1408]{1,0:T(8,128)(2,1)} %collective-permute-done.9.refs_13_), channel_id=1, source_target_pairs={{0,8},{4,0},{8,16},{12,4},{16,24},{20,12},{24,28},{28,20},{1,9},{5... | collective-permute-start | bytes 2162696 | tf_op jit(solution)/shard_map/ppermute | solution.py:218
  62.5 29.3 %collective-permute-start.14 = (bf16[256,1408]{1,0:T(8,128)(2,1)}, bf16[256,1408]{1,0:T(8,128)(2,1)}, u32[]{:S(2)}, u32[]{:S(2)}) collective-permute-start(bf16[256,1408]{1,0:T(8,128)(2,1)} %collective-permute-done.10.refs_9_), channel_id=1, source_target_pairs={{0,4},{4,12},{8,0},{12,20},{16,8},{20,28},{24,16},{28,24},{1,5},{5... | collective-permute-start | bytes 2162696 | tf_op jit(solution)/shard_map/ppermute | solution.py:218
  76.4 30.9 %collective-permute-start.11 = (bf16[256,1408]{1,0:T(8,128)(2,1)}, bf16[256,1408]{1,0:T(8,128)(2,1)}, u32[]{:S(2)}, u32[]{:S(2)}) collective-permute-start(bf16[256,1408]{1,0:T(8,128)(2,1)} %collective-permute-done.7.refs_21_), channel_id=1, source_target_pairs={{0,8},{4,0},{8,16},{12,4},{16,24},{20,12},{24,28},{28,20},{1,9},{5... | collective-permute-start | bytes 2162696 | tf_op jit(solution)/shard_map/ppermute | solution.py:218
  78.0 29.3 %collective-permute-start.12 = (bf16[256,1408]{1,0:T(8,128)(2,1)}, bf16[256,1408]{1,0:T(8,128)(2,1)}, u32[]{:S(2)}, u32[]{:S(2)}) collective-permute-start(bf16[256,1408]{1,0:T(8,128)(2,1)} %collective-permute-done.8.refs_17_), channel_id=1, source_target_pairs={{0,4},{4,12},{8,0},{12,20},{16,8},{20,28},{24,16},{28,24},{1,5},{5... | collective-permute-start | bytes 2162696 | tf_op jit(solution)/shard_map/ppermute | solution.py:218
  91.8 29.6 %collective-permute-start.16 = (bf16[256,1408]{1,0:T(8,128)(2,1)}, bf16[256,1408]{1,0:T(8,128)(2,1)}, u32[]{:S(2)}, u32[]{:S(2)}) collective-permute-start(bf16[256,1408]{1,0:T(8,128)(2,1)} %collective-permute-done.13.refs_12_), channel_id=1, source_target_pairs={{0,8},{4,0},{8,16},{12,4},{16,24},{20,12},{24,28},{28,20},{1,9},{5... | collective-permute-start | bytes 2162696 | tf_op jit(solution)/shard_map/ppermute | solution.py:218
  141.2 26.3 %collective-permute-start.23 = (bf16[1408,256]{1,0:T(8,128)(2,1)}, bf16[1408,256]{1,0:T(8,128)(2,1)S(1)}, u32[]{:S(2)}, u32[]{:S(2)}) collective-permute-start(bf16[1408,256]{1,0:T(8,128)(2,1)} %collective-permute-done.19.refs_11_), channel_id=1, source_target_pairs={{0,8},{4,0},{8,16},{12,4},{16,24},{20,12},{24,28},{28,20},{1,9},{5... | collective-permute-start | bytes 2162696 | tf_op jit(solution)/shard_map/ppermute | solution.py:218
  142.9 24.6 %collective-permute-start.24 = (bf16[1408,256]{1,0:T(8,128)(2,1)}, bf16[1408,256]{1,0:T(8,128)(2,1)}, u32[]{:S(2)}, u32[]{:S(2)}) collective-permute-start(bf16[1408,256]{1,0:T(8,128)(2,1)} %collective-permute-done.20.refs_5_), channel_id=1, source_target_pairs={{0,4},{4,12},{8,0},{12,20},{16,8},{20,28},{24,16},{28,24},{1,5},{5... | collective-permute-start | bytes 2162696 | tf_op jit(solution)/shard_map/ppermute | solution.py:218
  143.3 22.9 %collective-permute-start.17 = (bf16[256,768]{1,0:T(8,128)(2,1)S(1)}, bf16[256,768]{1,0:T(8,128)(2,1)S(1)}, u32[]{:S(2)}, u32[]{:S(2)}) collective-permute-start(bf16[256,768]{1,0:T(8,128)(2,1)S(1)} %constant_dynamic-update-slice_fusion.refs_7_.refs_4_), channel_id=1, source_target_pairs={{0,8},{4,0},{8,16},{12,4},{16,24},{20,12},{24,28},{28,20},{1,9},{5... | collective-permute-start | bytes 1179656 | tf_op jit(solution)/shard_map/ppermute | solution.py:218
  144.9 22.6 %collective-permute-start.18 = (bf16[256,768]{1,0:T(8,128)(2,1)S(1)}, bf16[256,768]{1,0:T(8,128)(2,1)S(1)}, u32[]{:S(2)}, u32[]{:S(2)}) collective-permute-start(bf16[256,768]{1,0:T(8,128)(2,1)S(1)} %constant_dynamic-update-slice_fusion.refs_7_.refs_4_), channel_id=1, source_target_pairs={{0,4},{4,12},{8,0},{12,20},{16,8},{20,28},{24,16},{28,24},{1,5},{5... | collective-permute-start | bytes 1179656 | tf_op jit(solution)/shard_map/ppermute | solution.py:218
  167.5 27.7 %collective-permute-start.27 = (bf16[1408,256]{1,0:T(8,128)(2,1)S(1)}, bf16[1408,256]{1,0:T(8,128)(2,1)}, u32[]{:S(2)}, u32[]{:S(2)}) collective-permute-start(bf16[1408,256]{1,0:T(8,128)(2,1)S(1)} %collective-permute-done.23.refs_10_), channel_id=1, source_target_pairs={{0,8},{4,0},{8,16},{12,4},{16,24},{20,12},{24,28},{28,20},{1,9},{5... | collective-permute-start | bytes 2162696 | tf_op jit(solution)/shard_map/ppermute | solution.py:218
  169.1 26.1 %collective-permute-start.28 = (bf16[1408,256]{1,0:T(8,128)(2,1)}, bf16[1408,256]{1,0:T(8,128)(2,1)}, u32[]{:S(2)}, u32[]{:S(2)}) collective-permute-start(bf16[1408,256]{1,0:T(8,128)(2,1)} %collective-permute-done.24.refs_6_), channel_id=1, source_target_pairs={{0,4},{4,12},{8,0},{12,20},{16,8},{20,28},{24,16},{28,24},{1,5},{5... | collective-permute-start | bytes 2162696 | tf_op jit(solution)/shard_map/ppermute | solution.py:218
  169.6 21.5 %collective-permute-start.21 = (bf16[256,768]{1,0:T(8,128)(2,1)S(1)}, bf16[256,768]{1,0:T(8,128)(2,1)S(1)}, u32[]{:S(2)}, u32[]{:S(2)}) collective-permute-start(bf16[256,768]{1,0:T(8,128)(2,1)S(1)} %collective-permute-done.17.refs_14_.refs_11_), channel_id=1, source_target_pairs={{0,8},{4,0},{8,16},{12,4},{16,24},{20,12},{24,28},{28,20},{1,9},{5... | collective-permute-start | bytes 1179656 | tf_op jit(solution)/shard_map/ppermute | solution.py:218
  171.2 21.7 %collective-permute-start.22 = (bf16[256,768]{1,0:T(8,128)(2,1)S(1)}, bf16[256,768]{1,0:T(8,128)(2,1)S(1)}, u32[]{:S(2)}, u32[]{:S(2)}) collective-permute-start(bf16[256,768]{1,0:T(8,128)(2,1)S(1)} %collective-permute-done.18.refs_8_.refs_5_), channel_id=1, source_target_pairs={{0,4},{4,12},{8,0},{12,20},{16,8},{20,28},{24,16},{28,24},{1,5},{5... | collective-permute-start | bytes 1179656 | tf_op jit(solution)/shard_map/ppermute | solution.py:218
  234.0 20.2 %collective-permute-start.37 = (bf16[768,512]{1,0:T(8,128)(2,1)S(1)}, bf16[768,512]{1,0:T(8,128)(2,1)}, u32[]{:S(2)}, u32[]{:S(2)}) collective-permute-start(bf16[768,512]{1,0:T(8,128)(2,1)S(1)} %bitcast.63), channel_id=1, source_target_pairs={{0,2},{1,3},{2,0},{3,1},{4,6},{5,7},{6,4},{7,5},{8,10},{9,11},{10,... | collective-permute-start | bytes 2359304 | tf_op jit(solution)/shard_map/ppermute | solution.py:269
  255.8 35.0 %collective-permute-start.43 = (bf16[768,512]{1,0:T(8,128)(2,1)S(1)}, bf16[768,512]{1,0:T(8,128)(2,1)S(1)}, u32[]{:S(2)}, u32[]{:S(2)}) collective-permute-start(bf16[768,512]{1,0:T(8,128)(2,1)S(1)} %fusion.7.refs_3_), channel_id=1, source_target_pairs={{0,2},{1,3},{2,0},{3,1},{4,6},{5,7},{6,4},{7,5},{8,10},{9,11},{10,... | collective-permute-start | bytes 2359304 | tf_op jit(solution)/shard_map/ppermute | solution.py:269
  259.4 30.2 %collective-permute-start.40 = (bf16[256,1408]{1,0:T(8,128)(2,1)}, bf16[256,1408]{1,0:T(8,128)(2,1)}, u32[]{:S(2)}, u32[]{:S(2)}) collective-permute-start(bf16[256,1408]{1,0:T(8,128)(2,1)} %collective-permute-done.33.refs_14_), channel_id=1, source_target_pairs={{0,8},{4,0},{8,16},{12,4},{16,24},{20,12},{24,28},{28,20},{1,9},{5... | collective-permute-start | bytes 2162696 | tf_op jit(solution)/shard_map/ppermute | solution.py:218
  260.9 30.0 %collective-permute-start.41 = (bf16[256,1408]{1,0:T(8,128)(2,1)}, bf16[256,1408]{1,0:T(8,128)(2,1)}, u32[]{:S(2)}, u32[]{:S(2)}) collective-permute-start(bf16[256,1408]{1,0:T(8,128)(2,1)} %collective-permute-done.34.refs_8_), channel_id=1, source_target_pairs={{0,4},{4,12},{8,0},{12,20},{16,8},{20,28},{24,16},{28,24},{1,5},{5... | collective-permute-start | bytes 2162696 | tf_op jit(solution)/shard_map/ppermute | solution.py:218
  293.4 31.6 %collective-permute-start.47 = (bf16[256,1408]{1,0:T(8,128)(2,1)}, bf16[256,1408]{1,0:T(8,128)(2,1)}, u32[]{:S(2)}, u32[]{:S(2)}) collective-permute-start(bf16[256,1408]{1,0:T(8,128)(2,1)} %collective-permute-done.40.refs_13_), channel_id=1, source_target_pairs={{0,8},{4,0},{8,16},{12,4},{16,24},{20,12},{24,28},{28,20},{1,9},{5... | collective-permute-start | bytes 2162696 | tf_op jit(solution)/shard_map/ppermute | solution.py:218
  294.2 31.6 %collective-permute-start.48 = (bf16[256,1408]{1,0:T(8,128)(2,1)}, bf16[256,1408]{1,0:T(8,128)(2,1)}, u32[]{:S(2)}, u32[]{:S(2)}) collective-permute-start(bf16[256,1408]{1,0:T(8,128)(2,1)} %collective-permute-done.41.refs_9_), channel_id=1, source_target_pairs={{0,4},{4,12},{8,0},{12,20},{16,8},{20,28},{24,16},{28,24},{1,5},{5... | collective-permute-start | bytes 2162696 | tf_op jit(solution)/shard_map/ppermute | solution.py:218
  338.7 20.8 %collective-permute-start.53 = (bf16[768,512]{1,0:T(8,128)(2,1)S(1)}, bf16[768,512]{1,0:T(8,128)(2,1)}, u32[]{:S(2)}, u32[]{:S(2)}) collective-permute-start(bf16[768,512]{1,0:T(8,128)(2,1)S(1)} %bitcast.62), channel_id=1, source_target_pairs={{0,2},{1,3},{2,0},{3,1},{4,6},{5,7},{6,4},{7,5},{8,10},{9,11},{10,... | collective-permute-start | bytes 2359304 | tf_op jit(solution)/shard_map/ppermute | solution.py:269
  342.2 31.9 %collective-permute-start.52 = (bf16[256,1408]{1,0:T(8,128)(2,1)}, bf16[256,1408]{1,0:T(8,128)(2,1)}, u32[]{:S(2)}, u32[]{:S(2)}) collective-permute-start(bf16[256,1408]{1,0:T(8,128)(2,1)} %collective-permute-done.47.refs_12_), channel_id=1, source_target_pairs={{0,8},{4,0},{8,16},{12,4},{16,24},{20,12},{24,28},{28,20},{1,9},{5... | collective-permute-start | bytes 2162696 | tf_op jit(solution)/shard_map/ppermute | solution.py:218
  361.1 25.9 %collective-permute-start.59 = (bf16[768,512]{1,0:T(8,128)(2,1)S(1)}, bf16[768,512]{1,0:T(8,128)(2,1)S(1)}, u32[]{:S(2)}, u32[]{:S(2)}) collective-permute-start(bf16[768,512]{1,0:T(8,128)(2,1)S(1)} %fusion.4.refs_3_), channel_id=1, source_target_pairs={{0,2},{1,3},{2,0},{3,1},{4,6},{5,7},{6,4},{7,5},{8,10},{9,11},{10,... | collective-permute-start | bytes 2359304 | tf_op jit(solution)/shard_map/ppermute | solution.py:269
  389.5 30.3 %collective-permute-start.63 = (bf16[704,256]{1,0:T(8,128)(2,1)S(1)}, bf16[704,256]{1,0:T(8,128)(2,1)}, u32[]{:S(2)}, u32[]{:S(2)}) collective-permute-start(bf16[704,256]{1,0:T(8,128)(2,1)S(1)} %collective-permute-done.56.refs_11_), channel_id=1, source_target_pairs={{0,8},{4,0},{8,16},{12,4},{16,24},{20,12},{24,28},{28,20},{1,9},{5... | collective-permute-start | bytes 1081352 | tf_op jit(solution)/shard_map/ppermute | solution.py:218
  398.8 21.1 %collective-permute-start.64 = (bf16[704,256]{1,0:T(8,128)(2,1)}, bf16[704,256]{1,0:T(8,128)(2,1)}, u32[]{:S(2)}, u32[]{:S(2)}) collective-permute-start(bf16[704,256]{1,0:T(8,128)(2,1)} %collective-permute-done.57.refs_5_), channel_id=1, source_target_pairs={{0,4},{4,12},{8,0},{12,20},{16,8},{20,28},{24,16},{28,24},{1,5},{5... | collective-permute-start | bytes 1081352 | tf_op jit(solution)/shard_map/ppermute | solution.py:218
  400.1 21.9 %collective-permute-start.61 = (bf16[704,256]{1,0:T(8,128)(2,1)}, bf16[704,256]{1,0:T(8,128)(2,1)}, u32[]{:S(2)}, u32[]{:S(2)}) collective-permute-start(bf16[704,256]{1,0:T(8,128)(2,1)} %copy-done.35), channel_id=1, source_target_pairs={{0,8},{4,0},{8,16},{12,4},{16,24},{20,12},{24,28},{28,20},{1,9},{5... | collective-permute-start | bytes 1081352 | tf_op jit(solution)/shard_map/ppermute | solution.py:218
  401.6 20.4 %collective-permute-start.62 = (bf16[704,256]{1,0:T(8,128)(2,1)}, bf16[704,256]{1,0:T(8,128)(2,1)}, u32[]{:S(2)}, u32[]{:S(2)}) collective-permute-start(bf16[704,256]{1,0:T(8,128)(2,1)} %copy-done.36), channel_id=1, source_target_pairs={{0,4},{4,12},{8,0},{12,20},{16,8},{20,28},{24,16},{28,24},{1,5},{5... | collective-permute-start | bytes 1081352 | tf_op jit(solution)/shard_map/ppermute | solution.py:218
  (85 other events, 1958.9 us)

commit v2 on v1

--- a/solution.py
+++ b/solution.py
@@ -198,30 +198,41 @@
         return [self.shards[offset] for offset in range(self.ring.count)]
 
 
+GATE_ONE, UP_ONE, DOWN_ONE, MIX, GATE_TWO, UP_TWO, DOWN_TWO, DOWN_MORE = range(8)
+
+
+def order_of(steps):
+    order = [GATE_ONE, UP_ONE] * steps + [DOWN_ONE, MIX] * steps
+    late = [DOWN_TWO, DOWN_MORE] * steps
+    for left in reversed(range(steps)):
+        order += [GATE_TWO, UP_TWO]
+        order += [late.pop(0) for _ in range(2 if left == 1 else min(left, 1))]
+    return order + late
+
+
+def may_launch(waiting, flying, depth):
+    return bool(waiting) and len(flying) < depth and waiting[0] not in flying
+
+
 class Pump:
-    def __init__(self, depth):
-        self.depth = depth
-        self.waiting = []
+    def __init__(self, groups, order, depth):
+        self.groups, self.depth = groups, depth
+        self.waiting = list(order)
         self.flying = []
         self.sent = 0
         self.mark = lax.axis_index("fs")
 
-    def add(self, *groups):
-        steps = max(group[0].steps() for group in groups)
-        for _ in range(steps):
-            self.waiting += [list(group) for group in groups]
-
     def launch(self, value):
-        group = self.waiting.pop(0)
-        sends = [send for item in group for send in item.sends()]
+        key = self.waiting.pop(0)
+        sends = [send for item in self.groups[key] for send in item.sends()]
         arrays, value = tie([array for array, _ in sends], value)
         landed = [lax.ppermute(a, "fs", way) for a, (_, way) in zip(arrays, sends)]
-        self.flying.append((group, landed, self.sent))
+        self.flying.append((key, landed, self.sent))
         self.sent += 1
         return value
 
     def fill(self, value):
-        while self.waiting and len(self.flying) < self.depth:
+        while may_launch(self.waiting, [key for key, _, _ in self.flying], self.depth):
             value = self.launch(value)
         return value
 
@@ -234,13 +245,13 @@
         for _ in range(times):
             if not self.flying:
                 return value
-            group, landed, _ = self.flying.pop(0)
+            key, landed, _ = self.flying.pop(0)
             landed, self.mark, value = tie(landed, self.mark, value)
             landed = list(landed)
-            for item in group:
+            for item in self.groups[key]:
                 item.accept(landed)
             self.mark, value = self.fill((self.mark, value))
-            if len(self.flying) == self.depth:
+            if self.flying:
                 self.mark = self.mark + 1
                 self.mark, value = tie(self.mark, value)
         return value
@@ -327,7 +338,7 @@
 def solution(mesh):
     order = grid_ring(mesh)
     cores = cores_of(mesh)
-    depth = 2
+    depth = 3
 
     def per_device(
         tokens,
@@ -349,7 +360,6 @@
         ring = Ring(order)
         features = Features(lax.axis_size("tp"), cores)
         channels = conv_ln_gain.shape[0] * lax.axis_size("tp")
-        pump = Pump(depth)
         wide = conv_value.shape[1]
         half = ffn_two_down.shape[0] // 2
         one_gate = Gathered(ring, ffn_one_gate, True)
@@ -369,10 +379,17 @@
             Gathered(ring, ffn_two_down[:half], True),
             Gathered(ring, ffn_two_down[half:], False),
         ]
-        pump.add([one_gate], [one_up])
-        pump.add([one_down], mixes)
-        pump.add([two_gate], [two_up])
-        pump.add([two_down[0]], [two_down[1]])
+        groups = {
+            GATE_ONE: [one_gate],
+            UP_ONE: [one_up],
+            DOWN_ONE: [one_down],
+            MIX: mixes,
+            GATE_TWO: [two_gate],
+            UP_TWO: [two_up],
+            DOWN_TWO: [two_down[0]],
+            DOWN_MORE: [two_down[1]],
+        }
+        pump = Pump(groups, order_of(ring.count // 2), depth)
 
         count = features.count
         each = ring.count // count
@@ -467,7 +484,7 @@
             feature_group_count=gated_lin.shape[1],
             precision=lax.Precision.HIGHEST,
         )[0]
-        convolved = pump.turn(convolved)
+        convolved = pump.turn(convolved, 2)
         sum_one, sum_two = lax.psum(
             (jnp.sum(convolved, axis=1), jnp.sum(convolved * convolved, axis=1)), "tp"
         )
@@ -483,7 +500,7 @@
         far = features.gather_far(stream_two)
         stream_two = pump.turn(stream_two, 3)
         parts = features.gather_near([stream_two] + far)
-        parts = pump.until([two_gate, two_up], pump.turn(parts))
+        parts = pump.until([two_gate, two_up], parts)
         hidden = hidden_of(
             parts, ffn_two_gain, [two_gate, two_up], (0, 0), ffn_two_up.shape[1], silu_times,
             jnp.bfloat16,

time: 490 us -> 477 us (0.973)
  waiting for transfers between devices: 304 us -> 291 us
    ppermute x56, waiting for transfers between devices: 278 us -> 264 us  [launch(): landed = [lax.ppermute(a, 'fs', way) for a, (_, way) in zip(arrays, sends)]]
  transfers between devices with their start and end apart: 74 -> 74, of which waited for: 43 -> 43; matrix products, arithmetic and copies ran while one was open for 4% -> 5% of each run, Pallas kernels for 9% -> 9%
where the time goes in v2:
time: 477 us; the launch traced here: 476 us
  waiting for transfers between devices  291 us (61%)
  Pallas kernels  80.8 us (17%)
  starting transfers between devices  66.3 us (14%)
  other arithmetic  17.4 us (4%)
  local copies, waits for them, and re-layouts  7.46 us (2%)
  matrix products  6.93 us (1%)
  blocking collectives  6.17 us (1%)
    ppermute x56, waiting for transfers between devices, launch(): landed = [lax.ppermute(a, 'fs', way) for a, (_, way) in zip(arrays, sends)]  264 us
    ppermute x56, starting transfers between devices, launch(): landed = [lax.ppermute(a, 'fs', way) for a, (_, way) in zip(arrays, sends)]  57.1 us
    pallas_call x3, Pallas kernels, hidden_of(): pl.pallas_call(lambda *refs: hidden_kernel(count, ring.count, len(sides),...  42.5 us
    pallas_call x6, Pallas kernels, terms_of(): pl.pallas_call(lambda *refs: terms_kernel(ring.count, len(sides), low, co...  38.4 us
    ppermute x6, waiting for transfers between devices, across_chip(): return lax.ppermute(value, 'tp', pairs)  17.5 us
  transfers between devices with their start and end apart: 74, of which 43 were waited for; matrix products, arithmetic and copies ran while one was open for 5% of the time, Pallas kernels for 9%

profile of v2, /device:TPU:0, one launch (start us, length us, event | category | flops | bytes accessed | tf_op | source)
XLA Modules:
  0.0 476.4 jit_solution(16036785259619583404)
XLA Ops:
  5.0 15.8 %collective-permute-done.refs_14_ = bf16[256,1408]{1,0:T(8,128)(2,1)S(1)} collective-permute-done((bf16[256,1408]{1,0:T(8,128)(2,1)}, bf16[256,1408]{1,0:T(8,128)(2,1)S(1)}, u32[]{:S(2)}, u32[]{:S(2)}) %collective-permute-start) | collective-permute-done | bytes 720928 | tf_op jit(solution)/shard_map/ppermute | solution.py:229
  25.8 15.7 %collective-permute-done.5.refs_22_ = bf16[256,1408]{1,0:T(8,128)(2,1)} collective-permute-done((bf16[256,1408]{1,0:T(8,128)(2,1)}, bf16[256,1408]{1,0:T(8,128)(2,1)}, u32[]{:S(2)}, u32[]{:S(2)}) %collective-permute-start.5) | collective-permute-done | bytes 720928 | tf_op jit(solution)/shard_map/ppermute | solution.py:229
  45.4 11.7 %collective-permute-done.3.refs_13_ = bf16[256,1408]{1,0:T(8,128)(2,1)} collective-permute-done((bf16[256,1408]{1,0:T(8,128)(2,1)S(1)}, bf16[256,1408]{1,0:T(8,128)(2,1)}, u32[]{:S(2)}, u32[]{:S(2)}) %collective-permute-start.3) | collective-permute-done | bytes 720928 | tf_op jit(solution)/shard_map/ppermute | solution.py:229
  62.7 9.8 %collective-permute-done.11.refs_21_ = bf16[256,1408]{1,0:T(8,128)(2,1)} collective-permute-done((bf16[256,1408]{1,0:T(8,128)(2,1)}, bf16[256,1408]{1,0:T(8,128)(2,1)}, u32[]{:S(2)}, u32[]{:S(2)}) %collective-permute-start.11) | collective-permute-done | bytes 720928 | tf_op jit(solution)/shard_map/ppermute | solution.py:229
  80.2 11.3 %collective-permute-done.10.refs_10_ = bf16[256,1408]{1,0:T(8,128)(2,1)} collective-permute-done((bf16[256,1408]{1,0:T(8,128)(2,1)}, bf16[256,1408]{1,0:T(8,128)(2,1)}, u32[]{:S(2)}, u32[]{:S(2)}) %collective-permute-start.10) | collective-permute-done | bytes 720928 | tf_op jit(solution)/shard_map/ppermute | solution.py:229
  93.2 10.2 %collective-permute-done.14.refs_20_ = bf16[256,1408]{1,0:T(8,128)(2,1)} collective-permute-done((bf16[256,1408]{1,0:T(8,128)(2,1)}, bf16[256,1408]{1,0:T(8,128)(2,1)}, u32[]{:S(2)}, u32[]{:S(2)}) %collective-permute-start.14) | collective-permute-done | bytes 720928 | tf_op jit(solution)/shard_map/ppermute | solution.py:229
  109.9 8.4 %collective-permute-done.13.refs_11_ = bf16[256,1408]{1,0:T(8,128)(2,1)} collective-permute-done((bf16[256,1408]{1,0:T(8,128)(2,1)}, bf16[256,1408]{1,0:T(8,128)(2,1)}, u32[]{:S(2)}, u32[]{:S(2)}) %collective-permute-start.13) | collective-permute-done | bytes 720928 | tf_op jit(solution)/shard_map/ppermute | solution.py:229
  121.7 17.8 %hidden.3.refs_3_ = bf16[768,1408]{1,0:T(8,128)(2,1)} custom-call(s32[8]{0:T(128)} %get-tuple-element.745.refs_0_, s32[4]{0:T(128)} %pad_add_fusion.refs_1_, f32[4,1,512]{2,1,0:T(1,128)} %bitcast.66, bf16[768,512]{1,0:T(8,128)(2,1)} %refs_3_, bf16[768,512]{1,0:T(8,128)(2,1)} %copy-done.22, bf16[768,512]{1,0:T(8,128)(2,1)} %copy-done.21, ...), custom_call_target="tpu_custom_call" | custom-call | flops 8858370048 | bytes 14680064 | tf_op jit(solution)/shard_map/hidden/pallas_call | solution.py:405
  143.6 20.3 %collective-permute-done.16.refs_14_.refs_11_ = bf16[256,768]{1,0:T(8,128)(2,1)S(1)} collective-permute-done((bf16[256,768]{1,0:T(8,128)(2,1)S(1)}, bf16[256,768]{1,0:T(8,128)(2,1)S(1)}, u32[]{:S(2)}, u32[]{:S(2)}) %collective-permute-start.16) | collective-permute-done | bytes 393248 | tf_op jit(solution)/shard_map/ppermute | solution.py:229
  169.3 20.6 %collective-permute-done.21.refs_13_.refs_10_ = bf16[256,768]{1,0:T(8,128)(2,1)S(1)} collective-permute-done((bf16[256,768]{1,0:T(8,128)(2,1)S(1)}, bf16[256,768]{1,0:T(8,128)(2,1)S(1)}, u32[]{:S(2)}, u32[]{:S(2)}) %collective-permute-start.21) | collective-permute-done | bytes 393248 | tf_op jit(solution)/shard_map/ppermute | solution.py:229
  194.3 9.1 %collective-permute-done.25.refs_12_.refs_9_ = bf16[256,768]{1,0:T(8,128)(2,1)S(1)} collective-permute-done((bf16[256,768]{1,0:T(8,128)(2,1)S(1)}, bf16[256,768]{1,0:T(8,128)(2,1)S(1)}, u32[]{:S(2)}, u32[]{:S(2)}) %collective-permute-start.25) | collective-permute-done | bytes 393248 | tf_op jit(solution)/shard_map/ppermute | solution.py:229
  206.2 6.3 %collective-permute-done.30.refs_8_ = bf16[1408,256]{1,0:T(8,128)(2,1)} collective-permute-done((bf16[1408,256]{1,0:T(8,128)(2,1)}, bf16[1408,256]{1,0:T(8,128)(2,1)}, u32[]{:S(2)}, u32[]{:S(2)}) %collective-permute-start.30) | collective-permute-done | bytes 720928 | tf_op jit(solution)/shard_map/ppermute | solution.py:229
  212.5 7.4 %far_terms.3 = (bf16[1,768,512]{2,1,0:T(8,128)(2,1)}, bf16[1,768,512]{2,1,0:T(8,128)(2,1)}) custom-call(s32[8]{0:T(128)} %get-tuple-element.744.refs_0_, s32[8]{0:T(128)} %get-tuple-element.737.refs_1_, s32[8]{0:T(128)} %get-tuple-element.735.refs_2_, bf16[768,1408]{1,0:T(8,128)(2,1)} %hidden.3.refs_3_, bf16[1408,256]{1,0:T(8,128)(2,1)} %refs_4_.3, ...), custom_call_target="tpu_custom_call" | custom-call | flops 2214592512 | bytes 2883584 | tf_op jit(solution)/shard_map/far_terms/pallas_call | solution.py:431
  223.9 7.3 %near_terms.3 = (bf16[1,768,512]{2,1,0:T(8,128)(2,1)}, bf16[1,768,512]{2,1,0:T(8,128)(2,1)}) custom-call(s32[8]{0:T(128)} %get-tuple-element.744.refs_0_, s32[8]{0:T(128)} %get-tuple-element.737.refs_1_, s32[8]{0:T(128)} %get-tuple-element.735.refs_2_, bf16[768,1408]{1,0:T(8,128)(2,1)} %hidden.3.refs_3_, bf16[1408,256]{1,0:T(8,128)(2,1)} %refs_4_.3, ...), custom_call_target="tpu_custom_call" | custom-call | flops 2214592512 | bytes 2883584 | tf_op jit(solution)/shard_map/near_terms/pallas_call | solution.py:431
  237.4 13.8 %collective-permute-done.35.refs_14_ = bf16[256,1408]{1,0:T(8,128)(2,1)} collective-permute-done((bf16[256,1408]{1,0:T(8,128)(2,1)}, bf16[256,1408]{1,0:T(8,128)(2,1)}, u32[]{:S(2)}, u32[]{:S(2)}) %collective-permute-start.35) | collective-permute-done | bytes 720928 | tf_op jit(solution)/shard_map/ppermute | solution.py:229
  257.8 9.0 %collective-permute-done.33.refs_22_ = bf16[256,1408]{1,0:T(8,128)(2,1)} collective-permute-done((bf16[256,1408]{1,0:T(8,128)(2,1)}, bf16[256,1408]{1,0:T(8,128)(2,1)}, u32[]{:S(2)}, u32[]{:S(2)}) %collective-permute-start.33) | collective-permute-done | bytes 720928 | tf_op jit(solution)/shard_map/ppermute | solution.py:229
  268.3 5.2 %collective-permute-done.31.refs_11_ = bf16[704,256]{1,0:T(8,128)(2,1)S(1)} collective-permute-done((bf16[704,256]{1,0:T(8,128)(2,1)}, bf16[704,256]{1,0:T(8,128)(2,1)S(1)}, u32[]{:S(2)}, u32[]{:S(2)}) %collective-permute-start.31) | collective-permute-done | bytes 360480 | tf_op jit(solution)/shard_map/ppermute | solution.py:229
  281.3 6.8 %hidden.4 = f32[768,256]{1,0:T(8,128)} custom-call(s32[8]{0:T(128)} %get-tuple-element.745.refs_0_, s32[4]{0:T(128)} %pad_add_fusion.refs_1_, f32[4,1,512]{2,1,0:T(1,128)} %bitcast.65, bf16[768,512]{1,0:T(8,128)(2,1)} %copy-done.2, bf16[768,512]{1,0:T(8,128)(2,1)} %copy-done.15, bf16[768,512]{1,0:T(8,128)(2,1)} %copy-done.14, bf16[768,512]{1,0:T(8,128)(2,1)} %copy-done.16, ...), custom_call_target="tpu_custom_call" | custom-call | flops 1610612736 | bytes 5242880 | tf_op jit(solution)/shard_map/hidden/pallas_call | solution.py:405
  288.2 6.9 %fusion.9 = f32[1,768,256]{2,0,1:T(1,128)S(1)} fusion(f32[1,768,256]{2,1,0:T(8,128)} %bitcast.61, f32[31,1,256]{2,0,1:T(8,128)S(1)} %bitcast.58), kind=kOutput, calls=%fused_computation.18 | convolution fusion | flops 72400896 | bytes 1604608 | tf_op jit(solution)/shard_map/conv_general_dilated | solution.py:478
  296.4 13.7 %collective-permute-done.42.refs_21_ = bf16[256,1408]{1,0:T(8,128)(2,1)} collective-permute-done((bf16[256,1408]{1,0:T(8,128)(2,1)}, bf16[256,1408]{1,0:T(8,128)(2,1)}, u32[]{:S(2)}, u32[]{:S(2)}) %collective-permute-start.42) | collective-permute-done | bytes 720928 | tf_op jit(solution)/shard_map/ppermute | solution.py:229
  311.4 6.2 %all-reduce = (f32[768]{0:T(1024)S(1)}, f32[768]{0:T(1024)S(1)}) all-reduce(f32[768]{0:T(1024)S(1)} %get-tuple-element.732, f32[768]{0:T(1024)S(1)} %get-tuple-element.731), channel_id=1, replica_groups=mesh['fs'=8,'tp'=4] {'tp'}, use_global_device_ids=true, to_apply=%region_3.4 | all-reduce | flops 1536 | bytes 12288 | tf_op jit(solution)/shard_map/psum | solution.py:488
  327.1 4.4 near_terms.4
  338.5 13.8 %collective-permute-done.49.refs_12_ = bf16[256,1408]{1,0:T(8,128)(2,1)} collective-permute-done((bf16[256,1408]{1,0:T(8,128)(2,1)}, bf16[256,1408]{1,0:T(8,128)(2,1)}, u32[]{:S(2)}, u32[]{:S(2)}) %collective-permute-start.49) | collective-permute-done | bytes 720928 | tf_op jit(solution)/shard_map/ppermute | solution.py:229
  358.0 9.8 %collective-permute-done.55.refs_20_ = bf16[256,1408]{1,0:T(8,128)(2,1)} collective-permute-done((bf16[256,1408]{1,0:T(8,128)(2,1)}, bf16[256,1408]{1,0:T(8,128)(2,1)}, u32[]{:S(2)}, u32[]{:S(2)}) %collective-permute-start.55) | collective-permute-done | bytes 720928 | tf_op jit(solution)/shard_map/ppermute | solution.py:229
  369.8 5.6 %collective-permute-done.58.refs_10_ = bf16[704,256]{1,0:T(8,128)(2,1)S(1)} collective-permute-done((bf16[704,256]{1,0:T(8,128)(2,1)S(1)}, bf16[704,256]{1,0:T(8,128)(2,1)S(1)}, u32[]{:S(2)}, u32[]{:S(2)}) %collective-permute-start.58) | collective-permute-done | bytes 360480 | tf_op jit(solution)/shard_map/ppermute | solution.py:229
  377.0 5.3 %collective-permute-done.53.refs_18_ = bf16[704,256]{1,0:T(8,128)(2,1)S(1)} collective-permute-done((bf16[704,256]{1,0:T(8,128)(2,1)}, bf16[704,256]{1,0:T(8,128)(2,1)S(1)}, u32[]{:S(2)}, u32[]{:S(2)}) %collective-permute-start.53) | collective-permute-done | bytes 360480 | tf_op jit(solution)/shard_map/ppermute | solution.py:229
  387.4 16.2 %collective-permute-done.60.refs_11_ = bf16[256,1408]{1,0:T(8,128)(2,1)S(1)} collective-permute-done((bf16[256,1408]{1,0:T(8,128)(2,1)}, bf16[256,1408]{1,0:T(8,128)(2,1)S(1)}, u32[]{:S(2)}, u32[]{:S(2)}) %collective-permute-start.60) | collective-permute-done | bytes 720928 | tf_op jit(solution)/shard_map/ppermute | solution.py:229
  406.6 17.9 %hidden.5.refs_3_ = bf16[768,1408]{1,0:T(8,128)(2,1)} custom-call(s32[8]{0:T(128)} %get-tuple-element.745.refs_0_, s32[4]{0:T(128)} %pad_add_fusion.refs_1_, f32[4,1,512]{2,1,0:T(1,128)} %bitcast.67, bf16[768,512]{1,0:T(8,128)(2,1)} %copy-done.12, bf16[768,512]{1,0:T(8,128)(2,1)} %copy-done.25, bf16[768,512]{1,0:T(8,128)(2,1)} %copy-done.24, ...), custom_call_target="tpu_custom_call" | custom-call | flops 8858370048 | bytes 14680064 | tf_op jit(solution)/shard_map/hidden/pallas_call | solution.py:405
  426.6 6.9 %collective-permute-done.70.refs_8_ = bf16[704,256]{1,0:T(8,128)(2,1)S(1)} collective-permute-done((bf16[704,256]{1,0:T(8,128)(2,1)S(1)}, bf16[704,256]{1,0:T(8,128)(2,1)S(1)}, u32[]{:S(2)}, u32[]{:S(2)}) %collective-permute-start.70) | collective-permute-done | bytes 360480 | tf_op jit(solution)/shard_map/ppermute | solution.py:229
  435.2 7.3 %far_terms.5 = (bf16[1,768,512]{2,1,0:T(8,128)(2,1)}, bf16[1,768,512]{2,1,0:T(8,128)(2,1)}) custom-call(s32[8]{0:T(128)} %get-tuple-element.744.refs_0_, s32[8]{0:T(128)} %get-tuple-element.737.refs_1_, s32[8]{0:T(128)} %get-tuple-element.735.refs_2_, bf16[768,1408]{1,0:T(8,128)(2,1)} %hidden.5.refs_3_, bf16[704,256]{1,0:T(8,128)(2,1)} %get-tuple-element.547.refs_4_, ...), custom_call_target="tpu_custom_call" | custom-call | flops 2214592512 | bytes 2883584 | tf_op jit(solution)/shard_map/far_terms/pallas_call | solution.py:431
  446.4 7.5 %near_terms.5 = (bf16[1,768,512]{2,1,0:T(8,128)(2,1)}, bf16[1,768,512]{2,1,0:T(8,128)(2,1)}) custom-call(s32[8]{0:T(128)} %get-tuple-element.744.refs_0_, s32[8]{0:T(128)} %get-tuple-element.737.refs_1_, s32[8]{0:T(128)} %get-tuple-element.735.refs_2_, bf16[768,1408]{1,0:T(8,128)(2,1)} %hidden.5.refs_3_, bf16[704,256]{1,0:T(8,128)(2,1)} %get-tuple-element.547.refs_4_, ...), custom_call_target="tpu_custom_call" | custom-call | flops 2214592512 | bytes 2883584 | tf_op jit(solution)/shard_map/near_terms/pallas_call | solution.py:431
  456.5 17.5 %collective-permute-done.73 = bf16[768,512]{1,0:T(8,128)(2,1)S(1)} collective-permute-done((bf16[768,512]{1,0:T(8,128)(2,1)S(1)}, bf16[768,512]{1,0:T(8,128)(2,1)S(1)}, u32[]{:S(2)}, u32[]{:S(2)}) %collective-permute-start.73) | collective-permute-done | bytes 786464 | tf_op jit(solution)/shard_map/ppermute | solution.py:280
  (223 shorter events, 130.6 us)
Async XLA Ops:
  0.0 22.1 %collective-permute-start.2 = (bf16[768,512]{1,0:T(8,128)(2,1)}, bf16[768,512]{1,0:T(8,128)(2,1)S(1)}, u32[]{:S(2)}, u32[]{:S(2)}) collective-permute-start(bf16[768,512]{1,0:T(8,128)(2,1)} %refs_3_), channel_id=1, source_target_pairs={{0,2},{1,3},{2,0},{3,1},{4,6},{5,7},{6,4},{7,5},{8,10},{9,11},{10,... | collective-permute-start | bytes 2359304 | tf_op jit(solution)/shard_map/ppermute | solution.py:280
  5.0 37.3 %collective-permute-start.7 = (bf16[768,512]{1,0:T(8,128)(2,1)}, bf16[768,512]{1,0:T(8,128)(2,1)S(1)}, u32[]{:S(2)}, u32[]{:S(2)}) collective-permute-start(bf16[768,512]{1,0:T(8,128)(2,1)} %refs_3_), channel_id=1, source_target_pairs={{0,1},{1,0},{2,3},{3,2},{4,5},{5,4},{6,7},{7,6},{8,9},{9,8},{10,11... | collective-permute-start | bytes 2359304 | tf_op jit(solution)/shard_map/ppermute | solution.py:272
  24.3 32.7 %collective-permute-start.3 = (bf16[256,1408]{1,0:T(8,128)(2,1)S(1)}, bf16[256,1408]{1,0:T(8,128)(2,1)}, u32[]{:S(2)}, u32[]{:S(2)}) collective-permute-start(bf16[256,1408]{1,0:T(8,128)(2,1)S(1)} %collective-permute-done.refs_14_), channel_id=1, source_target_pairs={{0,8},{4,0},{8,16},{12,4},{16,24},{20,12},{24,28},{28,20},{1,9},{5... | collective-permute-start | bytes 2162696 | tf_op jit(solution)/shard_map/ppermute | solution.py:229
  43.3 29.1 %collective-permute-start.11 = (bf16[256,1408]{1,0:T(8,128)(2,1)}, bf16[256,1408]{1,0:T(8,128)(2,1)}, u32[]{:S(2)}, u32[]{:S(2)}) collective-permute-start(bf16[256,1408]{1,0:T(8,128)(2,1)} %collective-permute-done.5.refs_22_), channel_id=1, source_target_pairs={{0,8},{4,0},{8,16},{12,4},{16,24},{20,12},{24,28},{28,20},{1,9},{5... | collective-permute-start | bytes 2162696 | tf_op jit(solution)/shard_map/ppermute | solution.py:229
  44.9 31.2 %collective-permute-start.12 = (bf16[256,1408]{1,0:T(8,128)(2,1)}, bf16[256,1408]{1,0:T(8,128)(2,1)}, u32[]{:S(2)}, u32[]{:S(2)}) collective-permute-start(bf16[256,1408]{1,0:T(8,128)(2,1)} %collective-permute-done.6.refs_16_), channel_id=1, source_target_pairs={{0,4},{4,12},{8,0},{12,20},{16,8},{20,28},{24,16},{28,24},{1,5},{5... | collective-permute-start | bytes 2162696 | tf_op jit(solution)/shard_map/ppermute | solution.py:229
  60.7 30.9 %collective-permute-start.10 = (bf16[256,1408]{1,0:T(8,128)(2,1)}, bf16[256,1408]{1,0:T(8,128)(2,1)}, u32[]{:S(2)}, u32[]{:S(2)}) collective-permute-start(bf16[256,1408]{1,0:T(8,128)(2,1)} %collective-permute-done.4.refs_9_), channel_id=1, source_target_pairs={{0,4},{4,12},{8,0},{12,20},{16,8},{20,28},{24,16},{28,24},{1,5},{5... | collective-permute-start | bytes 2162696 | tf_op jit(solution)/shard_map/ppermute | solution.py:229
  61.1 30.4 %collective-permute-start.9 = (bf16[256,1408]{1,0:T(8,128)(2,1)}, bf16[256,1408]{1,0:T(8,128)(2,1)}, u32[]{:S(2)}, u32[]{:S(2)}) collective-permute-start(bf16[256,1408]{1,0:T(8,128)(2,1)} %collective-permute-done.3.refs_13_), channel_id=1, source_target_pairs={{0,8},{4,0},{8,16},{12,4},{16,24},{20,12},{24,28},{28,20},{1,9},{5... | collective-permute-start | bytes 2162696 | tf_op jit(solution)/shard_map/ppermute | solution.py:229
  76.1 27.2 %collective-permute-start.14 = (bf16[256,1408]{1,0:T(8,128)(2,1)}, bf16[256,1408]{1,0:T(8,128)(2,1)}, u32[]{:S(2)}, u32[]{:S(2)}) collective-permute-start(bf16[256,1408]{1,0:T(8,128)(2,1)} %collective-permute-done.11.refs_21_), channel_id=1, source_target_pairs={{0,8},{4,0},{8,16},{12,4},{16,24},{20,12},{24,28},{28,20},{1,9},{5... | collective-permute-start | bytes 2162696 | tf_op jit(solution)/shard_map/ppermute | solution.py:229
  77.7 27.4 %collective-permute-start.15 = (bf16[256,1408]{1,0:T(8,128)(2,1)}, bf16[256,1408]{1,0:T(8,128)(2,1)}, u32[]{:S(2)}, u32[]{:S(2)}) collective-permute-start(bf16[256,1408]{1,0:T(8,128)(2,1)} %collective-permute-done.12.refs_17_), channel_id=1, source_target_pairs={{0,4},{4,12},{8,0},{12,20},{16,8},{20,28},{24,16},{28,24},{1,5},{5... | collective-permute-start | bytes 2162696 | tf_op jit(solution)/shard_map/ppermute | solution.py:229
  91.6 26.7 %collective-permute-start.13 = (bf16[256,1408]{1,0:T(8,128)(2,1)}, bf16[256,1408]{1,0:T(8,128)(2,1)}, u32[]{:S(2)}, u32[]{:S(2)}) collective-permute-start(bf16[256,1408]{1,0:T(8,128)(2,1)} %collective-permute-done.9.refs_12_), channel_id=1, source_target_pairs={{0,8},{4,0},{8,16},{12,4},{16,24},{20,12},{24,28},{28,20},{1,9},{5... | collective-permute-start | bytes 2162696 | tf_op jit(solution)/shard_map/ppermute | solution.py:229
  118.3 21.2 %collective-permute-start.18 = (bf16[1408,256]{1,0:T(8,128)(2,1)}, bf16[1408,256]{1,0:T(8,128)(2,1)}, u32[]{:S(2)}, u32[]{:S(2)}) collective-permute-start(bf16[1408,256]{1,0:T(8,128)(2,1)} %refs_4_.3), channel_id=1, source_target_pairs={{0,8},{4,0},{8,16},{12,4},{16,24},{20,12},{24,28},{28,20},{1,9},{5... | collective-permute-start | bytes 2162696 | tf_op jit(solution)/shard_map/ppermute | solution.py:229
  139.5 25.7 %collective-permute-start.23 = (bf16[1408,256]{1,0:T(8,128)(2,1)}, bf16[1408,256]{1,0:T(8,128)(2,1)}, u32[]{:S(2)}, u32[]{:S(2)}) collective-permute-start(bf16[1408,256]{1,0:T(8,128)(2,1)} %collective-permute-done.18.refs_11_), channel_id=1, source_target_pairs={{0,8},{4,0},{8,16},{12,4},{16,24},{20,12},{24,28},{28,20},{1,9},{5... | collective-permute-start | bytes 2162696 | tf_op jit(solution)/shard_map/ppermute | solution.py:229
  141.2 24.1 %collective-permute-start.24 = (bf16[1408,256]{1,0:T(8,128)(2,1)}, bf16[1408,256]{1,0:T(8,128)(2,1)}, u32[]{:S(2)}, u32[]{:S(2)}) collective-permute-start(bf16[1408,256]{1,0:T(8,128)(2,1)} %collective-permute-done.19.refs_5_), channel_id=1, source_target_pairs={{0,4},{4,12},{8,0},{12,20},{16,8},{20,28},{24,16},{28,24},{1,5},{5... | collective-permute-start | bytes 2162696 | tf_op jit(solution)/shard_map/ppermute | solution.py:229
  141.6 22.3 %collective-permute-start.16 = (bf16[256,768]{1,0:T(8,128)(2,1)S(1)}, bf16[256,768]{1,0:T(8,128)(2,1)S(1)}, u32[]{:S(2)}, u32[]{:S(2)}) collective-permute-start(bf16[256,768]{1,0:T(8,128)(2,1)S(1)} %constant_dynamic-update-slice_fusion.refs_7_.refs_4_), channel_id=1, source_target_pairs={{0,8},{4,0},{8,16},{12,4},{16,24},{20,12},{24,28},{28,20},{1,9},{5... | collective-permute-start | bytes 1179656 | tf_op jit(solution)/shard_map/ppermute | solution.py:229
  143.2 22.0 %collective-permute-start.17 = (bf16[256,768]{1,0:T(8,128)(2,1)S(1)}, bf16[256,768]{1,0:T(8,128)(2,1)S(1)}, u32[]{:S(2)}, u32[]{:S(2)}) collective-permute-start(bf16[256,768]{1,0:T(8,128)(2,1)S(1)} %constant_dynamic-update-slice_fusion.refs_7_.refs_4_), channel_id=1, source_target_pairs={{0,4},{4,12},{8,0},{12,20},{16,8},{20,28},{24,16},{28,24},{1,5},{5... | collective-permute-start | bytes 1179656 | tf_op jit(solution)/shard_map/ppermute | solution.py:229
  165.2 28.2 %collective-permute-start.27 = (bf16[1408,256]{1,0:T(8,128)(2,1)}, bf16[1408,256]{1,0:T(8,128)(2,1)}, u32[]{:S(2)}, u32[]{:S(2)}) collective-permute-start(bf16[1408,256]{1,0:T(8,128)(2,1)} %collective-permute-done.23.refs_10_), channel_id=1, source_target_pairs={{0,8},{4,0},{8,16},{12,4},{16,24},{20,12},{24,28},{28,20},{1,9},{5... | collective-permute-start | bytes 2162696 | tf_op jit(solution)/shard_map/ppermute | solution.py:229
  166.9 26.5 %collective-permute-start.28 = (bf16[1408,256]{1,0:T(8,128)(2,1)}, bf16[1408,256]{1,0:T(8,128)(2,1)}, u32[]{:S(2)}, u32[]{:S(2)}) collective-permute-start(bf16[1408,256]{1,0:T(8,128)(2,1)} %collective-permute-done.24.refs_6_), channel_id=1, source_target_pairs={{0,4},{4,12},{8,0},{12,20},{16,8},{20,28},{24,16},{28,24},{1,5},{5... | collective-permute-start | bytes 2162696 | tf_op jit(solution)/shard_map/ppermute | solution.py:229
  167.3 22.6 %collective-permute-start.21 = (bf16[256,768]{1,0:T(8,128)(2,1)S(1)}, bf16[256,768]{1,0:T(8,128)(2,1)S(1)}, u32[]{:S(2)}, u32[]{:S(2)}) collective-permute-start(bf16[256,768]{1,0:T(8,128)(2,1)S(1)} %collective-permute-done.16.refs_14_.refs_11_), channel_id=1, source_target_pairs={{0,8},{4,0},{8,16},{12,4},{16,24},{20,12},{24,28},{28,20},{1,9},{5... | collective-permute-start | bytes 1179656 | tf_op jit(solution)/shard_map/ppermute | solution.py:229
  169.3 22.1 %collective-permute-start.22 = (bf16[256,768]{1,0:T(8,128)(2,1)S(1)}, bf16[256,768]{1,0:T(8,128)(2,1)S(1)}, u32[]{:S(2)}, u32[]{:S(2)}) collective-permute-start(bf16[256,768]{1,0:T(8,128)(2,1)S(1)} %collective-permute-done.17.refs_8_.refs_5_), channel_id=1, source_target_pairs={{0,4},{4,12},{8,0},{12,20},{16,8},{20,28},{24,16},{28,24},{1,5},{5... | collective-permute-start | bytes 1179656 | tf_op jit(solution)/shard_map/ppermute | solution.py:229
  231.4 21.4 %collective-permute-start.39 = (bf16[768,512]{1,0:T(8,128)(2,1)S(1)}, bf16[768,512]{1,0:T(8,128)(2,1)}, u32[]{:S(2)}, u32[]{:S(2)}) collective-permute-start(bf16[768,512]{1,0:T(8,128)(2,1)S(1)} %bitcast.63), channel_id=1, source_target_pairs={{0,2},{1,3},{2,0},{3,1},{4,6},{5,7},{6,4},{7,5},{8,10},{9,11},{10,... | collective-permute-start | bytes 2359304 | tf_op jit(solution)/shard_map/ppermute | solution.py:280
  234.0 32.7 %collective-permute-start.33 = (bf16[256,1408]{1,0:T(8,128)(2,1)}, bf16[256,1408]{1,0:T(8,128)(2,1)}, u32[]{:S(2)}, u32[]{:S(2)}) collective-permute-start(bf16[256,1408]{1,0:T(8,128)(2,1)} %refs_15_.3), channel_id=1, source_target_pairs={{0,8},{4,0},{8,16},{12,4},{16,24},{20,12},{24,28},{28,20},{1,9},{5... | collective-permute-start | bytes 2162696 | tf_op jit(solution)/shard_map/ppermute | solution.py:229
  235.5 32.7 %collective-permute-start.34 = (bf16[256,1408]{1,0:T(8,128)(2,1)}, bf16[256,1408]{1,0:T(8,128)(2,1)}, u32[]{:S(2)}, u32[]{:S(2)}) collective-permute-start(bf16[256,1408]{1,0:T(8,128)(2,1)} %refs_15_.3), channel_id=1, source_target_pairs={{0,4},{4,12},{8,0},{12,20},{16,8},{20,28},{24,16},{28,24},{1,5},{5... | collective-permute-start | bytes 2162696 | tf_op jit(solution)/shard_map/ppermute | solution.py:229
  277.4 32.7 %collective-permute-start.42 = (bf16[256,1408]{1,0:T(8,128)(2,1)}, bf16[256,1408]{1,0:T(8,128)(2,1)}, u32[]{:S(2)}, u32[]{:S(2)}) collective-permute-start(bf16[256,1408]{1,0:T(8,128)(2,1)} %collective-permute-done.33.refs_22_), channel_id=1, source_target_pairs={{0,8},{4,0},{8,16},{12,4},{16,24},{20,12},{24,28},{28,20},{1,9},{5... | collective-permute-start | bytes 2162696 | tf_op jit(solution)/shard_map/ppermute | solution.py:229
  278.4 32.7 %collective-permute-start.43 = (bf16[256,1408]{1,0:T(8,128)(2,1)}, bf16[256,1408]{1,0:T(8,128)(2,1)}, u32[]{:S(2)}, u32[]{:S(2)}) collective-permute-start(bf16[256,1408]{1,0:T(8,128)(2,1)} %collective-permute-done.34.refs_16_), channel_id=1, source_target_pairs={{0,4},{4,12},{8,0},{12,20},{16,8},{20,28},{24,16},{28,24},{1,5},{5... | collective-permute-start | bytes 2162696 | tf_op jit(solution)/shard_map/ppermute | solution.py:229
  280.3 38.4 %collective-permute-start.40 = (bf16[704,256]{1,0:T(8,128)(2,1)S(1)}, bf16[704,256]{1,0:T(8,128)(2,1)}, u32[]{:S(2)}, u32[]{:S(2)}) collective-permute-start(bf16[704,256]{1,0:T(8,128)(2,1)S(1)} %copy-done.19), channel_id=1, source_target_pairs={{0,8},{4,0},{8,16},{12,4},{16,24},{20,12},{24,28},{28,20},{1,9},{5... | collective-permute-start | bytes 1081352 | tf_op jit(solution)/shard_map/ppermute | solution.py:229
  295.2 23.6 %collective-permute-start.41 = (bf16[704,256]{1,0:T(8,128)(2,1)S(1)}, bf16[704,256]{1,0:T(8,128)(2,1)}, u32[]{:S(2)}, u32[]{:S(2)}) collective-permute-start(bf16[704,256]{1,0:T(8,128)(2,1)S(1)} %copy-done.19), channel_id=1, source_target_pairs={{0,4},{4,12},{8,0},{12,20},{16,8},{20,28},{24,16},{28,24},{1,5},{5... | collective-permute-start | bytes 1081352 | tf_op jit(solution)/shard_map/ppermute | solution.py:229
  331.7 22.2 %collective-permute-start.57 = (bf16[768,512]{1,0:T(8,128)(2,1)S(1)}, bf16[768,512]{1,0:T(8,128)(2,1)}, u32[]{:S(2)}, u32[]{:S(2)}) collective-permute-start(bf16[768,512]{1,0:T(8,128)(2,1)S(1)} %bitcast.62), channel_id=1, source_target_pairs={{0,2},{1,3},{2,0},{3,1},{4,6},{5,7},{6,4},{7,5},{8,10},{9,11},{10,... | collective-permute-start | bytes 2359304 | tf_op jit(solution)/shard_map/ppermute | solution.py:280
  335.1 32.7 %collective-permute-start.55 = (bf16[256,1408]{1,0:T(8,128)(2,1)}, bf16[256,1408]{1,0:T(8,128)(2,1)}, u32[]{:S(2)}, u32[]{:S(2)}) collective-permute-start(bf16[256,1408]{1,0:T(8,128)(2,1)} %collective-permute-done.42.refs_21_), channel_id=1, source_target_pairs={{0,8},{4,0},{8,16},{12,4},{16,24},{20,12},{24,28},{28,20},{1,9},{5... | collective-permute-start | bytes 2162696 | tf_op jit(solution)/shard_map/ppermute | solution.py:229
  336.6 32.7 %collective-permute-start.56 = (bf16[256,1408]{1,0:T(8,128)(2,1)}, bf16[256,1408]{1,0:T(8,128)(2,1)}, u32[]{:S(2)}, u32[]{:S(2)}) collective-permute-start(bf16[256,1408]{1,0:T(8,128)(2,1)} %collective-permute-done.43.refs_17_), channel_id=1, source_target_pairs={{0,4},{4,12},{8,0},{12,20},{16,8},{20,28},{24,16},{28,24},{1,5},{5... | collective-permute-start | bytes 2162696 | tf_op jit(solution)/shard_map/ppermute | solution.py:229
  355.4 28.9 %collective-permute-start.62 = (bf16[768,512]{1,0:T(8,128)(2,1)S(1)}, bf16[768,512]{1,0:T(8,128)(2,1)S(1)}, u32[]{:S(2)}, u32[]{:S(2)}) collective-permute-start(bf16[768,512]{1,0:T(8,128)(2,1)S(1)} %fusion.4.refs_3_), channel_id=1, source_target_pairs={{0,2},{1,3},{2,0},{3,1},{4,6},{5,7},{6,4},{7,5},{8,10},{9,11},{10,... | collective-permute-start | bytes 2359304 | tf_op jit(solution)/shard_map/ppermute | solution.py:280
  386.4 38.1 %collective-permute-start.66 = (bf16[704,256]{1,0:T(8,128)(2,1)}, bf16[704,256]{1,0:T(8,128)(2,1)S(1)}, u32[]{:S(2)}, u32[]{:S(2)}) collective-permute-start(bf16[704,256]{1,0:T(8,128)(2,1)} %copy-done.31), channel_id=1, source_target_pairs={{0,8},{4,0},{8,16},{12,4},{16,24},{20,12},{24,28},{28,20},{1,9},{5... | collective-permute-start | bytes 1081352 | tf_op jit(solution)/shard_map/ppermute | solution.py:229
  404.5 21.2 %collective-permute-start.64 = (bf16[704,256]{1,0:T(8,128)(2,1)}, bf16[704,256]{1,0:T(8,128)(2,1)}, u32[]{:S(2)}, u32[]{:S(2)}) collective-permute-start(bf16[704,256]{1,0:T(8,128)(2,1)} %copy-done.33), channel_id=1, source_target_pairs={{0,8},{4,0},{8,16},{12,4},{16,24},{20,12},{24,28},{28,20},{1,9},{5... | collective-permute-start | bytes 1081352 | tf_op jit(solution)/shard_map/ppermute | solution.py:229
  (80 other events, 1920.3 us)

commit v3 on v2

--- a/solution.py
+++ b/solution.py
@@ -46,20 +46,33 @@
     out, normed, left, right, sems = refs[blocks + sides * rows :]
     depth = shards[0][0].shape[0]
     width = left.shape[1]
-    copies = []
-    for which, whole in enumerate((left, right)):
-        source = shards[which % sides]
-        for slot in range(rows):
-            at = pl.multiple_of(spots[slot] * depth, depth)
-            copies.append(
-                pltpu.make_async_copy(
-                    source[slot].at[:, pl.ds(lanes[which], width)],
-                    whole.at[pl.ds(at, depth), :],
-                    sems.at[which, slot],
+    tile = 256
+    whole_tiles = width // tile
+    cut = (whole_tiles + 1) // 2 * tile
+
+    def copies_of(chunk, low, length):
+        copies = []
+        for which, whole in enumerate((left, right)):
+            source = shards[which % sides]
+            for slot in range(rows):
+                at = pl.multiple_of(spots[slot] * depth, depth)
+                copies.append(
+                    pltpu.make_async_copy(
+                        source[slot].at[:, pl.ds(lanes[which] + low, length)],
+                        whole.at[pl.ds(at, depth), pl.ds(low, length)],
+                        sems.at[chunk, which, slot],
+                    )
                 )
-            )
-    for copy in copies:
-        copy.start()
+        return copies
+
+    chunks = [
+        copies_of(chunk, low, length)
+        for chunk, (low, length) in enumerate([(0, cut), (cut, width - cut)])
+        if length
+    ]
+    for copies in chunks:
+        for copy in copies:
+            copy.start()
 
     count, size = tokens[0].shape
     step = 64 if count % 64 == 0 else count
@@ -74,19 +87,17 @@
             scaled = part * scale * gain[turn[place_at]]
             normed[here, place_at * size : (place_at + 1) * size] = scaled.astype(jnp.bfloat16)
 
-    for copy in copies:
-        copy.wait()
-
     def product(whole, here):
         return jnp.dot(normed[...], whole[:, here], preferred_element_type=jnp.float32)
 
-    tile = 256
-    whole_tiles = width // tile
-
-    @pl.loop(0, whole_tiles)
-    def _(index):
-        here = pl.ds(pl.multiple_of(index * tile, tile), tile)
-        out[:, here] = act(product(left, here), product(right, here)).astype(out.dtype)
+    for chunk, copies in enumerate(chunks):
+        for copy in copies:
+            copy.wait()
+
+        @pl.loop(*((0, cut // tile) if chunk == 0 else (cut // tile, whole_tiles)))
+        def _(index):
+            here = pl.ds(pl.multiple_of(index * tile, tile), tile)
+            out[:, here] = act(product(left, here), product(right, here)).astype(out.dtype)
 
     rest = width - whole_tiles * tile
     if rest:
@@ -99,42 +110,64 @@
             out[:, here] = act(product(left, here), product(right, here)).astype(out.dtype)
 
 
-def terms_kernel(slots, parts, low, cores, far, whose, where, inside, hidden, *refs):
-    shards = refs[: slots * parts]
-    outs = refs[slots * parts : slots * parts + cores]
-    columns, sems = refs[slots * parts + cores :]
-    depth, width = shards[0].shape[0], columns.shape[2]
+ALL, EARLY, LAST = range(3)
+
+
+def terms_kernel(slots, parts, low, cores, far, when, whose, where, inside, hidden, *refs):
+    last = slots // 2
+    used = [slot for slot in range(slots) if when == ALL or (slot == last) == (when == LAST)]
+    shards = refs[: len(used) * parts]
+    outs = refs[len(used) * parts : len(used) * parts + cores]
+    columns, sems = refs[len(used) * parts + cores :]
+    width = columns.shape[2]
+    depths = [shards[part * len(used)].shape[0] for part in range(parts)]
+    spans = [(sum(depths[:part]), depths[part]) for part in range(parts)]
 
     def wanted(slot):
         return where[slot] > 0 if far else where[slot] == 0
 
-    for slot in range(slots):
+    def put(slot, value):
+        first = 0 if when == LAST else pl.multiple_of(inside[slot] * width, width)
+        to = where[slot] - 1 if far else 0
+        for core in range(cores):
+
+            @pl.when(whose[slot] == core)
+            def _(core=core):
+                outs[core][to, :, pl.ds(first, width)] = value
+
+    for number, slot in enumerate(used):
 
         @pl.when(wanted(slot))
-        def _(slot=slot):
+        def _(number=number, slot=slot):
             for part in range(parts):
                 pltpu.make_async_copy(
-                    shards[part * slots + slot].at[:, pl.ds(low, width)],
-                    columns.at[slot, pl.ds(part * depth, depth), :],
+                    shards[part * len(used) + number].at[:, pl.ds(low, width)],
+                    columns.at[slot, pl.ds(*spans[part]), :],
                     sems.at[part, slot],
                 ).start()
 
+    def product(slot):
+        for part in range(parts):
+            landing = columns.at[slot, pl.ds(*spans[part]), :]
+            pltpu.make_async_copy(landing, landing, sems.at[part, slot]).wait()
+        value = jnp.dot(hidden[...], columns[slot], preferred_element_type=jnp.float32)
+        put(slot, value.astype(jnp.bfloat16))
+
+    if when == LAST:
+        for out in outs:
+            out[...] = jnp.zeros_like(out)
+        pl.when(wanted(last))(lambda: product(last))
+        return
+    if when == EARLY:
+        empty = jnp.zeros((hidden.shape[0], width), jnp.bfloat16)
+        pl.when(wanted(last))(lambda: put(last, empty))
+
     @pl.loop(0, slots)
     def _(slot):
-        @pl.when(wanted(slot))
-        def _():
-            for part in range(parts):
-                landing = columns.at[slot, pl.ds(part * depth, depth), :]
-                pltpu.make_async_copy(landing, landing, sems.at[part, slot]).wait()
-            value = jnp.dot(hidden[...], columns[slot], preferred_element_type=jnp.float32)
-            value = value.astype(jnp.bfloat16)
-            here = pl.ds(pl.multiple_of(inside[slot] * width, width), width)
-            to = where[slot] - 1 if far else 0
-            for core in range(cores):
-
-                @pl.when(whose[slot] == core)
-                def _(core=core):
-                    outs[core][to, :, here] = value
+        here = wanted(slot)
+        if when == EARLY:
+            here = jnp.logical_and(here, slot != last)
+        pl.when(here)(lambda: product(slot))
 
 
 def silu_times(gate, up):
@@ -194,6 +227,9 @@
                 self.behind = shard
                 self.shards[self.step] = shard
 
+    def nearly(self):
+        return len(self.shards) >= self.ring.count - 1
+
     def listed(self):
         return [self.shards[offset] for offset in range(self.ring.count)]
 
@@ -238,6 +274,11 @@
 
     def until(self, items, value):
         while not all(item.complete() for item in items):
+            value = self.turn(value)
+        return value
+
+    def until_nearly(self, items, value):
+        while not all(item.nearly() for item in items):
             value = self.turn(value)
         return value
 
@@ -328,10 +369,14 @@
         return [self.across_chip(sums[shift - 1], shift) for shift in range(1, self.chips)]
 
 
-def add_up(current, own, landed, factor):
-    total = own[0]
-    for part in landed:
-        total = total + part.astype(jnp.float32)
+def add_up(current, sums, factor):
+    totals = []
+    for own, landed in sums:
+        total = own[0]
+        for part in landed:
+            total = total + part.astype(jnp.float32)
+        totals.append(total)
+    total = jnp.concatenate(totals, axis=0) if len(totals) > 1 else totals[0]
     return (current.astype(jnp.float32) + factor * total).astype(jnp.bfloat16)
 
 
@@ -364,7 +409,12 @@
         half = ffn_two_down.shape[0] // 2
         one_gate = Gathered(ring, ffn_one_gate, True)
         one_up = Gathered(ring, ffn_one_up, False)
-        one_down = Gathered(ring, ffn_one_down, True)
+        cut = conv_value.size + conv_gate.size + conv_out.size + ffn_one_down.size
+        cut = cut // (2 * ffn_one_down.shape[1]) // 16 * 16
+        one_down = [
+            Gathered(ring, ffn_one_down[:cut], True),
+            Gathered(ring, ffn_one_down[cut:], False),
+        ]
         if conv_value.shape[0] == conv_out.shape[0]:
             mixed = jnp.concatenate([conv_value, conv_gate, conv_out], axis=1)
             mix_in = mix_out = Gathered(ring, mixed, False)
@@ -382,7 +432,7 @@
         groups = {
             GATE_ONE: [one_gate],
             UP_ONE: [one_up],
-            DOWN_ONE: [one_down],
+            DOWN_ONE: one_down,
             MIX: mixes,
             GATE_TWO: [two_gate],
             UP_TWO: [two_up],
@@ -399,7 +449,8 @@
         vmem, smem, hbm = pltpu.VMEM, pltpu.SMEM, pltpu.HBM
 
         def hidden_of(parts, gain_vec, sides, lanes, width, act, dtype):
-            length, size = parts[0].shape
+            size = parts[0].shape[1]
+            length = parts[0].shape[0]
             rows = count * size
             arrays = [shard for side in sides for shard in side.listed()]
             return pl.pallas_call(
@@ -407,13 +458,16 @@
                     count, ring.count, len(sides), lanes, act, *refs
                 ),
                 out_shape=jax.ShapeDtypeStruct((length, width), dtype),
-                in_specs=[spec(smem)] * 2 + [spec(vmem)] * (1 + count) + [spec(hbm)] * len(arrays),
+                in_specs=[spec(smem)] * 2
+                + [spec(vmem)]
+                + [spec(vmem)] * count
+                + [spec(hbm)] * len(arrays),
                 out_specs=spec(vmem),
                 scratch_shapes=[
                     pltpu.VMEM((length, rows), jnp.bfloat16),
                     pltpu.VMEM((rows, width), jnp.bfloat16),
                     pltpu.VMEM((rows, width), jnp.bfloat16),
-                    pltpu.SemaphoreType.DMA((2, ring.count)),
+                    pltpu.SemaphoreType.DMA((2, 2, ring.count)),
                 ],
                 cost_estimate=pl.CostEstimate(
                     flops=4 * length * rows * width,
@@ -423,13 +477,22 @@
                 name="hidden",
             )(spots, blocks, gain_vec.reshape(count, 1, size), *parts, *arrays)
 
-        def terms_of(hidden, sides, low, width, far):
+        def terms_of(hidden, sides, low, width, far, when=ALL):
             length, depth_all = hidden.shape
-            arrays = [shard for side in sides for shard in side.listed()]
+            last = ring.count // 2
+            arrays = [
+                side.shards[slot]
+                for side in sides
+                for slot in range(ring.count)
+                if when == ALL or (slot == last) == (when == LAST)
+            ]
             chips = features.chips - 1 if far else 1
-            out = jax.ShapeDtypeStruct((chips, length, each * width), jnp.bfloat16)
+            wide_out = width if when == LAST else each * width
+            out = jax.ShapeDtypeStruct((chips, length, wide_out), jnp.bfloat16)
             return pl.pallas_call(
-                lambda *refs: terms_kernel(ring.count, len(sides), low, cores, far, *refs),
+                lambda *refs: terms_kernel(
+                    ring.count, len(sides), low, cores, far, when, *refs
+                ),
                 out_shape=[out] * cores,
                 in_specs=[spec(smem)] * 3 + [spec(vmem)] + [spec(hbm)] * len(arrays),
                 out_specs=[spec(vmem)] * cores,
@@ -445,15 +508,32 @@
                 name="far_terms" if far else "near_terms",
             )(*targets, hidden, *arrays)
 
-        def scatter(hidden, sides, low, width, turns):
-            landed = []
+        def far_in_two(hidden, sides, low, width):
+            hidden = pump.until_nearly(sides, hidden)
+            early = features.over_cores(terms_of(hidden, sides, low, width, True, EARLY))
+            hidden, early = pump.until(sides, (hidden, early))
+            late = features.over_cores(terms_of(hidden, sides, low, width, True, LAST))
+            spot = targets[2][ring.count // 2]
+            spread = [jnp.where(spot == place_at, late, 0.0) for place_at in range(each)]
+            return hidden, early + jnp.concatenate(spread, axis=-1)
+
+        def scatter(hiddens, sides, low, width, turns, waits=False):
+            landed = [[] for _ in hiddens]
+            hiddens = list(hiddens)
             if features.chips > 1:
-                sums = features.over_cores(terms_of(hidden, sides, low, width, True))
-                hidden, sums = tie(hidden, sums)
-                landed = features.over_chips(sums)
-            terms = terms_of(hidden, sides, low, width, False)
-            own = features.over_cores(terms)
-            return pump.turn(own, turns), landed
+                for number in reversed(range(len(hiddens))):
+                    if waits:
+                        hiddens[number], sums = far_in_two(hiddens[number], sides, low, width)
+                    else:
+                        terms = terms_of(hiddens[number], sides, low, width, True)
+                        sums = features.over_cores(terms)
+                    hiddens, sums = tie(hiddens, sums.astype(jnp.bfloat16))
+                    landed[number] = features.over_chips(sums)
+            owns = []
+            for hidden in hiddens:
+                terms = terms_of(hidden, sides, low, width, False)
+                owns.append(features.over_cores(terms))
+            return list(zip(pump.turn(owns, turns), landed))
 
         tokens = pump.fill(tokens)
         far = features.gather_far(tokens)
@@ -464,9 +544,9 @@
             parts, ffn_one_gain, [one_gate, one_up], (0, 0), ffn_one_up.shape[1], silu_times,
             jnp.bfloat16,
         )
-        hidden = pump.until([one_down] + mixes, hidden)
-        own, landed = scatter(hidden, [one_down], 0, ffn_one_down.shape[1], 1)
-        stream_one = add_up(tokens, own, landed, 0.5)
+        hidden = pump.until(one_down + mixes, hidden)
+        sums = scatter([hidden], one_down, 0, ffn_one_down.shape[1], 1)
+        stream_one = add_up(tokens, sums, 0.5)
 
         far = features.gather_far(stream_one)
         stream_one = pump.turn(stream_one, 2)
@@ -494,8 +574,8 @@
             (convolved - mean_val) * lax.rsqrt(varied + 1e-05) * conv_ln_gain
         ).astype(jnp.bfloat16)
         active = pump.turn(active)
-        own, landed = scatter(active, [mix_out], out_from, conv_out.shape[1], 1)
-        stream_two = add_up(stream_one, own, landed, 1.0)
+        sums = scatter([active], [mix_out], out_from, conv_out.shape[1], 1)
+        stream_two = add_up(stream_one, sums, 1.0)
 
         far = features.gather_far(stream_two)
         stream_two = pump.turn(stream_two, 3)
@@ -505,9 +585,11 @@
             parts, ffn_two_gain, [two_gate, two_up], (0, 0), ffn_two_up.shape[1], silu_times,
             jnp.bfloat16,
         )
-        hidden = pump.until(two_down, hidden)
-        own, landed = scatter(hidden, two_down, 0, ffn_two_down.shape[1], 0)
-        return jnp.where(pump.mark < 0, stream_two, add_up(stream_two, own, landed, 0.5))
+        waits = features.chips > 1 and ring.count % 2 == 0
+        if not waits:
+            hidden = pump.until(two_down, hidden)
+        sums = scatter([hidden], two_down, 0, ffn_two_down.shape[1], 0, waits)
+        return jnp.where(pump.mark < 0, stream_two, add_up(stream_two, sums, 0.5))
 
     in_specs = (
         P("fs", "tp"),

time: 477 us -> 481 us (level)
  waiting for transfers between devices: 291 us -> 280 us
  starting transfers between devices: 66.3 us -> 72.9 us
    ppermute x56 -> x63, waiting for transfers between devices: 264 us -> 255 us  [launch(): landed = [lax.ppermute(a, 'fs', way) for a, (_, way) in zip(arrays, sends)]]
    ppermute x56 -> x63, starting transfers between devices: 57.1 us -> 64.1 us  [launch(): landed = [lax.ppermute(a, 'fs', way) for a, (_, way) in zip(arrays, sends)]]
    pallas_call x6 -> x7, Pallas kernels: 38.4 us -> 42.2 us  [terms_of(): pl.pallas_call(lambda *refs: terms_kernel(ring.count, len(sides), low, co...]
  transfers between devices with their start and end apart: 74 -> 82, of which waited for: 43 -> 43; matrix products, arithmetic and copies ran while one was open for 5% -> 5% of each run, Pallas kernels for 9% -> 8%
where the time goes in v3:
time: 481 us; the launch traced here: 479 us
  waiting for transfers between devices  280 us (58%)
  Pallas kernels  82 us (17%)
  starting transfers between devices  72.9 us (15%)
  other arithmetic  19 us (4%)
  local copies, waits for them, and re-layouts  10.1 us (2%)
  matrix products  6.93 us (1%)
  blocking collectives  6.2 us (1%)
    ppermute x63, waiting for transfers between devices, launch(): landed = [lax.ppermute(a, 'fs', way) for a, (_, way) in zip(arrays, sends)]  255 us
    ppermute x63, starting transfers between devices, launch(): landed = [lax.ppermute(a, 'fs', way) for a, (_, way) in zip(arrays, sends)]  64.1 us
    pallas_call x7, Pallas kernels, terms_of(): pl.pallas_call(lambda *refs: terms_kernel(ring.count, len(sides), low, co...  42.2 us
    pallas_call x3, Pallas kernels, hidden_of(): pl.pallas_call(lambda *refs: hidden_kernel(count, ring.count, len(sides),...  39.8 us
    ppermute x6, waiting for transfers between devices, across_chip(): return lax.ppermute(value, 'tp', pairs)  17.4 us
  transfers between devices with their start and end apart: 82, of which 43 were waited for; matrix products, arithmetic and copies ran while one was open for 5% of the time, Pallas kernels for 8%

profile of v3, /device:TPU:0, one launch (start us, length us, event | category | flops | bytes accessed | tf_op | source)
XLA Modules:
  0.0 479.5 jit_solution(16252739640367563224)
XLA Ops:
  5.1 15.8 %collective-permute-done.refs_14_ = bf16[256,1408]{1,0:T(8,128)(2,1)S(1)} collective-permute-done((bf16[256,1408]{1,0:T(8,128)(2,1)}, bf16[256,1408]{1,0:T(8,128)(2,1)S(1)}, u32[]{:S(2)}, u32[]{:S(2)}) %collective-permute-start) | collective-permute-done | bytes 720928 | tf_op jit(solution)/shard_map/ppermute | solution.py:265
  25.9 15.7 %collective-permute-done.5.refs_22_ = bf16[256,1408]{1,0:T(8,128)(2,1)} collective-permute-done((bf16[256,1408]{1,0:T(8,128)(2,1)}, bf16[256,1408]{1,0:T(8,128)(2,1)}, u32[]{:S(2)}, u32[]{:S(2)}) %collective-permute-start.5) | collective-permute-done | bytes 720928 | tf_op jit(solution)/shard_map/ppermute | solution.py:265
  45.4 11.7 %collective-permute-done.3.refs_13_ = bf16[256,1408]{1,0:T(8,128)(2,1)} collective-permute-done((bf16[256,1408]{1,0:T(8,128)(2,1)S(1)}, bf16[256,1408]{1,0:T(8,128)(2,1)}, u32[]{:S(2)}, u32[]{:S(2)}) %collective-permute-start.3) | collective-permute-done | bytes 720928 | tf_op jit(solution)/shard_map/ppermute | solution.py:265
  62.8 9.8 %collective-permute-done.11.refs_21_ = bf16[256,1408]{1,0:T(8,128)(2,1)} collective-permute-done((bf16[256,1408]{1,0:T(8,128)(2,1)}, bf16[256,1408]{1,0:T(8,128)(2,1)}, u32[]{:S(2)}, u32[]{:S(2)}) %collective-permute-start.11) | collective-permute-done | bytes 720928 | tf_op jit(solution)/shard_map/ppermute | solution.py:265
  80.4 11.2 %collective-permute-done.10.refs_10_ = bf16[256,1408]{1,0:T(8,128)(2,1)} collective-permute-done((bf16[256,1408]{1,0:T(8,128)(2,1)}, bf16[256,1408]{1,0:T(8,128)(2,1)}, u32[]{:S(2)}, u32[]{:S(2)}) %collective-permute-start.10) | collective-permute-done | bytes 720928 | tf_op jit(solution)/shard_map/ppermute | solution.py:265
  93.2 10.2 %collective-permute-done.14.refs_20_ = bf16[256,1408]{1,0:T(8,128)(2,1)} collective-permute-done((bf16[256,1408]{1,0:T(8,128)(2,1)}, bf16[256,1408]{1,0:T(8,128)(2,1)}, u32[]{:S(2)}, u32[]{:S(2)}) %collective-permute-start.14) | collective-permute-done | bytes 720928 | tf_op jit(solution)/shard_map/ppermute | solution.py:265
  110.4 7.9 %collective-permute-done.13.refs_11_ = bf16[256,1408]{1,0:T(8,128)(2,1)} collective-permute-done((bf16[256,1408]{1,0:T(8,128)(2,1)}, bf16[256,1408]{1,0:T(8,128)(2,1)}, u32[]{:S(2)}, u32[]{:S(2)}) %collective-permute-start.13) | collective-permute-done | bytes 720928 | tf_op jit(solution)/shard_map/ppermute | solution.py:265
  124.0 16.5 %hidden.3.refs_3_ = bf16[768,1408]{1,0:T(8,128)(2,1)} custom-call(s32[8]{0:T(128)} %get-tuple-element.785.refs_0_, s32[4]{0:T(128)} %pad_add_fusion.refs_1_, f32[4,1,512]{2,1,0:T(1,128)} %bitcast.62, bf16[768,512]{1,0:T(8,128)(2,1)} %refs_3_, bf16[768,512]{1,0:T(8,128)(2,1)} %copy-done.27, bf16[768,512]{1,0:T(8,128)(2,1)} %copy-done.26, ...), custom_call_target="tpu_custom_call" | custom-call | flops 8858370048 | bytes 14680064 | tf_op jit(solution)/shard_map/hidden/pallas_call | solution.py:456
  146.2 19.9 %collective-permute-done.17.refs_8_.refs_5_ = bf16[256,768]{1,0:T(8,128)(2,1)S(1)} collective-permute-done((bf16[256,768]{1,0:T(8,128)(2,1)S(1)}, bf16[256,768]{1,0:T(8,128)(2,1)S(1)}, u32[]{:S(2)}, u32[]{:S(2)}) %collective-permute-start.17) | collective-permute-done | bytes 393248 | tf_op jit(solution)/shard_map/ppermute | solution.py:265
  182.1 9.0 %collective-permute-done.33.refs_17_ = bf16[320,256]{1,0:T(8,128)(2,1)} collective-permute-done((bf16[320,256]{1,0:T(8,128)(2,1)S(1)}, bf16[320,256]{1,0:T(8,128)(2,1)}, u32[]{:S(2)}, u32[]{:S(2)}) %collective-permute-start.33) | collective-permute-done | bytes 163872 | tf_op jit(solution)/shard_map/ppermute | solution.py:265
  191.5 7.6 %collective-permute-done.34.refs_15_ = bf16[320,256]{1,0:T(8,128)(2,1)} collective-permute-done((bf16[320,256]{1,0:T(8,128)(2,1)}, bf16[320,256]{1,0:T(8,128)(2,1)}, u32[]{:S(2)}, u32[]{:S(2)}) %collective-permute-start.34) | collective-permute-done | bytes 163872 | tf_op jit(solution)/shard_map/ppermute | solution.py:265
  202.7 8.5 %collective-permute-done.37.refs_16_ = bf16[320,256]{1,0:T(8,128)(2,1)} collective-permute-done((bf16[320,256]{1,0:T(8,128)(2,1)}, bf16[320,256]{1,0:T(8,128)(2,1)}, u32[]{:S(2)}, u32[]{:S(2)}) %collective-permute-start.37) | collective-permute-done | bytes 163872 | tf_op jit(solution)/shard_map/ppermute | solution.py:265
  211.3 7.5 %far_terms.4 = (bf16[1,768,512]{2,1,0:T(8,128)(2,1)}, bf16[1,768,512]{2,1,0:T(8,128)(2,1)}) custom-call(s32[8]{0:T(128)} %get-tuple-element.784.refs_0_, s32[8]{0:T(128)} %get-tuple-element.775.refs_1_, s32[8]{0:T(128)} %get-tuple-element.773.refs_2_, bf16[768,1408]{1,0:T(8,128)(2,1)} %hidden.3.refs_3_, bf16[1088,256]{1,0:T(8,128)(2,1)} %copy-done.19, ...), custom_call_target="tpu_custom_call" | custom-call | flops 2214592512 | bytes 2883584 | tf_op jit(solution)/shard_map/far_terms/pallas_call | solution.py:492
  222.7 7.4 %near_terms.3 = (bf16[1,768,512]{2,1,0:T(8,128)(2,1)}, bf16[1,768,512]{2,1,0:T(8,128)(2,1)}) custom-call(s32[8]{0:T(128)} %get-tuple-element.784.refs_0_, s32[8]{0:T(128)} %get-tuple-element.775.refs_1_, s32[8]{0:T(128)} %get-tuple-element.773.refs_2_, bf16[768,1408]{1,0:T(8,128)(2,1)} %hidden.3.refs_3_, bf16[1088,256]{1,0:T(8,128)(2,1)} %copy-done.19, ...), custom_call_target="tpu_custom_call" | custom-call | flops 2214592512 | bytes 2883584 | tf_op jit(solution)/shard_map/near_terms/pallas_call | solution.py:492
  236.1 13.8 %collective-permute-done.42.refs_14_ = bf16[256,1408]{1,0:T(8,128)(2,1)} collective-permute-done((bf16[256,1408]{1,0:T(8,128)(2,1)}, bf16[256,1408]{1,0:T(8,128)(2,1)}, u32[]{:S(2)}, u32[]{:S(2)}) %collective-permute-start.42) | collective-permute-done | bytes 720928 | tf_op jit(solution)/shard_map/ppermute | solution.py:265
  256.6 8.8 %collective-permute-done.40.refs_22_ = bf16[256,1408]{1,0:T(8,128)(2,1)} collective-permute-done((bf16[256,1408]{1,0:T(8,128)(2,1)}, bf16[256,1408]{1,0:T(8,128)(2,1)}, u32[]{:S(2)}, u32[]{:S(2)}) %collective-permute-start.40) | collective-permute-done | bytes 720928 | tf_op jit(solution)/shard_map/ppermute | solution.py:265
  267.0 5.2 %collective-permute-done.38.refs_10_.refs_11_ = bf16[704,256]{1,0:T(8,128)(2,1)S(1)} collective-permute-done((bf16[704,256]{1,0:T(8,128)(2,1)}, bf16[704,256]{1,0:T(8,128)(2,1)S(1)}, u32[]{:S(2)}, u32[]{:S(2)}) %collective-permute-start.38) | collective-permute-done | bytes 360480 | tf_op jit(solution)/shard_map/ppermute | solution.py:265
  280.4 6.9 %hidden.4 = f32[768,256]{1,0:T(8,128)} custom-call(s32[8]{0:T(128)} %get-tuple-element.785.refs_0_, s32[4]{0:T(128)} %pad_add_fusion.refs_1_, f32[4,1,512]{2,1,0:T(1,128)} %bitcast.61, bf16[768,512]{1,0:T(8,128)(2,1)} %copy-done.2, bf16[768,512]{1,0:T(8,128)(2,1)} %copy-done.15, bf16[768,512]{1,0:T(8,128)(2,1)} %copy-done.14, bf16[768,512]{1,0:T(8,128)(2,1)} %copy-done.16, ...), custom_call_target="tpu_custom_call" | custom-call | flops 1610612736 | bytes 5242880 | tf_op jit(solution)/shard_map/hidden/pallas_call | solution.py:456
  287.3 6.9 %fusion.10 = f32[1,768,256]{2,0,1:T(1,128)S(1)} fusion(f32[1,768,256]{2,1,0:T(8,128)} %bitcast.57, f32[31,1,256]{2,0,1:T(8,128)S(1)} %bitcast.54), kind=kOutput, calls=%fused_computation.20 | convolution fusion | flops 72400896 | bytes 1604608 | tf_op jit(solution)/shard_map/conv_general_dilated | solution.py:558
  295.1 13.8 %collective-permute-done.49.refs_21_ = bf16[256,1408]{1,0:T(8,128)(2,1)} collective-permute-done((bf16[256,1408]{1,0:T(8,128)(2,1)}, bf16[256,1408]{1,0:T(8,128)(2,1)}, u32[]{:S(2)}, u32[]{:S(2)}) %collective-permute-start.49) | collective-permute-done | bytes 720928 | tf_op jit(solution)/shard_map/ppermute | solution.py:265
  310.5 6.2 %all-reduce = (f32[768]{0:T(1024)S(1)}, f32[768]{0:T(1024)S(1)}) all-reduce(f32[768]{0:T(1024)S(1)} %get-tuple-element.770, f32[768]{0:T(1024)S(1)} %get-tuple-element.769), channel_id=1, replica_groups=mesh['fs'=8,'tp'=4] {'tp'}, use_global_device_ids=true, to_apply=%region_3.4 | all-reduce | flops 1536 | bytes 12288 | tf_op jit(solution)/shard_map/psum | solution.py:568
  336.7 13.8 %collective-permute-done.56.refs_12_ = bf16[256,1408]{1,0:T(8,128)(2,1)} collective-permute-done((bf16[256,1408]{1,0:T(8,128)(2,1)}, bf16[256,1408]{1,0:T(8,128)(2,1)}, u32[]{:S(2)}, u32[]{:S(2)}) %collective-permute-start.56) | collective-permute-done | bytes 720928 | tf_op jit(solution)/shard_map/ppermute | solution.py:265
  356.2 9.9 %collective-permute-done.62.refs_20_ = bf16[256,1408]{1,0:T(8,128)(2,1)} collective-permute-done((bf16[256,1408]{1,0:T(8,128)(2,1)}, bf16[256,1408]{1,0:T(8,128)(2,1)}, u32[]{:S(2)}, u32[]{:S(2)}) %collective-permute-start.62) | collective-permute-done | bytes 720928 | tf_op jit(solution)/shard_map/ppermute | solution.py:265
  368.1 5.6 %collective-permute-done.65.refs_9_.refs_10_ = bf16[704,256]{1,0:T(8,128)(2,1)S(1)} collective-permute-done((bf16[704,256]{1,0:T(8,128)(2,1)S(1)}, bf16[704,256]{1,0:T(8,128)(2,1)S(1)}, u32[]{:S(2)}, u32[]{:S(2)}) %collective-permute-start.65) | collective-permute-done | bytes 360480 | tf_op jit(solution)/shard_map/ppermute | solution.py:265
  374.1 6.4 %collective-permute-done.60.refs_16_.refs_18_ = bf16[704,256]{1,0:T(8,128)(2,1)S(1)} collective-permute-done((bf16[704,256]{1,0:T(8,128)(2,1)}, bf16[704,256]{1,0:T(8,128)(2,1)S(1)}, u32[]{:S(2)}, u32[]{:S(2)}) %collective-permute-start.60) | collective-permute-done | bytes 360480 | tf_op jit(solution)/shard_map/ppermute | solution.py:265
  384.6 16.7 %collective-permute-done.67.refs_11_ = bf16[256,1408]{1,0:T(8,128)(2,1)S(1)} collective-permute-done((bf16[256,1408]{1,0:T(8,128)(2,1)}, bf16[256,1408]{1,0:T(8,128)(2,1)S(1)}, u32[]{:S(2)}, u32[]{:S(2)}) %collective-permute-start.67) | collective-permute-done | bytes 720928 | tf_op jit(solution)/shard_map/ppermute | solution.py:265
  405.0 16.4 %hidden.5.refs_3_ = bf16[768,1408]{1,0:T(8,128)(2,1)} custom-call(s32[8]{0:T(128)} %get-tuple-element.785.refs_0_, s32[4]{0:T(128)} %pad_add_fusion.refs_1_, f32[4,1,512]{2,1,0:T(1,128)} %bitcast.63, bf16[768,512]{1,0:T(8,128)(2,1)} %copy-done.12, bf16[768,512]{1,0:T(8,128)(2,1)} %copy-done.30, bf16[768,512]{1,0:T(8,128)(2,1)} %copy-done.29, ...), custom_call_target="tpu_custom_call" | custom-call | flops 8858370048 | bytes 14680064 | tf_op jit(solution)/shard_map/hidden/pallas_call | solution.py:456
  422.2 6.5 %far_terms.6 = (bf16[1,768,512]{2,1,0:T(8,128)(2,1)}, bf16[1,768,512]{2,1,0:T(8,128)(2,1)}) custom-call(s32[8]{0:T(128)} %get-tuple-element.784.refs_0_, s32[8]{0:T(128)} %get-tuple-element.775.refs_1_, s32[8]{0:T(128)} %get-tuple-element.773.refs_2_, bf16[768,1408]{1,0:T(8,128)(2,1)} %hidden.5.refs_3_, bf16[704,256]{1,0:T(8,128)(2,1)} %get-tuple-element.574.refs_4_, ...), custom_call_target="tpu_custom_call" | custom-call | flops 2214592512 | bytes 2883584 | tf_op jit(solution)/shard_map/far_terms/pallas_call | solution.py:492
  432.7 7.2 %collective-permute-done.77.refs_4_.refs_8_ = bf16[704,256]{1,0:T(8,128)(2,1)S(1)} collective-permute-done((bf16[704,256]{1,0:T(8,128)(2,1)}, bf16[704,256]{1,0:T(8,128)(2,1)S(1)}, u32[]{:S(2)}, u32[]{:S(2)}) %collective-permute-start.77) | collective-permute-done | bytes 360480 | tf_op jit(solution)/shard_map/ppermute | solution.py:265
  441.4 4.5 far_terms.7
  449.4 7.5 %near_terms.5 = (bf16[1,768,512]{2,1,0:T(8,128)(2,1)}, bf16[1,768,512]{2,1,0:T(8,128)(2,1)}) custom-call(s32[8]{0:T(128)} %get-tuple-element.784.refs_0_, s32[8]{0:T(128)} %get-tuple-element.775.refs_1_, s32[8]{0:T(128)} %get-tuple-element.773.refs_2_, bf16[768,1408]{1,0:T(8,128)(2,1)} %hidden.5.refs_3_, bf16[704,256]{1,0:T(8,128)(2,1)} %get-tuple-element.574.refs_4_, ...), custom_call_target="tpu_custom_call" | custom-call | flops 2214592512 | bytes 2883584 | tf_op jit(solution)/shard_map/near_terms/pallas_call | solution.py:492
  459.6 17.4 %collective-permute-done.81 = bf16[768,512]{1,0:T(8,128)(2,1)S(1)} collective-permute-done((bf16[768,512]{1,0:T(8,128)(2,1)S(1)}, bf16[768,512]{1,0:T(8,128)(2,1)S(1)}, u32[]{:S(2)}, u32[]{:S(2)}) %collective-permute-start.81) | collective-permute-done | bytes 786464 | tf_op jit(solution)/shard_map/ppermute | solution.py:321
  (263 shorter events, 145.3 us)
Async XLA Ops:
  0.0 22.2 %collective-permute-start.2 = (bf16[768,512]{1,0:T(8,128)(2,1)}, bf16[768,512]{1,0:T(8,128)(2,1)S(1)}, u32[]{:S(2)}, u32[]{:S(2)}) collective-permute-start(bf16[768,512]{1,0:T(8,128)(2,1)} %refs_3_), channel_id=1, source_target_pairs={{0,2},{1,3},{2,0},{3,1},{4,6},{5,7},{6,4},{7,5},{8,10},{9,11},{10,... | collective-permute-start | bytes 2359304 | tf_op jit(solution)/shard_map/ppermute | solution.py:321
  5.1 37.3 %collective-permute-start.7 = (bf16[768,512]{1,0:T(8,128)(2,1)}, bf16[768,512]{1,0:T(8,128)(2,1)S(1)}, u32[]{:S(2)}, u32[]{:S(2)}) collective-permute-start(bf16[768,512]{1,0:T(8,128)(2,1)} %refs_3_), channel_id=1, source_target_pairs={{0,1},{1,0},{2,3},{3,2},{4,5},{5,4},{6,7},{7,6},{8,9},{9,8},{10,11... | collective-permute-start | bytes 2359304 | tf_op jit(solution)/shard_map/ppermute | solution.py:313
  24.3 32.7 %collective-permute-start.3 = (bf16[256,1408]{1,0:T(8,128)(2,1)S(1)}, bf16[256,1408]{1,0:T(8,128)(2,1)}, u32[]{:S(2)}, u32[]{:S(2)}) collective-permute-start(bf16[256,1408]{1,0:T(8,128)(2,1)S(1)} %collective-permute-done.refs_14_), channel_id=1, source_target_pairs={{0,8},{4,0},{8,16},{12,4},{16,24},{20,12},{24,28},{28,20},{1,9},{5... | collective-permute-start | bytes 2162696 | tf_op jit(solution)/shard_map/ppermute | solution.py:265
  43.4 29.2 %collective-permute-start.11 = (bf16[256,1408]{1,0:T(8,128)(2,1)}, bf16[256,1408]{1,0:T(8,128)(2,1)}, u32[]{:S(2)}, u32[]{:S(2)}) collective-permute-start(bf16[256,1408]{1,0:T(8,128)(2,1)} %collective-permute-done.5.refs_22_), channel_id=1, source_target_pairs={{0,8},{4,0},{8,16},{12,4},{16,24},{20,12},{24,28},{28,20},{1,9},{5... | collective-permute-start | bytes 2162696 | tf_op jit(solution)/shard_map/ppermute | solution.py:265
  44.9 31.3 %collective-permute-start.12 = (bf16[256,1408]{1,0:T(8,128)(2,1)}, bf16[256,1408]{1,0:T(8,128)(2,1)}, u32[]{:S(2)}, u32[]{:S(2)}) collective-permute-start(bf16[256,1408]{1,0:T(8,128)(2,1)} %collective-permute-done.6.refs_16_), channel_id=1, source_target_pairs={{0,4},{4,12},{8,0},{12,20},{16,8},{20,28},{24,16},{28,24},{1,5},{5... | collective-permute-start | bytes 2162696 | tf_op jit(solution)/shard_map/ppermute | solution.py:265
  60.7 30.9 %collective-permute-start.10 = (bf16[256,1408]{1,0:T(8,128)(2,1)}, bf16[256,1408]{1,0:T(8,128)(2,1)}, u32[]{:S(2)}, u32[]{:S(2)}) collective-permute-start(bf16[256,1408]{1,0:T(8,128)(2,1)} %collective-permute-done.4.refs_9_), channel_id=1, source_target_pairs={{0,4},{4,12},{8,0},{12,20},{16,8},{20,28},{24,16},{28,24},{1,5},{5... | collective-permute-start | bytes 2162696 | tf_op jit(solution)/shard_map/ppermute | solution.py:265
  61.2 30.4 %collective-permute-start.9 = (bf16[256,1408]{1,0:T(8,128)(2,1)}, bf16[256,1408]{1,0:T(8,128)(2,1)}, u32[]{:S(2)}, u32[]{:S(2)}) collective-permute-start(bf16[256,1408]{1,0:T(8,128)(2,1)} %collective-permute-done.3.refs_13_), channel_id=1, source_target_pairs={{0,8},{4,0},{8,16},{12,4},{16,24},{20,12},{24,28},{28,20},{1,9},{5... | collective-permute-start | bytes 2162696 | tf_op jit(solution)/shard_map/ppermute | solution.py:265
  76.2 27.2 %collective-permute-start.14 = (bf16[256,1408]{1,0:T(8,128)(2,1)}, bf16[256,1408]{1,0:T(8,128)(2,1)}, u32[]{:S(2)}, u32[]{:S(2)}) collective-permute-start(bf16[256,1408]{1,0:T(8,128)(2,1)} %collective-permute-done.11.refs_21_), channel_id=1, source_target_pairs={{0,8},{4,0},{8,16},{12,4},{16,24},{20,12},{24,28},{28,20},{1,9},{5... | collective-permute-start | bytes 2162696 | tf_op jit(solution)/shard_map/ppermute | solution.py:265
  77.8 27.4 %collective-permute-start.15 = (bf16[256,1408]{1,0:T(8,128)(2,1)}, bf16[256,1408]{1,0:T(8,128)(2,1)}, u32[]{:S(2)}, u32[]{:S(2)}) collective-permute-start(bf16[256,1408]{1,0:T(8,128)(2,1)} %collective-permute-done.12.refs_17_), channel_id=1, source_target_pairs={{0,4},{4,12},{8,0},{12,20},{16,8},{20,28},{24,16},{28,24},{1,5},{5... | collective-permute-start | bytes 2162696 | tf_op jit(solution)/shard_map/ppermute | solution.py:265
  91.6 26.7 %collective-permute-start.13 = (bf16[256,1408]{1,0:T(8,128)(2,1)}, bf16[256,1408]{1,0:T(8,128)(2,1)}, u32[]{:S(2)}, u32[]{:S(2)}) collective-permute-start(bf16[256,1408]{1,0:T(8,128)(2,1)} %collective-permute-done.9.refs_12_), channel_id=1, source_target_pairs={{0,8},{4,0},{8,16},{12,4},{16,24},{20,12},{24,28},{28,20},{1,9},{5... | collective-permute-start | bytes 2162696 | tf_op jit(solution)/shard_map/ppermute | solution.py:265
  118.4 22.2 %collective-permute-start.18 = (bf16[1088,256]{1,0:T(8,128)(2,1)S(1)}, bf16[1088,256]{1,0:T(8,128)(2,1)}, u32[]{:S(2)}, u32[]{:S(2)}) collective-permute-start(bf16[1088,256]{1,0:T(8,128)(2,1)S(1)} %slice.17.refs_4_), channel_id=1, source_target_pairs={{0,8},{4,0},{8,16},{12,4},{16,24},{20,12},{24,28},{28,20},{1,9},{5... | collective-permute-start | bytes 1671176 | tf_op jit(solution)/shard_map/ppermute | solution.py:265
  122.4 23.4 %collective-permute-start.16 = (bf16[256,768]{1,0:T(8,128)(2,1)S(1)}, bf16[256,768]{1,0:T(8,128)(2,1)S(1)}, u32[]{:S(2)}, u32[]{:S(2)}) collective-permute-start(bf16[256,768]{1,0:T(8,128)(2,1)S(1)} %constant_dynamic-update-slice_fusion.refs_7_.refs_4_), channel_id=1, source_target_pairs={{0,8},{4,0},{8,16},{12,4},{16,24},{20,12},{24,28},{28,20},{1,9},{5... | collective-permute-start | bytes 1179656 | tf_op jit(solution)/shard_map/ppermute | solution.py:265
  140.5 29.2 %collective-permute-start.25 = (bf16[1088,256]{1,0:T(8,128)(2,1)}, bf16[1088,256]{1,0:T(8,128)(2,1)}, u32[]{:S(2)}, u32[]{:S(2)}) collective-permute-start(bf16[1088,256]{1,0:T(8,128)(2,1)} %collective-permute-done.18.refs_11_), channel_id=1, source_target_pairs={{0,8},{4,0},{8,16},{12,4},{16,24},{20,12},{24,28},{28,20},{1,9},{5... | collective-permute-start | bytes 1671176 | tf_op jit(solution)/shard_map/ppermute | solution.py:265
  142.2 27.5 %collective-permute-start.26 = (bf16[1088,256]{1,0:T(8,128)(2,1)}, bf16[1088,256]{1,0:T(8,128)(2,1)}, u32[]{:S(2)}, u32[]{:S(2)}) collective-permute-start(bf16[1088,256]{1,0:T(8,128)(2,1)} %collective-permute-done.19.refs_5_), channel_id=1, source_target_pairs={{0,4},{4,12},{8,0},{12,20},{16,8},{20,28},{24,16},{28,24},{1,5},{5... | collective-permute-start | bytes 1671176 | tf_op jit(solution)/shard_map/ppermute | solution.py:265
  142.6 23.6 %collective-permute-start.17 = (bf16[256,768]{1,0:T(8,128)(2,1)S(1)}, bf16[256,768]{1,0:T(8,128)(2,1)S(1)}, u32[]{:S(2)}, u32[]{:S(2)}) collective-permute-start(bf16[256,768]{1,0:T(8,128)(2,1)S(1)} %constant_dynamic-update-slice_fusion.refs_7_.refs_4_), channel_id=1, source_target_pairs={{0,4},{4,12},{8,0},{12,20},{16,8},{20,28},{24,16},{28,24},{1,5},{5... | collective-permute-start | bytes 1179656 | tf_op jit(solution)/shard_map/ppermute | solution.py:265
  143.1 25.0 %collective-permute-start.27 = (bf16[320,256]{1,0:T(8,128)(2,1)S(1)}, bf16[320,256]{1,0:T(8,128)(2,1)S(1)}, u32[]{:S(2)}, u32[]{:S(2)}) collective-permute-start(bf16[320,256]{1,0:T(8,128)(2,1)S(1)} %collective-permute-done.20.refs_19_), channel_id=1, source_target_pairs={{0,8},{4,0},{8,16},{12,4},{16,24},{20,12},{24,28},{28,20},{1,9},{5... | collective-permute-start | bytes 491528 | tf_op jit(solution)/shard_map/ppermute | solution.py:265
  145.8 23.9 %collective-permute-start.28 = (bf16[320,256]{1,0:T(8,128)(2,1)S(1)}, bf16[320,256]{1,0:T(8,128)(2,1)S(1)}, u32[]{:S(2)}, u32[]{:S(2)}) collective-permute-start(bf16[320,256]{1,0:T(8,128)(2,1)S(1)} %collective-permute-done.21.refs_13_), channel_id=1, source_target_pairs={{0,4},{4,12},{8,0},{12,20},{16,8},{20,28},{24,16},{28,24},{1,5},{5... | collective-permute-start | bytes 491528 | tf_op jit(solution)/shard_map/ppermute | solution.py:265
  169.7 29.5 %collective-permute-start.31 = (bf16[1088,256]{1,0:T(8,128)(2,1)}, bf16[1088,256]{1,0:T(8,128)(2,1)}, u32[]{:S(2)}, u32[]{:S(2)}) collective-permute-start(bf16[1088,256]{1,0:T(8,128)(2,1)} %collective-permute-done.25.refs_10_), channel_id=1, source_target_pairs={{0,8},{4,0},{8,16},{12,4},{16,24},{20,12},{24,28},{28,20},{1,9},{5... | collective-permute-start | bytes 1671176 | tf_op jit(solution)/shard_map/ppermute | solution.py:265
  171.7 27.5 %collective-permute-start.32 = (bf16[1088,256]{1,0:T(8,128)(2,1)}, bf16[1088,256]{1,0:T(8,128)(2,1)}, u32[]{:S(2)}, u32[]{:S(2)}) collective-permute-start(bf16[1088,256]{1,0:T(8,128)(2,1)} %collective-permute-done.26.refs_6_), channel_id=1, source_target_pairs={{0,4},{4,12},{8,0},{12,20},{16,8},{20,28},{24,16},{28,24},{1,5},{5... | collective-permute-start | bytes 1671176 | tf_op jit(solution)/shard_map/ppermute | solution.py:265
  180.1 21.4 %collective-permute-start.29 = (bf16[256,768]{1,0:T(8,128)(2,1)S(1)}, bf16[256,768]{1,0:T(8,128)(2,1)S(1)}, u32[]{:S(2)}, u32[]{:S(2)}) collective-permute-start(bf16[256,768]{1,0:T(8,128)(2,1)S(1)} %collective-permute-done.23.refs_13_.refs_10_), channel_id=1, source_target_pairs={{0,8},{4,0},{8,16},{12,4},{16,24},{20,12},{24,28},{28,20},{1,9},{5... | collective-permute-start | bytes 1179656 | tf_op jit(solution)/shard_map/ppermute | solution.py:265
  230.3 21.2 %collective-permute-start.46 = (bf16[768,512]{1,0:T(8,128)(2,1)S(1)}, bf16[768,512]{1,0:T(8,128)(2,1)}, u32[]{:S(2)}, u32[]{:S(2)}) collective-permute-start(bf16[768,512]{1,0:T(8,128)(2,1)S(1)} %bitcast.58), channel_id=1, source_target_pairs={{0,2},{1,3},{2,0},{3,1},{4,6},{5,7},{6,4},{7,5},{8,10},{9,11},{10,... | collective-permute-start | bytes 2359304 | tf_op jit(solution)/shard_map/ppermute | solution.py:321
  232.7 32.7 %collective-permute-start.40 = (bf16[256,1408]{1,0:T(8,128)(2,1)}, bf16[256,1408]{1,0:T(8,128)(2,1)}, u32[]{:S(2)}, u32[]{:S(2)}) collective-permute-start(bf16[256,1408]{1,0:T(8,128)(2,1)} %refs_15_.3), channel_id=1, source_target_pairs={{0,8},{4,0},{8,16},{12,4},{16,24},{20,12},{24,28},{28,20},{1,9},{5... | collective-permute-start | bytes 2162696 | tf_op jit(solution)/shard_map/ppermute | solution.py:265
  234.2 32.7 %collective-permute-start.41 = (bf16[256,1408]{1,0:T(8,128)(2,1)}, bf16[256,1408]{1,0:T(8,128)(2,1)}, u32[]{:S(2)}, u32[]{:S(2)}) collective-permute-start(bf16[256,1408]{1,0:T(8,128)(2,1)} %refs_15_.3), channel_id=1, source_target_pairs={{0,4},{4,12},{8,0},{12,20},{16,8},{20,28},{24,16},{28,24},{1,5},{5... | collective-permute-start | bytes 2162696 | tf_op jit(solution)/shard_map/ppermute | solution.py:265
  276.1 32.7 %collective-permute-start.49 = (bf16[256,1408]{1,0:T(8,128)(2,1)}, bf16[256,1408]{1,0:T(8,128)(2,1)}, u32[]{:S(2)}, u32[]{:S(2)}) collective-permute-start(bf16[256,1408]{1,0:T(8,128)(2,1)} %collective-permute-done.40.refs_22_), channel_id=1, source_target_pairs={{0,8},{4,0},{8,16},{12,4},{16,24},{20,12},{24,28},{28,20},{1,9},{5... | collective-permute-start | bytes 2162696 | tf_op jit(solution)/shard_map/ppermute | solution.py:265
  277.5 32.7 %collective-permute-start.50 = (bf16[256,1408]{1,0:T(8,128)(2,1)}, bf16[256,1408]{1,0:T(8,128)(2,1)}, u32[]{:S(2)}, u32[]{:S(2)}) collective-permute-start(bf16[256,1408]{1,0:T(8,128)(2,1)} %collective-permute-done.41.refs_16_), channel_id=1, source_target_pairs={{0,4},{4,12},{8,0},{12,20},{16,8},{20,28},{24,16},{28,24},{1,5},{5... | collective-permute-start | bytes 2162696 | tf_op jit(solution)/shard_map/ppermute | solution.py:265
  279.0 38.8 %collective-permute-start.47 = (bf16[704,256]{1,0:T(8,128)(2,1)S(1)}, bf16[704,256]{1,0:T(8,128)(2,1)}, u32[]{:S(2)}, u32[]{:S(2)}) collective-permute-start(bf16[704,256]{1,0:T(8,128)(2,1)S(1)} %copy-done.20), channel_id=1, source_target_pairs={{0,8},{4,0},{8,16},{12,4},{16,24},{20,12},{24,28},{28,20},{1,9},{5... | collective-permute-start | bytes 1081352 | tf_op jit(solution)/shard_map/ppermute | solution.py:265
  294.4 23.4 %collective-permute-start.48 = (bf16[704,256]{1,0:T(8,128)(2,1)S(1)}, bf16[704,256]{1,0:T(8,128)(2,1)}, u32[]{:S(2)}, u32[]{:S(2)}) collective-permute-start(bf16[704,256]{1,0:T(8,128)(2,1)S(1)} %copy-done.20), channel_id=1, source_target_pairs={{0,4},{4,12},{8,0},{12,20},{16,8},{20,28},{24,16},{28,24},{1,5},{5... | collective-permute-start | bytes 1081352 | tf_op jit(solution)/shard_map/ppermute | solution.py:265
  333.3 32.7 %collective-permute-start.62 = (bf16[256,1408]{1,0:T(8,128)(2,1)}, bf16[256,1408]{1,0:T(8,128)(2,1)}, u32[]{:S(2)}, u32[]{:S(2)}) collective-permute-start(bf16[256,1408]{1,0:T(8,128)(2,1)} %collective-permute-done.49.refs_21_), channel_id=1, source_target_pairs={{0,8},{4,0},{8,16},{12,4},{16,24},{20,12},{24,28},{28,20},{1,9},{5... | collective-permute-start | bytes 2162696 | tf_op jit(solution)/shard_map/ppermute | solution.py:265
  333.7 32.7 %collective-permute-start.63 = (bf16[256,1408]{1,0:T(8,128)(2,1)}, bf16[256,1408]{1,0:T(8,128)(2,1)}, u32[]{:S(2)}, u32[]{:S(2)}) collective-permute-start(bf16[256,1408]{1,0:T(8,128)(2,1)} %collective-permute-done.50.refs_17_), channel_id=1, source_target_pairs={{0,4},{4,12},{8,0},{12,20},{16,8},{20,28},{24,16},{28,24},{1,5},{5... | collective-permute-start | bytes 2162696 | tf_op jit(solution)/shard_map/ppermute | solution.py:265
  352.5 29.5 %collective-permute-start.69 = (bf16[768,512]{1,0:T(8,128)(2,1)S(1)}, bf16[768,512]{1,0:T(8,128)(2,1)S(1)}, u32[]{:S(2)}, u32[]{:S(2)}) collective-permute-start(bf16[768,512]{1,0:T(8,128)(2,1)S(1)} %fusion.5.refs_3_), channel_id=1, source_target_pairs={{0,2},{1,3},{2,0},{3,1},{4,6},{5,7},{6,4},{7,5},{8,10},{9,11},{10,... | collective-permute-start | bytes 2359304 | tf_op jit(solution)/shard_map/ppermute | solution.py:321
  381.3 21.6 %collective-permute-start.68 = (bf16[768,512]{1,0:T(8,128)(2,1)S(1)}, bf16[768,512]{1,0:T(8,128)(2,1)S(1)}, u32[]{:S(2)}, u32[]{:S(2)}) collective-permute-start(bf16[768,512]{1,0:T(8,128)(2,1)S(1)} %fusion.5.refs_3_), channel_id=1, source_target_pairs={{0,1},{1,0},{2,3},{3,2},{4,5},{5,4},{6,7},{7,6},{8,9},{9,8},{10,11... | collective-permute-start | bytes 2359304 | tf_op jit(solution)/shard_map/ppermute | solution.py:313
  384.1 37.3 %collective-permute-start.73 = (bf16[704,256]{1,0:T(8,128)(2,1)}, bf16[704,256]{1,0:T(8,128)(2,1)S(1)}, u32[]{:S(2)}, u32[]{:S(2)}) collective-permute-start(bf16[704,256]{1,0:T(8,128)(2,1)} %copy-done.36), channel_id=1, source_target_pairs={{0,8},{4,0},{8,16},{12,4},{16,24},{20,12},{24,28},{28,20},{1,9},{5... | collective-permute-start | bytes 1081352 | tf_op jit(solution)/shard_map/ppermute | solution.py:265
  (97 other events, 2456.2 us)

commit v4 on v3

--- a/solution.py
+++ b/solution.py
@@ -510,9 +510,11 @@
 
         def far_in_two(hidden, sides, low, width):
             hidden = pump.until_nearly(sides, hidden)
-            early = features.over_cores(terms_of(hidden, sides, low, width, True, EARLY))
+            early = terms_of(hidden, sides, low, width, True, EARLY)
             hidden, early = pump.until(sides, (hidden, early))
-            late = features.over_cores(terms_of(hidden, sides, low, width, True, LAST))
+            early = features.over_cores(early)
+            late = terms_of(hidden, sides, low, width, True, LAST)
+            late = features.over_cores(late)
             spot = targets[2][ring.count // 2]
             spread = [jnp.where(spot == place_at, late, 0.0) for place_at in range(each)]
             return hidden, early + jnp.concatenate(spread, axis=-1)

time: 481 us -> 471 us (0.979)
  waiting for transfers between devices: 280 us -> 273 us
    ppermute x63, waiting for transfers between devices: 255 us -> 249 us  [launch(): landed = [lax.ppermute(a, 'fs', way) for a, (_, way) in zip(arrays, sends)]]
  transfers between devices with their start and end apart: 82 -> 82, of which waited for: 43 -> 42; matrix products, arithmetic and copies ran while one was open for 5% -> 5% of each run, Pallas kernels for 8% -> 11%
where the time goes in v4:
time: 471 us; the launch traced here: 469 us
  waiting for transfers between devices  273 us (58%)
  Pallas kernels  82 us (17%)
  starting transfers between devices  72.9 us (15%)
  other arithmetic  17.5 us (4%)
  local copies, waits for them, and re-layouts  8.82 us (2%)
  matrix products  6.93 us (1%)
  blocking collectives  6.2 us (1%)
    ppermute x63, waiting for transfers between devices, launch(): landed = [lax.ppermute(a, 'fs', way) for a, (_, way) in zip(arrays, sends)]  249 us
    ppermute x63, starting transfers between devices, launch(): landed = [lax.ppermute(a, 'fs', way) for a, (_, way) in zip(arrays, sends)]  64.2 us
    pallas_call x7, Pallas kernels, terms_of(): pl.pallas_call(lambda *refs: terms_kernel(ring.count, len(sides), low, co...  42.2 us
    pallas_call x3, Pallas kernels, hidden_of(): pl.pallas_call(lambda *refs: hidden_kernel(count, ring.count, len(sides),...  39.8 us
    ppermute x6, waiting for transfers between devices, across_chip(): return lax.ppermute(value, 'tp', pairs)  17.4 us
  transfers between devices with their start and end apart: 82, of which 42 were waited for; matrix products, arithmetic and copies ran while one was open for 5% of the time, Pallas kernels for 11%

profile of v4, /device:TPU:0, one launch (start us, length us, event | category | flops | bytes accessed | tf_op | source)
XLA Modules:
  0.0 469.4 jit_solution(695002573828527502)
XLA Ops:
  5.1 15.8 %collective-permute-done.refs_14_ = bf16[256,1408]{1,0:T(8,128)(2,1)S(1)} collective-permute-done((bf16[256,1408]{1,0:T(8,128)(2,1)}, bf16[256,1408]{1,0:T(8,128)(2,1)S(1)}, u32[]{:S(2)}, u32[]{:S(2)}) %collective-permute-start) | collective-permute-done | bytes 720928 | tf_op jit(solution)/shard_map/ppermute | solution.py:265
  25.9 15.7 %collective-permute-done.5.refs_22_ = bf16[256,1408]{1,0:T(8,128)(2,1)} collective-permute-done((bf16[256,1408]{1,0:T(8,128)(2,1)}, bf16[256,1408]{1,0:T(8,128)(2,1)}, u32[]{:S(2)}, u32[]{:S(2)}) %collective-permute-start.5) | collective-permute-done | bytes 720928 | tf_op jit(solution)/shard_map/ppermute | solution.py:265
  45.4 11.7 %collective-permute-done.3.refs_13_ = bf16[256,1408]{1,0:T(8,128)(2,1)} collective-permute-done((bf16[256,1408]{1,0:T(8,128)(2,1)S(1)}, bf16[256,1408]{1,0:T(8,128)(2,1)}, u32[]{:S(2)}, u32[]{:S(2)}) %collective-permute-start.3) | collective-permute-done | bytes 720928 | tf_op jit(solution)/shard_map/ppermute | solution.py:265
  62.8 9.8 %collective-permute-done.11.refs_21_ = bf16[256,1408]{1,0:T(8,128)(2,1)} collective-permute-done((bf16[256,1408]{1,0:T(8,128)(2,1)}, bf16[256,1408]{1,0:T(8,128)(2,1)}, u32[]{:S(2)}, u32[]{:S(2)}) %collective-permute-start.11) | collective-permute-done | bytes 720928 | tf_op jit(solution)/shard_map/ppermute | solution.py:265
  80.4 11.3 %collective-permute-done.10.refs_10_ = bf16[256,1408]{1,0:T(8,128)(2,1)} collective-permute-done((bf16[256,1408]{1,0:T(8,128)(2,1)}, bf16[256,1408]{1,0:T(8,128)(2,1)}, u32[]{:S(2)}, u32[]{:S(2)}) %collective-permute-start.10) | collective-permute-done | bytes 720928 | tf_op jit(solution)/shard_map/ppermute | solution.py:265
  93.2 10.2 %collective-permute-done.14.refs_20_ = bf16[256,1408]{1,0:T(8,128)(2,1)} collective-permute-done((bf16[256,1408]{1,0:T(8,128)(2,1)}, bf16[256,1408]{1,0:T(8,128)(2,1)}, u32[]{:S(2)}, u32[]{:S(2)}) %collective-permute-start.14) | collective-permute-done | bytes 720928 | tf_op jit(solution)/shard_map/ppermute | solution.py:265
  110.4 8.0 %collective-permute-done.13.refs_11_ = bf16[256,1408]{1,0:T(8,128)(2,1)} collective-permute-done((bf16[256,1408]{1,0:T(8,128)(2,1)}, bf16[256,1408]{1,0:T(8,128)(2,1)}, u32[]{:S(2)}, u32[]{:S(2)}) %collective-permute-start.13) | collective-permute-done | bytes 720928 | tf_op jit(solution)/shard_map/ppermute | solution.py:265
  124.0 16.4 %hidden.3.refs_3_ = bf16[768,1408]{1,0:T(8,128)(2,1)} custom-call(s32[8]{0:T(128)} %get-tuple-element.791.refs_0_, s32[4]{0:T(128)} %pad_add_fusion.refs_1_, f32[4,1,512]{2,1,0:T(1,128)} %bitcast.62, bf16[768,512]{1,0:T(8,128)(2,1)} %refs_3_, bf16[768,512]{1,0:T(8,128)(2,1)} %copy-done.28, bf16[768,512]{1,0:T(8,128)(2,1)} %copy-done.27, ...), custom_call_target="tpu_custom_call" | custom-call | flops 8858370048 | bytes 14680064 | tf_op jit(solution)/shard_map/hidden/pallas_call | solution.py:456
  146.2 19.9 %collective-permute-done.17.refs_8_.refs_5_ = bf16[256,768]{1,0:T(8,128)(2,1)S(1)} collective-permute-done((bf16[256,768]{1,0:T(8,128)(2,1)S(1)}, bf16[256,768]{1,0:T(8,128)(2,1)S(1)}, u32[]{:S(2)}, u32[]{:S(2)}) %collective-permute-start.17) | collective-permute-done | bytes 393248 | tf_op jit(solution)/shard_map/ppermute | solution.py:265
  173.7 4.5 collective-permute-done.23.refs_13_.refs_10_
  182.1 9.0 %collective-permute-done.33.refs_17_ = bf16[320,256]{1,0:T(8,128)(2,1)} collective-permute-done((bf16[320,256]{1,0:T(8,128)(2,1)S(1)}, bf16[320,256]{1,0:T(8,128)(2,1)}, u32[]{:S(2)}, u32[]{:S(2)}) %collective-permute-start.33) | collective-permute-done | bytes 163872 | tf_op jit(solution)/shard_map/ppermute | solution.py:265
  191.5 7.6 %collective-permute-done.34.refs_15_ = bf16[320,256]{1,0:T(8,128)(2,1)} collective-permute-done((bf16[320,256]{1,0:T(8,128)(2,1)}, bf16[320,256]{1,0:T(8,128)(2,1)}, u32[]{:S(2)}, u32[]{:S(2)}) %collective-permute-start.34) | collective-permute-done | bytes 163872 | tf_op jit(solution)/shard_map/ppermute | solution.py:265
  202.7 8.5 %collective-permute-done.37.refs_16_ = bf16[320,256]{1,0:T(8,128)(2,1)} collective-permute-done((bf16[320,256]{1,0:T(8,128)(2,1)}, bf16[320,256]{1,0:T(8,128)(2,1)}, u32[]{:S(2)}, u32[]{:S(2)}) %collective-permute-start.37) | collective-permute-done | bytes 163872 | tf_op jit(solution)/shard_map/ppermute | solution.py:265
  211.3 7.5 %far_terms.4 = (bf16[1,768,512]{2,1,0:T(8,128)(2,1)}, bf16[1,768,512]{2,1,0:T(8,128)(2,1)}) custom-call(s32[8]{0:T(128)} %get-tuple-element.790.refs_0_, s32[8]{0:T(128)} %get-tuple-element.781.refs_1_, s32[8]{0:T(128)} %get-tuple-element.779.refs_2_, bf16[768,1408]{1,0:T(8,128)(2,1)} %hidden.3.refs_3_, bf16[1088,256]{1,0:T(8,128)(2,1)} %copy-done.20, ...), custom_call_target="tpu_custom_call" | custom-call | flops 2214592512 | bytes 2883584 | tf_op jit(solution)/shard_map/far_terms/pallas_call | solution.py:492
  222.7 7.4 %near_terms.3 = (bf16[1,768,512]{2,1,0:T(8,128)(2,1)}, bf16[1,768,512]{2,1,0:T(8,128)(2,1)}) custom-call(s32[8]{0:T(128)} %get-tuple-element.790.refs_0_, s32[8]{0:T(128)} %get-tuple-element.781.refs_1_, s32[8]{0:T(128)} %get-tuple-element.779.refs_2_, bf16[768,1408]{1,0:T(8,128)(2,1)} %hidden.3.refs_3_, bf16[1088,256]{1,0:T(8,128)(2,1)} %copy-done.20, ...), custom_call_target="tpu_custom_call" | custom-call | flops 2214592512 | bytes 2883584 | tf_op jit(solution)/shard_map/near_terms/pallas_call | solution.py:492
  236.2 13.8 %collective-permute-done.42.refs_14_ = bf16[256,1408]{1,0:T(8,128)(2,1)} collective-permute-done((bf16[256,1408]{1,0:T(8,128)(2,1)}, bf16[256,1408]{1,0:T(8,128)(2,1)}, u32[]{:S(2)}, u32[]{:S(2)}) %collective-permute-start.42) | collective-permute-done | bytes 720928 | tf_op jit(solution)/shard_map/ppermute | solution.py:265
  256.7 8.8 %collective-permute-done.40.refs_22_ = bf16[256,1408]{1,0:T(8,128)(2,1)} collective-permute-done((bf16[256,1408]{1,0:T(8,128)(2,1)}, bf16[256,1408]{1,0:T(8,128)(2,1)}, u32[]{:S(2)}, u32[]{:S(2)}) %collective-permute-start.40) | collective-permute-done | bytes 720928 | tf_op jit(solution)/shard_map/ppermute | solution.py:265
  267.0 5.2 %collective-permute-done.38.refs_10_.refs_11_ = bf16[704,256]{1,0:T(8,128)(2,1)S(1)} collective-permute-done((bf16[704,256]{1,0:T(8,128)(2,1)}, bf16[704,256]{1,0:T(8,128)(2,1)S(1)}, u32[]{:S(2)}, u32[]{:S(2)}) %collective-permute-start.38) | collective-permute-done | bytes 360480 | tf_op jit(solution)/shard_map/ppermute | solution.py:265
  280.4 6.9 %hidden.4 = f32[768,256]{1,0:T(8,128)} custom-call(s32[8]{0:T(128)} %get-tuple-element.791.refs_0_, s32[4]{0:T(128)} %pad_add_fusion.refs_1_, f32[4,1,512]{2,1,0:T(1,128)} %bitcast.61, bf16[768,512]{1,0:T(8,128)(2,1)} %copy-done.2, bf16[768,512]{1,0:T(8,128)(2,1)} %copy-done.15, bf16[768,512]{1,0:T(8,128)(2,1)} %copy-done.14, bf16[768,512]{1,0:T(8,128)(2,1)} %copy-done.16, ...), custom_call_target="tpu_custom_call" | custom-call | flops 1610612736 | bytes 5242880 | tf_op jit(solution)/shard_map/hidden/pallas_call | solution.py:456
  287.4 6.9 %fusion.10 = f32[1,768,256]{2,0,1:T(1,128)S(1)} fusion(f32[1,768,256]{2,1,0:T(8,128)} %bitcast.57, f32[31,1,256]{2,0,1:T(8,128)S(1)} %bitcast.54), kind=kOutput, calls=%fused_computation.19 | convolution fusion | flops 72400896 | bytes 1604608 | tf_op jit(solution)/shard_map/conv_general_dilated | solution.py:560
  295.1 13.8 %collective-permute-done.49.refs_21_ = bf16[256,1408]{1,0:T(8,128)(2,1)} collective-permute-done((bf16[256,1408]{1,0:T(8,128)(2,1)}, bf16[256,1408]{1,0:T(8,128)(2,1)}, u32[]{:S(2)}, u32[]{:S(2)}) %collective-permute-start.49) | collective-permute-done | bytes 720928 | tf_op jit(solution)/shard_map/ppermute | solution.py:265
  310.5 6.2 %all-reduce = (f32[768]{0:T(1024)S(1)}, f32[768]{0:T(1024)S(1)}) all-reduce(f32[768]{0:T(1024)S(1)} %get-tuple-element.776, f32[768]{0:T(1024)S(1)} %get-tuple-element.775), channel_id=1, replica_groups=mesh['fs'=8,'tp'=4] {'tp'}, use_global_device_ids=true, to_apply=%region_3.4 | all-reduce | flops 1536 | bytes 12288 | tf_op jit(solution)/shard_map/psum | solution.py:570
  336.7 13.8 %collective-permute-done.56.refs_12_ = bf16[256,1408]{1,0:T(8,128)(2,1)} collective-permute-done((bf16[256,1408]{1,0:T(8,128)(2,1)}, bf16[256,1408]{1,0:T(8,128)(2,1)}, u32[]{:S(2)}, u32[]{:S(2)}) %collective-permute-start.56) | collective-permute-done | bytes 720928 | tf_op jit(solution)/shard_map/ppermute | solution.py:265
  356.2 9.9 %collective-permute-done.62.refs_20_ = bf16[256,1408]{1,0:T(8,128)(2,1)} collective-permute-done((bf16[256,1408]{1,0:T(8,128)(2,1)}, bf16[256,1408]{1,0:T(8,128)(2,1)}, u32[]{:S(2)}, u32[]{:S(2)}) %collective-permute-start.62) | collective-permute-done | bytes 720928 | tf_op jit(solution)/shard_map/ppermute | solution.py:265
  368.1 5.6 %collective-permute-done.65.refs_9_.refs_10_ = bf16[704,256]{1,0:T(8,128)(2,1)S(1)} collective-permute-done((bf16[704,256]{1,0:T(8,128)(2,1)S(1)}, bf16[704,256]{1,0:T(8,128)(2,1)S(1)}, u32[]{:S(2)}, u32[]{:S(2)}) %collective-permute-start.65) | collective-permute-done | bytes 360480 | tf_op jit(solution)/shard_map/ppermute | solution.py:265
  374.2 6.3 %collective-permute-done.60.refs_16_.refs_18_ = bf16[704,256]{1,0:T(8,128)(2,1)S(1)} collective-permute-done((bf16[704,256]{1,0:T(8,128)(2,1)}, bf16[704,256]{1,0:T(8,128)(2,1)S(1)}, u32[]{:S(2)}, u32[]{:S(2)}) %collective-permute-start.60) | collective-permute-done | bytes 360480 | tf_op jit(solution)/shard_map/ppermute | solution.py:265
  384.6 16.7 %collective-permute-done.67.refs_11_ = bf16[256,1408]{1,0:T(8,128)(2,1)S(1)} collective-permute-done((bf16[256,1408]{1,0:T(8,128)(2,1)}, bf16[256,1408]{1,0:T(8,128)(2,1)S(1)}, u32[]{:S(2)}, u32[]{:S(2)}) %collective-permute-start.67) | collective-permute-done | bytes 720928 | tf_op jit(solution)/shard_map/ppermute | solution.py:265
  405.1 16.4 %hidden.5.refs_3_ = bf16[768,1408]{1,0:T(8,128)(2,1)} custom-call(s32[8]{0:T(128)} %get-tuple-element.791.refs_0_, s32[4]{0:T(128)} %pad_add_fusion.refs_1_, f32[4,1,512]{2,1,0:T(1,128)} %bitcast.63, bf16[768,512]{1,0:T(8,128)(2,1)} %copy-done.12, bf16[768,512]{1,0:T(8,128)(2,1)} %copy-done.31, bf16[768,512]{1,0:T(8,128)(2,1)} %copy-done.30, ...), custom_call_target="tpu_custom_call" | custom-call | flops 8858370048 | bytes 14680064 | tf_op jit(solution)/shard_map/hidden/pallas_call | solution.py:456
  423.6 6.5 %far_terms.6 = (bf16[1,768,512]{2,1,0:T(8,128)(2,1)}, bf16[1,768,512]{2,1,0:T(8,128)(2,1)}) custom-call(s32[8]{0:T(128)} %get-tuple-element.790.refs_0_, s32[8]{0:T(128)} %get-tuple-element.781.refs_1_, s32[8]{0:T(128)} %get-tuple-element.779.refs_2_, bf16[768,1408]{1,0:T(8,128)(2,1)} %hidden.5.refs_3_, bf16[704,256]{1,0:T(8,128)(2,1)} %get-tuple-element.577.refs_4_, ...), custom_call_target="tpu_custom_call" | custom-call | flops 2214592512 | bytes 2883584 | tf_op jit(solution)/shard_map/far_terms/pallas_call | solution.py:492
  431.3 4.6 far_terms.7
  439.3 7.5 %near_terms.5 = (bf16[1,768,512]{2,1,0:T(8,128)(2,1)}, bf16[1,768,512]{2,1,0:T(8,128)(2,1)}) custom-call(s32[8]{0:T(128)} %get-tuple-element.790.refs_0_, s32[8]{0:T(128)} %get-tuple-element.781.refs_1_, s32[8]{0:T(128)} %get-tuple-element.779.refs_2_, bf16[768,1408]{1,0:T(8,128)(2,1)} %hidden.5.refs_3_, bf16[704,256]{1,0:T(8,128)(2,1)} %get-tuple-element.577.refs_4_, ...), custom_call_target="tpu_custom_call" | custom-call | flops 2214592512 | bytes 2883584 | tf_op jit(solution)/shard_map/near_terms/pallas_call | solution.py:492
  449.5 17.4 %collective-permute-done.81 = bf16[768,512]{1,0:T(8,128)(2,1)S(1)} collective-permute-done((bf16[768,512]{1,0:T(8,128)(2,1)S(1)}, bf16[768,512]{1,0:T(8,128)(2,1)S(1)}, u32[]{:S(2)}, u32[]{:S(2)}) %collective-permute-start.81) | collective-permute-done | bytes 786464 | tf_op jit(solution)/shard_map/ppermute | solution.py:321
  (264 shorter events, 138.0 us)
Async XLA Ops:
  0.0 22.2 %collective-permute-start.2 = (bf16[768,512]{1,0:T(8,128)(2,1)}, bf16[768,512]{1,0:T(8,128)(2,1)S(1)}, u32[]{:S(2)}, u32[]{:S(2)}) collective-permute-start(bf16[768,512]{1,0:T(8,128)(2,1)} %refs_3_), channel_id=1, source_target_pairs={{0,2},{1,3},{2,0},{3,1},{4,6},{5,7},{6,4},{7,5},{8,10},{9,11},{10,... | collective-permute-start | bytes 2359304 | tf_op jit(solution)/shard_map/ppermute | solution.py:321
  5.1 37.3 %collective-permute-start.7 = (bf16[768,512]{1,0:T(8,128)(2,1)}, bf16[768,512]{1,0:T(8,128)(2,1)S(1)}, u32[]{:S(2)}, u32[]{:S(2)}) collective-permute-start(bf16[768,512]{1,0:T(8,128)(2,1)} %refs_3_), channel_id=1, source_target_pairs={{0,1},{1,0},{2,3},{3,2},{4,5},{5,4},{6,7},{7,6},{8,9},{9,8},{10,11... | collective-permute-start | bytes 2359304 | tf_op jit(solution)/shard_map/ppermute | solution.py:313
  24.3 32.7 %collective-permute-start.3 = (bf16[256,1408]{1,0:T(8,128)(2,1)S(1)}, bf16[256,1408]{1,0:T(8,128)(2,1)}, u32[]{:S(2)}, u32[]{:S(2)}) collective-permute-start(bf16[256,1408]{1,0:T(8,128)(2,1)S(1)} %collective-permute-done.refs_14_), channel_id=1, source_target_pairs={{0,8},{4,0},{8,16},{12,4},{16,24},{20,12},{24,28},{28,20},{1,9},{5... | collective-permute-start | bytes 2162696 | tf_op jit(solution)/shard_map/ppermute | solution.py:265
  43.4 29.2 %collective-permute-start.11 = (bf16[256,1408]{1,0:T(8,128)(2,1)}, bf16[256,1408]{1,0:T(8,128)(2,1)}, u32[]{:S(2)}, u32[]{:S(2)}) collective-permute-start(bf16[256,1408]{1,0:T(8,128)(2,1)} %collective-permute-done.5.refs_22_), channel_id=1, source_target_pairs={{0,8},{4,0},{8,16},{12,4},{16,24},{20,12},{24,28},{28,20},{1,9},{5... | collective-permute-start | bytes 2162696 | tf_op jit(solution)/shard_map/ppermute | solution.py:265
  44.9 31.3 %collective-permute-start.12 = (bf16[256,1408]{1,0:T(8,128)(2,1)}, bf16[256,1408]{1,0:T(8,128)(2,1)}, u32[]{:S(2)}, u32[]{:S(2)}) collective-permute-start(bf16[256,1408]{1,0:T(8,128)(2,1)} %collective-permute-done.6.refs_16_), channel_id=1, source_target_pairs={{0,4},{4,12},{8,0},{12,20},{16,8},{20,28},{24,16},{28,24},{1,5},{5... | collective-permute-start | bytes 2162696 | tf_op jit(solution)/shard_map/ppermute | solution.py:265
  60.7 30.9 %collective-permute-start.10 = (bf16[256,1408]{1,0:T(8,128)(2,1)}, bf16[256,1408]{1,0:T(8,128)(2,1)}, u32[]{:S(2)}, u32[]{:S(2)}) collective-permute-start(bf16[256,1408]{1,0:T(8,128)(2,1)} %collective-permute-done.4.refs_9_), channel_id=1, source_target_pairs={{0,4},{4,12},{8,0},{12,20},{16,8},{20,28},{24,16},{28,24},{1,5},{5... | collective-permute-start | bytes 2162696 | tf_op jit(solution)/shard_map/ppermute | solution.py:265
  61.2 30.4 %collective-permute-start.9 = (bf16[256,1408]{1,0:T(8,128)(2,1)}, bf16[256,1408]{1,0:T(8,128)(2,1)}, u32[]{:S(2)}, u32[]{:S(2)}) collective-permute-start(bf16[256,1408]{1,0:T(8,128)(2,1)} %collective-permute-done.3.refs_13_), channel_id=1, source_target_pairs={{0,8},{4,0},{8,16},{12,4},{16,24},{20,12},{24,28},{28,20},{1,9},{5... | collective-permute-start | bytes 2162696 | tf_op jit(solution)/shard_map/ppermute | solution.py:265
  76.2 27.2 %collective-permute-start.14 = (bf16[256,1408]{1,0:T(8,128)(2,1)}, bf16[256,1408]{1,0:T(8,128)(2,1)}, u32[]{:S(2)}, u32[]{:S(2)}) collective-permute-start(bf16[256,1408]{1,0:T(8,128)(2,1)} %collective-permute-done.11.refs_21_), channel_id=1, source_target_pairs={{0,8},{4,0},{8,16},{12,4},{16,24},{20,12},{24,28},{28,20},{1,9},{5... | collective-permute-start | bytes 2162696 | tf_op jit(solution)/shard_map/ppermute | solution.py:265
  77.8 27.4 %collective-permute-start.15 = (bf16[256,1408]{1,0:T(8,128)(2,1)}, bf16[256,1408]{1,0:T(8,128)(2,1)}, u32[]{:S(2)}, u32[]{:S(2)}) collective-permute-start(bf16[256,1408]{1,0:T(8,128)(2,1)} %collective-permute-done.12.refs_17_), channel_id=1, source_target_pairs={{0,4},{4,12},{8,0},{12,20},{16,8},{20,28},{24,16},{28,24},{1,5},{5... | collective-permute-start | bytes 2162696 | tf_op jit(solution)/shard_map/ppermute | solution.py:265
  91.6 26.7 %collective-permute-start.13 = (bf16[256,1408]{1,0:T(8,128)(2,1)}, bf16[256,1408]{1,0:T(8,128)(2,1)}, u32[]{:S(2)}, u32[]{:S(2)}) collective-permute-start(bf16[256,1408]{1,0:T(8,128)(2,1)} %collective-permute-done.9.refs_12_), channel_id=1, source_target_pairs={{0,8},{4,0},{8,16},{12,4},{16,24},{20,12},{24,28},{28,20},{1,9},{5... | collective-permute-start | bytes 2162696 | tf_op jit(solution)/shard_map/ppermute | solution.py:265
  118.4 22.2 %collective-permute-start.18 = (bf16[1088,256]{1,0:T(8,128)(2,1)S(1)}, bf16[1088,256]{1,0:T(8,128)(2,1)}, u32[]{:S(2)}, u32[]{:S(2)}) collective-permute-start(bf16[1088,256]{1,0:T(8,128)(2,1)S(1)} %slice.17.refs_4_), channel_id=1, source_target_pairs={{0,8},{4,0},{8,16},{12,4},{16,24},{20,12},{24,28},{28,20},{1,9},{5... | collective-permute-start | bytes 1671176 | tf_op jit(solution)/shard_map/ppermute | solution.py:265
  122.4 23.4 %collective-permute-start.16 = (bf16[256,768]{1,0:T(8,128)(2,1)S(1)}, bf16[256,768]{1,0:T(8,128)(2,1)S(1)}, u32[]{:S(2)}, u32[]{:S(2)}) collective-permute-start(bf16[256,768]{1,0:T(8,128)(2,1)S(1)} %constant_dynamic-update-slice_fusion.refs_7_.refs_4_), channel_id=1, source_target_pairs={{0,8},{4,0},{8,16},{12,4},{16,24},{20,12},{24,28},{28,20},{1,9},{5... | collective-permute-start | bytes 1179656 | tf_op jit(solution)/shard_map/ppermute | solution.py:265
  140.5 29.2 %collective-permute-start.25 = (bf16[1088,256]{1,0:T(8,128)(2,1)}, bf16[1088,256]{1,0:T(8,128)(2,1)}, u32[]{:S(2)}, u32[]{:S(2)}) collective-permute-start(bf16[1088,256]{1,0:T(8,128)(2,1)} %collective-permute-done.18.refs_11_), channel_id=1, source_target_pairs={{0,8},{4,0},{8,16},{12,4},{16,24},{20,12},{24,28},{28,20},{1,9},{5... | collective-permute-start | bytes 1671176 | tf_op jit(solution)/shard_map/ppermute | solution.py:265
  142.2 27.5 %collective-permute-start.26 = (bf16[1088,256]{1,0:T(8,128)(2,1)}, bf16[1088,256]{1,0:T(8,128)(2,1)}, u32[]{:S(2)}, u32[]{:S(2)}) collective-permute-start(bf16[1088,256]{1,0:T(8,128)(2,1)} %collective-permute-done.19.refs_5_), channel_id=1, source_target_pairs={{0,4},{4,12},{8,0},{12,20},{16,8},{20,28},{24,16},{28,24},{1,5},{5... | collective-permute-start | bytes 1671176 | tf_op jit(solution)/shard_map/ppermute | solution.py:265
  142.6 23.6 %collective-permute-start.17 = (bf16[256,768]{1,0:T(8,128)(2,1)S(1)}, bf16[256,768]{1,0:T(8,128)(2,1)S(1)}, u32[]{:S(2)}, u32[]{:S(2)}) collective-permute-start(bf16[256,768]{1,0:T(8,128)(2,1)S(1)} %constant_dynamic-update-slice_fusion.refs_7_.refs_4_), channel_id=1, source_target_pairs={{0,4},{4,12},{8,0},{12,20},{16,8},{20,28},{24,16},{28,24},{1,5},{5... | collective-permute-start | bytes 1179656 | tf_op jit(solution)/shard_map/ppermute | solution.py:265
  143.1 25.0 %collective-permute-start.27 = (bf16[320,256]{1,0:T(8,128)(2,1)S(1)}, bf16[320,256]{1,0:T(8,128)(2,1)S(1)}, u32[]{:S(2)}, u32[]{:S(2)}) collective-permute-start(bf16[320,256]{1,0:T(8,128)(2,1)S(1)} %collective-permute-done.20.refs_19_), channel_id=1, source_target_pairs={{0,8},{4,0},{8,16},{12,4},{16,24},{20,12},{24,28},{28,20},{1,9},{5... | collective-permute-start | bytes 491528 | tf_op jit(solution)/shard_map/ppermute | solution.py:265
  145.8 23.9 %collective-permute-start.28 = (bf16[320,256]{1,0:T(8,128)(2,1)S(1)}, bf16[320,256]{1,0:T(8,128)(2,1)S(1)}, u32[]{:S(2)}, u32[]{:S(2)}) collective-permute-start(bf16[320,256]{1,0:T(8,128)(2,1)S(1)} %collective-permute-done.21.refs_13_), channel_id=1, source_target_pairs={{0,4},{4,12},{8,0},{12,20},{16,8},{20,28},{24,16},{28,24},{1,5},{5... | collective-permute-start | bytes 491528 | tf_op jit(solution)/shard_map/ppermute | solution.py:265
  169.7 29.5 %collective-permute-start.31 = (bf16[1088,256]{1,0:T(8,128)(2,1)}, bf16[1088,256]{1,0:T(8,128)(2,1)}, u32[]{:S(2)}, u32[]{:S(2)}) collective-permute-start(bf16[1088,256]{1,0:T(8,128)(2,1)} %collective-permute-done.25.refs_10_), channel_id=1, source_target_pairs={{0,8},{4,0},{8,16},{12,4},{16,24},{20,12},{24,28},{28,20},{1,9},{5... | collective-permute-start | bytes 1671176 | tf_op jit(solution)/shard_map/ppermute | solution.py:265
  171.7 27.5 %collective-permute-start.32 = (bf16[1088,256]{1,0:T(8,128)(2,1)}, bf16[1088,256]{1,0:T(8,128)(2,1)}, u32[]{:S(2)}, u32[]{:S(2)}) collective-permute-start(bf16[1088,256]{1,0:T(8,128)(2,1)} %collective-permute-done.26.refs_6_), channel_id=1, source_target_pairs={{0,4},{4,12},{8,0},{12,20},{16,8},{20,28},{24,16},{28,24},{1,5},{5... | collective-permute-start | bytes 1671176 | tf_op jit(solution)/shard_map/ppermute | solution.py:265
  180.1 21.4 %collective-permute-start.29 = (bf16[256,768]{1,0:T(8,128)(2,1)S(1)}, bf16[256,768]{1,0:T(8,128)(2,1)S(1)}, u32[]{:S(2)}, u32[]{:S(2)}) collective-permute-start(bf16[256,768]{1,0:T(8,128)(2,1)S(1)} %collective-permute-done.23.refs_13_.refs_10_), channel_id=1, source_target_pairs={{0,8},{4,0},{8,16},{12,4},{16,24},{20,12},{24,28},{28,20},{1,9},{5... | collective-permute-start | bytes 1179656 | tf_op jit(solution)/shard_map/ppermute | solution.py:265
  230.3 21.2 %collective-permute-start.46 = (bf16[768,512]{1,0:T(8,128)(2,1)S(1)}, bf16[768,512]{1,0:T(8,128)(2,1)}, u32[]{:S(2)}, u32[]{:S(2)}) collective-permute-start(bf16[768,512]{1,0:T(8,128)(2,1)S(1)} %bitcast.58), channel_id=1, source_target_pairs={{0,2},{1,3},{2,0},{3,1},{4,6},{5,7},{6,4},{7,5},{8,10},{9,11},{10,... | collective-permute-start | bytes 2359304 | tf_op jit(solution)/shard_map/ppermute | solution.py:321
  232.7 32.7 %collective-permute-start.40 = (bf16[256,1408]{1,0:T(8,128)(2,1)}, bf16[256,1408]{1,0:T(8,128)(2,1)}, u32[]{:S(2)}, u32[]{:S(2)}) collective-permute-start(bf16[256,1408]{1,0:T(8,128)(2,1)} %refs_15_.3), channel_id=1, source_target_pairs={{0,8},{4,0},{8,16},{12,4},{16,24},{20,12},{24,28},{28,20},{1,9},{5... | collective-permute-start | bytes 2162696 | tf_op jit(solution)/shard_map/ppermute | solution.py:265
  234.2 32.7 %collective-permute-start.41 = (bf16[256,1408]{1,0:T(8,128)(2,1)}, bf16[256,1408]{1,0:T(8,128)(2,1)}, u32[]{:S(2)}, u32[]{:S(2)}) collective-permute-start(bf16[256,1408]{1,0:T(8,128)(2,1)} %refs_15_.3), channel_id=1, source_target_pairs={{0,4},{4,12},{8,0},{12,20},{16,8},{20,28},{24,16},{28,24},{1,5},{5... | collective-permute-start | bytes 2162696 | tf_op jit(solution)/shard_map/ppermute | solution.py:265
  276.1 32.7 %collective-permute-start.49 = (bf16[256,1408]{1,0:T(8,128)(2,1)}, bf16[256,1408]{1,0:T(8,128)(2,1)}, u32[]{:S(2)}, u32[]{:S(2)}) collective-permute-start(bf16[256,1408]{1,0:T(8,128)(2,1)} %collective-permute-done.40.refs_22_), channel_id=1, source_target_pairs={{0,8},{4,0},{8,16},{12,4},{16,24},{20,12},{24,28},{28,20},{1,9},{5... | collective-permute-start | bytes 2162696 | tf_op jit(solution)/shard_map/ppermute | solution.py:265
  277.5 32.7 %collective-permute-start.50 = (bf16[256,1408]{1,0:T(8,128)(2,1)}, bf16[256,1408]{1,0:T(8,128)(2,1)}, u32[]{:S(2)}, u32[]{:S(2)}) collective-permute-start(bf16[256,1408]{1,0:T(8,128)(2,1)} %collective-permute-done.41.refs_16_), channel_id=1, source_target_pairs={{0,4},{4,12},{8,0},{12,20},{16,8},{20,28},{24,16},{28,24},{1,5},{5... | collective-permute-start | bytes 2162696 | tf_op jit(solution)/shard_map/ppermute | solution.py:265
  279.0 38.8 %collective-permute-start.47 = (bf16[704,256]{1,0:T(8,128)(2,1)S(1)}, bf16[704,256]{1,0:T(8,128)(2,1)}, u32[]{:S(2)}, u32[]{:S(2)}) collective-permute-start(bf16[704,256]{1,0:T(8,128)(2,1)S(1)} %copy-done.21), channel_id=1, source_target_pairs={{0,8},{4,0},{8,16},{12,4},{16,24},{20,12},{24,28},{28,20},{1,9},{5... | collective-permute-start | bytes 1081352 | tf_op jit(solution)/shard_map/ppermute | solution.py:265
  294.4 23.5 %collective-permute-start.48 = (bf16[704,256]{1,0:T(8,128)(2,1)S(1)}, bf16[704,256]{1,0:T(8,128)(2,1)}, u32[]{:S(2)}, u32[]{:S(2)}) collective-permute-start(bf16[704,256]{1,0:T(8,128)(2,1)S(1)} %copy-done.21), channel_id=1, source_target_pairs={{0,4},{4,12},{8,0},{12,20},{16,8},{20,28},{24,16},{28,24},{1,5},{5... | collective-permute-start | bytes 1081352 | tf_op jit(solution)/shard_map/ppermute | solution.py:265
  333.3 32.7 %collective-permute-start.62 = (bf16[256,1408]{1,0:T(8,128)(2,1)}, bf16[256,1408]{1,0:T(8,128)(2,1)}, u32[]{:S(2)}, u32[]{:S(2)}) collective-permute-start(bf16[256,1408]{1,0:T(8,128)(2,1)} %collective-permute-done.49.refs_21_), channel_id=1, source_target_pairs={{0,8},{4,0},{8,16},{12,4},{16,24},{20,12},{24,28},{28,20},{1,9},{5... | collective-permute-start | bytes 2162696 | tf_op jit(solution)/shard_map/ppermute | solution.py:265
  333.8 32.7 %collective-permute-start.63 = (bf16[256,1408]{1,0:T(8,128)(2,1)}, bf16[256,1408]{1,0:T(8,128)(2,1)}, u32[]{:S(2)}, u32[]{:S(2)}) collective-permute-start(bf16[256,1408]{1,0:T(8,128)(2,1)} %collective-permute-done.50.refs_17_), channel_id=1, source_target_pairs={{0,4},{4,12},{8,0},{12,20},{16,8},{20,28},{24,16},{28,24},{1,5},{5... | collective-permute-start | bytes 2162696 | tf_op jit(solution)/shard_map/ppermute | solution.py:265
  352.6 29.4 %collective-permute-start.69 = (bf16[768,512]{1,0:T(8,128)(2,1)S(1)}, bf16[768,512]{1,0:T(8,128)(2,1)S(1)}, u32[]{:S(2)}, u32[]{:S(2)}) collective-permute-start(bf16[768,512]{1,0:T(8,128)(2,1)S(1)} %fusion.5.refs_3_), channel_id=1, source_target_pairs={{0,2},{1,3},{2,0},{3,1},{4,6},{5,7},{6,4},{7,5},{8,10},{9,11},{10,... | collective-permute-start | bytes 2359304 | tf_op jit(solution)/shard_map/ppermute | solution.py:321
  381.3 21.7 %collective-permute-start.68 = (bf16[768,512]{1,0:T(8,128)(2,1)S(1)}, bf16[768,512]{1,0:T(8,128)(2,1)S(1)}, u32[]{:S(2)}, u32[]{:S(2)}) collective-permute-start(bf16[768,512]{1,0:T(8,128)(2,1)S(1)} %fusion.5.refs_3_), channel_id=1, source_target_pairs={{0,1},{1,0},{2,3},{3,2},{4,5},{5,4},{6,7},{7,6},{8,9},{9,8},{10,11... | collective-permute-start | bytes 2359304 | tf_op jit(solution)/shard_map/ppermute | solution.py:313
  384.1 37.4 %collective-permute-start.73 = (bf16[704,256]{1,0:T(8,128)(2,1)}, bf16[704,256]{1,0:T(8,128)(2,1)S(1)}, u32[]{:S(2)}, u32[]{:S(2)}) collective-permute-start(bf16[704,256]{1,0:T(8,128)(2,1)} %copy-done.37), channel_id=1, source_target_pairs={{0,8},{4,0},{8,16},{12,4},{16,24},{20,12},{24,28},{28,20},{1,9},{5... | collective-permute-start | bytes 1081352 | tf_op jit(solution)/shard_map/ppermute | solution.py:265
  (98 other events, 2463.0 us)

commit v5 on v4

--- a/solution.py
+++ b/solution.py
@@ -135,6 +135,19 @@
             def _(core=core):
                 outs[core][to, :, pl.ds(first, width)] = value
 
+    if when == LAST:
+        for out in outs:
+            out[...] = jnp.zeros_like(out)
+
+        @pl.when(wanted(last))
+        def _():
+            for part, shard in enumerate(shards):
+                columns[0, pl.ds(*spans[part]), :] = shard[:, low : low + width]
+            value = jnp.dot(hidden[...], columns[0], preferred_element_type=jnp.float32)
+            put(last, value.astype(jnp.bfloat16))
+
+        return
+
     for number, slot in enumerate(used):
 
         @pl.when(wanted(slot))
@@ -153,11 +166,6 @@
         value = jnp.dot(hidden[...], columns[slot], preferred_element_type=jnp.float32)
         put(slot, value.astype(jnp.bfloat16))
 
-    if when == LAST:
-        for out in outs:
-            out[...] = jnp.zeros_like(out)
-        pl.when(wanted(last))(lambda: product(last))
-        return
     if when == EARLY:
         empty = jnp.zeros((hidden.shape[0], width), jnp.bfloat16)
         pl.when(wanted(last))(lambda: put(last, empty))
@@ -383,7 +391,7 @@
 def solution(mesh):
     order = grid_ring(mesh)
     cores = cores_of(mesh)
-    depth = 3
+    depth = 4
 
     def per_device(
         tokens,
@@ -494,10 +502,12 @@
                     ring.count, len(sides), low, cores, far, when, *refs
                 ),
                 out_shape=[out] * cores,
-                in_specs=[spec(smem)] * 3 + [spec(vmem)] + [spec(hbm)] * len(arrays),
+                in_specs=[spec(smem)] * 3
+                + [spec(vmem)]
+                + [spec(vmem if when == LAST else hbm)] * len(arrays),
                 out_specs=[spec(vmem)] * cores,
                 scratch_shapes=[
-                    pltpu.VMEM((ring.count, depth_all, width), jnp.bfloat16),
+                    pltpu.VMEM((1 if when == LAST else ring.count, depth_all, width), jnp.bfloat16),
                     pltpu.SemaphoreType.DMA((len(sides), ring.count)),
                 ],
                 cost_estimate=pl.CostEstimate(

time: 471 us -> 472 us (level)
  transfers between devices with their start and end apart: 82 -> 82, of which waited for: 42 -> 40; matrix products, arithmetic and copies ran while one was open for 5% -> 5% of each run, Pallas kernels for 11% -> 11%
where the time goes in v5:
time: 472 us; the launch traced here: 471 us
  waiting for transfers between devices  275 us (58%)
  Pallas kernels  81.1 us (17%)
  starting transfers between devices  74.3 us (16%)
  other arithmetic  17.5 us (4%)
  local copies, waits for them, and re-layouts  8.42 us (2%)
  matrix products  6.93 us (1%)
  blocking collectives  6.17 us (1%)
    ppermute x63, waiting for transfers between devices, launch(): landed = [lax.ppermute(a, 'fs', way) for a, (_, way) in zip(arrays, sends)]  250 us
    ppermute x63, starting transfers between devices, launch(): landed = [lax.ppermute(a, 'fs', way) for a, (_, way) in zip(arrays, sends)]  65.6 us
    pallas_call x7, Pallas kernels, terms_of(): pl.pallas_call(lambda *refs: terms_kernel(ring.count, len(sides), low, co...  41.3 us
    pallas_call x3, Pallas kernels, hidden_of(): pl.pallas_call(lambda *refs: hidden_kernel(count, ring.count, len(sides),...  39.8 us
    ppermute x6, waiting for transfers between devices, across_chip(): return lax.ppermute(value, 'tp', pairs)  17.4 us
  transfers between devices with their start and end apart: 82, of which 40 were waited for; matrix products, arithmetic and copies ran while one was open for 5% of the time, Pallas kernels for 11%

profile of v5, /device:TPU:0, one launch (start us, length us, event | category | flops | bytes accessed | tf_op | source)
XLA Modules:
  0.0 471.1 jit_solution(8270509136428519040)
XLA Ops:
  5.1 15.8 %collective-permute-done.2.refs_14_ = bf16[256,1408]{1,0:T(8,128)(2,1)S(1)} collective-permute-done((bf16[256,1408]{1,0:T(8,128)(2,1)}, bf16[256,1408]{1,0:T(8,128)(2,1)S(1)}, u32[]{:S(2)}, u32[]{:S(2)}) %collective-permute-start.2) | collective-permute-done | bytes 720928 | tf_op jit(solution)/shard_map/ppermute | solution.py:273
  25.4 15.9 %collective-permute-done.refs_22_ = bf16[256,1408]{1,0:T(8,128)(2,1)} collective-permute-done((bf16[256,1408]{1,0:T(8,128)(2,1)}, bf16[256,1408]{1,0:T(8,128)(2,1)}, u32[]{:S(2)}, u32[]{:S(2)}) %collective-permute-start) | collective-permute-done | bytes 720928 | tf_op jit(solution)/shard_map/ppermute | solution.py:273
  45.4 13.3 %collective-permute-done.10.refs_9_ = bf16[256,1408]{1,0:T(8,128)(2,1)} collective-permute-done((bf16[256,1408]{1,0:T(8,128)(2,1)}, bf16[256,1408]{1,0:T(8,128)(2,1)}, u32[]{:S(2)}, u32[]{:S(2)}) %collective-permute-start.10) | collective-permute-done | bytes 720928 | tf_op jit(solution)/shard_map/ppermute | solution.py:273
  62.6 13.4 %collective-permute-done.7.refs_21_ = bf16[256,1408]{1,0:T(8,128)(2,1)} collective-permute-done((bf16[256,1408]{1,0:T(8,128)(2,1)}, bf16[256,1408]{1,0:T(8,128)(2,1)}, u32[]{:S(2)}, u32[]{:S(2)}) %collective-permute-start.7) | collective-permute-done | bytes 720928 | tf_op jit(solution)/shard_map/ppermute | solution.py:273
  80.2 11.3 %collective-permute-done.13.refs_12_ = bf16[256,1408]{1,0:T(8,128)(2,1)} collective-permute-done((bf16[256,1408]{1,0:T(8,128)(2,1)}, bf16[256,1408]{1,0:T(8,128)(2,1)}, u32[]{:S(2)}, u32[]{:S(2)}) %collective-permute-start.13) | collective-permute-done | bytes 720928 | tf_op jit(solution)/shard_map/ppermute | solution.py:273
  93.0 13.9 %collective-permute-done.11.refs_20_ = bf16[256,1408]{1,0:T(8,128)(2,1)} collective-permute-done((bf16[256,1408]{1,0:T(8,128)(2,1)}, bf16[256,1408]{1,0:T(8,128)(2,1)}, u32[]{:S(2)}, u32[]{:S(2)}) %collective-permute-start.11) | collective-permute-done | bytes 720928 | tf_op jit(solution)/shard_map/ppermute | solution.py:273
  112.6 8.4 %collective-permute-done.22.refs_11_ = bf16[256,1408]{1,0:T(8,128)(2,1)} collective-permute-done((bf16[256,1408]{1,0:T(8,128)(2,1)}, bf16[256,1408]{1,0:T(8,128)(2,1)}, u32[]{:S(2)}, u32[]{:S(2)}) %collective-permute-start.22) | collective-permute-done | bytes 720928 | tf_op jit(solution)/shard_map/ppermute | solution.py:273
  126.6 16.5 %hidden.3.refs_3_ = bf16[768,1408]{1,0:T(8,128)(2,1)} custom-call(s32[8]{0:T(128)} %get-tuple-element.773.refs_0_, s32[4]{0:T(128)} %pad_add_fusion.refs_1_, f32[4,1,512]{2,1,0:T(1,128)} %bitcast.62, bf16[768,512]{1,0:T(8,128)(2,1)} %refs_3_, bf16[768,512]{1,0:T(8,128)(2,1)} %copy-done.29, bf16[768,512]{1,0:T(8,128)(2,1)} %copy-done.28, ...), custom_call_target="tpu_custom_call" | custom-call | flops 8858370048 | bytes 14680064 | tf_op jit(solution)/shard_map/hidden/pallas_call | solution.py:464
  149.4 19.1 %collective-permute-done.16.refs_8_.refs_5_ = bf16[256,768]{1,0:T(8,128)(2,1)S(1)} collective-permute-done((bf16[256,768]{1,0:T(8,128)(2,1)S(1)}, bf16[256,768]{1,0:T(8,128)(2,1)S(1)}, u32[]{:S(2)}, u32[]{:S(2)}) %collective-permute-start.16) | collective-permute-done | bytes 393248 | tf_op jit(solution)/shard_map/ppermute | solution.py:273
  175.8 4.6 collective-permute-done.23.refs_13_.refs_10_
  184.3 7.7 %collective-permute-done.33.refs_17_ = bf16[320,256]{1,0:T(8,128)(2,1)} collective-permute-done((bf16[320,256]{1,0:T(8,128)(2,1)S(1)}, bf16[320,256]{1,0:T(8,128)(2,1)}, u32[]{:S(2)}, u32[]{:S(2)}) %collective-permute-start.33) | collective-permute-done | bytes 163872 | tf_op jit(solution)/shard_map/ppermute | solution.py:273
  192.4 9.4 %collective-permute-done.34.refs_15_ = bf16[320,256]{1,0:T(8,128)(2,1)} collective-permute-done((bf16[320,256]{1,0:T(8,128)(2,1)}, bf16[320,256]{1,0:T(8,128)(2,1)}, u32[]{:S(2)}, u32[]{:S(2)}) %collective-permute-start.34) | collective-permute-done | bytes 163872 | tf_op jit(solution)/shard_map/ppermute | solution.py:273
  205.7 7.2 %collective-permute-done.41.refs_16_ = bf16[320,256]{1,0:T(8,128)(2,1)} collective-permute-done((bf16[320,256]{1,0:T(8,128)(2,1)}, bf16[320,256]{1,0:T(8,128)(2,1)}, u32[]{:S(2)}, u32[]{:S(2)}) %collective-permute-start.41) | collective-permute-done | bytes 163872 | tf_op jit(solution)/shard_map/ppermute | solution.py:273
  212.9 7.5 %far_terms.4 = (bf16[1,768,512]{2,1,0:T(8,128)(2,1)}, bf16[1,768,512]{2,1,0:T(8,128)(2,1)}) custom-call(s32[8]{0:T(128)} %get-tuple-element.772.refs_0_, s32[8]{0:T(128)} %get-tuple-element.763.refs_1_, s32[8]{0:T(128)} %get-tuple-element.761.refs_2_, bf16[768,1408]{1,0:T(8,128)(2,1)} %hidden.3.refs_3_, bf16[1088,256]{1,0:T(8,128)(2,1)} %copy-done.20, ...), custom_call_target="tpu_custom_call" | custom-call | flops 2214592512 | bytes 2883584 | tf_op jit(solution)/shard_map/far_terms/pallas_call | solution.py:500
  224.3 7.4 %near_terms.3 = (bf16[1,768,512]{2,1,0:T(8,128)(2,1)}, bf16[1,768,512]{2,1,0:T(8,128)(2,1)}) custom-call(s32[8]{0:T(128)} %get-tuple-element.772.refs_0_, s32[8]{0:T(128)} %get-tuple-element.763.refs_1_, s32[8]{0:T(128)} %get-tuple-element.761.refs_2_, bf16[768,1408]{1,0:T(8,128)(2,1)} %hidden.3.refs_3_, bf16[1088,256]{1,0:T(8,128)(2,1)} %copy-done.20, ...), custom_call_target="tpu_custom_call" | custom-call | flops 2214592512 | bytes 2883584 | tf_op jit(solution)/shard_map/near_terms/pallas_call | solution.py:500
  237.9 13.8 %collective-permute-done.37.refs_14_ = bf16[256,1408]{1,0:T(8,128)(2,1)} collective-permute-done((bf16[256,1408]{1,0:T(8,128)(2,1)}, bf16[256,1408]{1,0:T(8,128)(2,1)}, u32[]{:S(2)}, u32[]{:S(2)}) %collective-permute-start.37) | collective-permute-done | bytes 720928 | tf_op jit(solution)/shard_map/ppermute | solution.py:273
  258.8 8.4 %collective-permute-done.35.refs_22_ = bf16[256,1408]{1,0:T(8,128)(2,1)} collective-permute-done((bf16[256,1408]{1,0:T(8,128)(2,1)}, bf16[256,1408]{1,0:T(8,128)(2,1)}, u32[]{:S(2)}, u32[]{:S(2)}) %collective-permute-start.35) | collective-permute-done | bytes 720928 | tf_op jit(solution)/shard_map/ppermute | solution.py:273
  269.2 4.7 %collective-permute-done.47.refs_10_.refs_11_ = bf16[704,256]{1,0:T(8,128)(2,1)S(1)} collective-permute-done((bf16[704,256]{1,0:T(8,128)(2,1)S(1)}, bf16[704,256]{1,0:T(8,128)(2,1)S(1)}, u32[]{:S(2)}, u32[]{:S(2)}) %collective-permute-start.47) | collective-permute-done | bytes 360480 | tf_op jit(solution)/shard_map/ppermute | solution.py:273
  282.2 6.9 %hidden.4 = f32[768,256]{1,0:T(8,128)} custom-call(s32[8]{0:T(128)} %get-tuple-element.773.refs_0_, s32[4]{0:T(128)} %pad_add_fusion.refs_1_, f32[4,1,512]{2,1,0:T(1,128)} %bitcast.61, bf16[768,512]{1,0:T(8,128)(2,1)} %copy-done.2, bf16[768,512]{1,0:T(8,128)(2,1)} %copy-done.15, bf16[768,512]{1,0:T(8,128)(2,1)} %copy-done.14, bf16[768,512]{1,0:T(8,128)(2,1)} %copy-done.16, ...), custom_call_target="tpu_custom_call" | custom-call | flops 1610612736 | bytes 5242880 | tf_op jit(solution)/shard_map/hidden/pallas_call | solution.py:464
  289.1 6.9 %fusion.10 = f32[1,768,256]{2,0,1:T(1,128)S(1)} fusion(f32[1,768,256]{2,1,0:T(8,128)} %bitcast.57, f32[31,1,256]{2,0,1:T(8,128)S(1)} %bitcast.54), kind=kOutput, calls=%fused_computation.19 | convolution fusion | flops 72400896 | bytes 1604608 | tf_op jit(solution)/shard_map/conv_general_dilated | solution.py:570
  298.2 12.9 %collective-permute-done.49.refs_21_ = bf16[256,1408]{1,0:T(8,128)(2,1)} collective-permute-done((bf16[256,1408]{1,0:T(8,128)(2,1)}, bf16[256,1408]{1,0:T(8,128)(2,1)}, u32[]{:S(2)}, u32[]{:S(2)}) %collective-permute-start.49) | collective-permute-done | bytes 720928 | tf_op jit(solution)/shard_map/ppermute | solution.py:273
  312.3 6.2 %all-reduce = (f32[768]{0:T(1024)S(1)}, f32[768]{0:T(1024)S(1)}) all-reduce(f32[768]{0:T(1024)S(1)} %get-tuple-element.758, f32[768]{0:T(1024)S(1)} %get-tuple-element.757), channel_id=1, replica_groups=mesh['fs'=8,'tp'=4] {'tp'}, use_global_device_ids=true, to_apply=%region_3.4 | all-reduce | flops 1536 | bytes 12288 | tf_op jit(solution)/shard_map/psum | solution.py:580
  327.9 4.4 near_terms.4
  339.4 13.8 %collective-permute-done.62.refs_12_ = bf16[256,1408]{1,0:T(8,128)(2,1)} collective-permute-done((bf16[256,1408]{1,0:T(8,128)(2,1)}, bf16[256,1408]{1,0:T(8,128)(2,1)}, u32[]{:S(2)}, u32[]{:S(2)}) %collective-permute-start.62) | collective-permute-done | bytes 720928 | tf_op jit(solution)/shard_map/ppermute | solution.py:273
  358.2 10.4 %collective-permute-done.60.refs_20_ = bf16[256,1408]{1,0:T(8,128)(2,1)} collective-permute-done((bf16[256,1408]{1,0:T(8,128)(2,1)}, bf16[256,1408]{1,0:T(8,128)(2,1)}, u32[]{:S(2)}, u32[]{:S(2)}) %collective-permute-start.60) | collective-permute-done | bytes 720928 | tf_op jit(solution)/shard_map/ppermute | solution.py:273
  370.7 5.6 %collective-permute-done.58.refs_9_.refs_10_ = bf16[704,256]{1,0:T(8,128)(2,1)S(1)} collective-permute-done((bf16[704,256]{1,0:T(8,128)(2,1)S(1)}, bf16[704,256]{1,0:T(8,128)(2,1)S(1)}, u32[]{:S(2)}, u32[]{:S(2)}) %collective-permute-start.58) | collective-permute-done | bytes 360480 | tf_op jit(solution)/shard_map/ppermute | solution.py:273
  377.2 6.0 %collective-permute-done.56.refs_16_.refs_18_ = bf16[704,256]{1,0:T(8,128)(2,1)S(1)} collective-permute-done((bf16[704,256]{1,0:T(8,128)(2,1)}, bf16[704,256]{1,0:T(8,128)(2,1)S(1)}, u32[]{:S(2)}, u32[]{:S(2)}) %collective-permute-start.56) | collective-permute-done | bytes 360480 | tf_op jit(solution)/shard_map/ppermute | solution.py:273
  387.6 16.3 %collective-permute-done.72.refs_11_ = bf16[256,1408]{1,0:T(8,128)(2,1)S(1)} collective-permute-done((bf16[256,1408]{1,0:T(8,128)(2,1)}, bf16[256,1408]{1,0:T(8,128)(2,1)S(1)}, u32[]{:S(2)}, u32[]{:S(2)}) %collective-permute-start.72) | collective-permute-done | bytes 720928 | tf_op jit(solution)/shard_map/ppermute | solution.py:273
  407.2 16.4 %hidden.5.refs_3_ = bf16[768,1408]{1,0:T(8,128)(2,1)} custom-call(s32[8]{0:T(128)} %get-tuple-element.773.refs_0_, s32[4]{0:T(128)} %pad_add_fusion.refs_1_, f32[4,1,512]{2,1,0:T(1,128)} %bitcast.63, bf16[768,512]{1,0:T(8,128)(2,1)} %copy-done.12, bf16[768,512]{1,0:T(8,128)(2,1)} %copy-done.32, bf16[768,512]{1,0:T(8,128)(2,1)} %copy-done.31, ...), custom_call_target="tpu_custom_call" | custom-call | flops 8858370048 | bytes 14680064 | tf_op jit(solution)/shard_map/hidden/pallas_call | solution.py:464
  425.7 6.5 %far_terms.6 = (bf16[1,768,512]{2,1,0:T(8,128)(2,1)}, bf16[1,768,512]{2,1,0:T(8,128)(2,1)}) custom-call(s32[8]{0:T(128)} %get-tuple-element.772.refs_0_, s32[8]{0:T(128)} %get-tuple-element.763.refs_1_, s32[8]{0:T(128)} %get-tuple-element.761.refs_2_, bf16[768,1408]{1,0:T(8,128)(2,1)} %hidden.5.refs_3_, bf16[704,256]{1,0:T(8,128)(2,1)} %get-tuple-element.602.refs_4_, ...), custom_call_target="tpu_custom_call" | custom-call | flops 2214592512 | bytes 2883584 | tf_op jit(solution)/shard_map/far_terms/pallas_call | solution.py:500
  441.1 7.5 %near_terms.5 = (bf16[1,768,512]{2,1,0:T(8,128)(2,1)}, bf16[1,768,512]{2,1,0:T(8,128)(2,1)}) custom-call(s32[8]{0:T(128)} %get-tuple-element.772.refs_0_, s32[8]{0:T(128)} %get-tuple-element.763.refs_1_, s32[8]{0:T(128)} %get-tuple-element.761.refs_2_, bf16[768,1408]{1,0:T(8,128)(2,1)} %hidden.5.refs_3_, bf16[704,256]{1,0:T(8,128)(2,1)} %get-tuple-element.602.refs_4_, ...), custom_call_target="tpu_custom_call" | custom-call | flops 2214592512 | bytes 2883584 | tf_op jit(solution)/shard_map/near_terms/pallas_call | solution.py:500
  451.2 17.4 %collective-permute-done.81 = bf16[768,512]{1,0:T(8,128)(2,1)S(1)} collective-permute-done((bf16[768,512]{1,0:T(8,128)(2,1)S(1)}, bf16[768,512]{1,0:T(8,128)(2,1)S(1)}, u32[]{:S(2)}, u32[]{:S(2)}) %collective-permute-start.81) | collective-permute-done | bytes 786464 | tf_op jit(solution)/shard_map/ppermute | solution.py:329
  (264 shorter events, 133.7 us)
Async XLA Ops:
  0.0 22.3 %collective-permute-start.4 = (bf16[768,512]{1,0:T(8,128)(2,1)}, bf16[768,512]{1,0:T(8,128)(2,1)S(1)}, u32[]{:S(2)}, u32[]{:S(2)}) collective-permute-start(bf16[768,512]{1,0:T(8,128)(2,1)} %refs_3_), channel_id=1, source_target_pairs={{0,2},{1,3},{2,0},{3,1},{4,6},{5,7},{6,4},{7,5},{8,10},{9,11},{10,... | collective-permute-start | bytes 2359304 | tf_op jit(solution)/shard_map/ppermute | solution.py:329
  5.1 38.2 %collective-permute-start.5 = (bf16[768,512]{1,0:T(8,128)(2,1)}, bf16[768,512]{1,0:T(8,128)(2,1)S(1)}, u32[]{:S(2)}, u32[]{:S(2)}) collective-permute-start(bf16[768,512]{1,0:T(8,128)(2,1)} %refs_3_), channel_id=1, source_target_pairs={{0,1},{1,0},{2,3},{3,2},{4,5},{5,4},{6,7},{7,6},{8,9},{9,8},{10,11... | collective-permute-start | bytes 2359304 | tf_op jit(solution)/shard_map/ppermute | solution.py:321
  24.4 34.3 %collective-permute-start.10 = (bf16[256,1408]{1,0:T(8,128)(2,1)}, bf16[256,1408]{1,0:T(8,128)(2,1)}, u32[]{:S(2)}, u32[]{:S(2)}) collective-permute-start(bf16[256,1408]{1,0:T(8,128)(2,1)} %collective-permute-done.3.refs_8_), channel_id=1, source_target_pairs={{0,4},{4,12},{8,0},{12,20},{16,8},{20,28},{24,16},{28,24},{1,5},{5... | collective-permute-start | bytes 2162696 | tf_op jit(solution)/shard_map/ppermute | solution.py:273
  43.3 32.7 %collective-permute-start.7 = (bf16[256,1408]{1,0:T(8,128)(2,1)}, bf16[256,1408]{1,0:T(8,128)(2,1)}, u32[]{:S(2)}, u32[]{:S(2)}) collective-permute-start(bf16[256,1408]{1,0:T(8,128)(2,1)} %collective-permute-done.refs_22_), channel_id=1, source_target_pairs={{0,8},{4,0},{8,16},{12,4},{16,24},{20,12},{24,28},{28,20},{1,9},{5... | collective-permute-start | bytes 2162696 | tf_op jit(solution)/shard_map/ppermute | solution.py:273
  45.0 31.0 %collective-permute-start.8 = (bf16[256,1408]{1,0:T(8,128)(2,1)}, bf16[256,1408]{1,0:T(8,128)(2,1)}, u32[]{:S(2)}, u32[]{:S(2)}) collective-permute-start(bf16[256,1408]{1,0:T(8,128)(2,1)} %collective-permute-done.1.refs_16_), channel_id=1, source_target_pairs={{0,4},{4,12},{8,0},{12,20},{16,8},{20,28},{24,16},{28,24},{1,5},{5... | collective-permute-start | bytes 2162696 | tf_op jit(solution)/shard_map/ppermute | solution.py:273
  60.5 30.9 %collective-permute-start.13 = (bf16[256,1408]{1,0:T(8,128)(2,1)}, bf16[256,1408]{1,0:T(8,128)(2,1)}, u32[]{:S(2)}, u32[]{:S(2)}) collective-permute-start(bf16[256,1408]{1,0:T(8,128)(2,1)} %collective-permute-done.9.refs_13_), channel_id=1, source_target_pairs={{0,8},{4,0},{8,16},{12,4},{16,24},{20,12},{24,28},{28,20},{1,9},{5... | collective-permute-start | bytes 2162696 | tf_op jit(solution)/shard_map/ppermute | solution.py:273
  62.1 29.3 %collective-permute-start.14 = (bf16[256,1408]{1,0:T(8,128)(2,1)}, bf16[256,1408]{1,0:T(8,128)(2,1)}, u32[]{:S(2)}, u32[]{:S(2)}) collective-permute-start(bf16[256,1408]{1,0:T(8,128)(2,1)} %collective-permute-done.10.refs_9_), channel_id=1, source_target_pairs={{0,4},{4,12},{8,0},{12,20},{16,8},{20,28},{24,16},{28,24},{1,5},{5... | collective-permute-start | bytes 2162696 | tf_op jit(solution)/shard_map/ppermute | solution.py:273
  76.0 30.9 %collective-permute-start.11 = (bf16[256,1408]{1,0:T(8,128)(2,1)}, bf16[256,1408]{1,0:T(8,128)(2,1)}, u32[]{:S(2)}, u32[]{:S(2)}) collective-permute-start(bf16[256,1408]{1,0:T(8,128)(2,1)} %collective-permute-done.7.refs_21_), channel_id=1, source_target_pairs={{0,8},{4,0},{8,16},{12,4},{16,24},{20,12},{24,28},{28,20},{1,9},{5... | collective-permute-start | bytes 2162696 | tf_op jit(solution)/shard_map/ppermute | solution.py:273
  77.6 29.3 %collective-permute-start.12 = (bf16[256,1408]{1,0:T(8,128)(2,1)}, bf16[256,1408]{1,0:T(8,128)(2,1)}, u32[]{:S(2)}, u32[]{:S(2)}) collective-permute-start(bf16[256,1408]{1,0:T(8,128)(2,1)} %collective-permute-done.8.refs_17_), channel_id=1, source_target_pairs={{0,4},{4,12},{8,0},{12,20},{16,8},{20,28},{24,16},{28,24},{1,5},{5... | collective-permute-start | bytes 2162696 | tf_op jit(solution)/shard_map/ppermute | solution.py:273
  91.5 29.5 %collective-permute-start.22 = (bf16[256,1408]{1,0:T(8,128)(2,1)}, bf16[256,1408]{1,0:T(8,128)(2,1)}, u32[]{:S(2)}, u32[]{:S(2)}) collective-permute-start(bf16[256,1408]{1,0:T(8,128)(2,1)} %collective-permute-done.13.refs_12_), channel_id=1, source_target_pairs={{0,8},{4,0},{8,16},{12,4},{16,24},{20,12},{24,28},{28,20},{1,9},{5... | collective-permute-start | bytes 2162696 | tf_op jit(solution)/shard_map/ppermute | solution.py:273
  121.0 22.2 %collective-permute-start.17 = (bf16[1088,256]{1,0:T(8,128)(2,1)S(1)}, bf16[1088,256]{1,0:T(8,128)(2,1)}, u32[]{:S(2)}, u32[]{:S(2)}) collective-permute-start(bf16[1088,256]{1,0:T(8,128)(2,1)S(1)} %slice.16.refs_4_), channel_id=1, source_target_pairs={{0,8},{4,0},{8,16},{12,4},{16,24},{20,12},{24,28},{28,20},{1,9},{5... | collective-permute-start | bytes 1671176 | tf_op jit(solution)/shard_map/ppermute | solution.py:273
  125.0 23.4 %collective-permute-start.15 = (bf16[256,768]{1,0:T(8,128)(2,1)S(1)}, bf16[256,768]{1,0:T(8,128)(2,1)S(1)}, u32[]{:S(2)}, u32[]{:S(2)}) collective-permute-start(bf16[256,768]{1,0:T(8,128)(2,1)S(1)} %constant_dynamic-update-slice_fusion.refs_7_.refs_4_), channel_id=1, source_target_pairs={{0,8},{4,0},{8,16},{12,4},{16,24},{20,12},{24,28},{28,20},{1,9},{5... | collective-permute-start | bytes 1179656 | tf_op jit(solution)/shard_map/ppermute | solution.py:273
  143.1 28.9 %collective-permute-start.25 = (bf16[1088,256]{1,0:T(8,128)(2,1)}, bf16[1088,256]{1,0:T(8,128)(2,1)}, u32[]{:S(2)}, u32[]{:S(2)}) collective-permute-start(bf16[1088,256]{1,0:T(8,128)(2,1)} %collective-permute-done.17.refs_11_), channel_id=1, source_target_pairs={{0,8},{4,0},{8,16},{12,4},{16,24},{20,12},{24,28},{28,20},{1,9},{5... | collective-permute-start | bytes 1671176 | tf_op jit(solution)/shard_map/ppermute | solution.py:273
  144.8 27.2 %collective-permute-start.26 = (bf16[1088,256]{1,0:T(8,128)(2,1)}, bf16[1088,256]{1,0:T(8,128)(2,1)}, u32[]{:S(2)}, u32[]{:S(2)}) collective-permute-start(bf16[1088,256]{1,0:T(8,128)(2,1)} %collective-permute-done.18.refs_5_), channel_id=1, source_target_pairs={{0,4},{4,12},{8,0},{12,20},{16,8},{20,28},{24,16},{28,24},{1,5},{5... | collective-permute-start | bytes 1671176 | tf_op jit(solution)/shard_map/ppermute | solution.py:273
  145.2 23.3 %collective-permute-start.16 = (bf16[256,768]{1,0:T(8,128)(2,1)S(1)}, bf16[256,768]{1,0:T(8,128)(2,1)S(1)}, u32[]{:S(2)}, u32[]{:S(2)}) collective-permute-start(bf16[256,768]{1,0:T(8,128)(2,1)S(1)} %constant_dynamic-update-slice_fusion.refs_7_.refs_4_), channel_id=1, source_target_pairs={{0,4},{4,12},{8,0},{12,20},{16,8},{20,28},{24,16},{28,24},{1,5},{5... | collective-permute-start | bytes 1179656 | tf_op jit(solution)/shard_map/ppermute | solution.py:273
  145.7 24.6 %collective-permute-start.27 = (bf16[320,256]{1,0:T(8,128)(2,1)S(1)}, bf16[320,256]{1,0:T(8,128)(2,1)S(1)}, u32[]{:S(2)}, u32[]{:S(2)}) collective-permute-start(bf16[320,256]{1,0:T(8,128)(2,1)S(1)} %collective-permute-done.19.refs_19_), channel_id=1, source_target_pairs={{0,8},{4,0},{8,16},{12,4},{16,24},{20,12},{24,28},{28,20},{1,9},{5... | collective-permute-start | bytes 491528 | tf_op jit(solution)/shard_map/ppermute | solution.py:273
  148.4 23.6 %collective-permute-start.28 = (bf16[320,256]{1,0:T(8,128)(2,1)}, bf16[320,256]{1,0:T(8,128)(2,1)S(1)}, u32[]{:S(2)}, u32[]{:S(2)}) collective-permute-start(bf16[320,256]{1,0:T(8,128)(2,1)} %collective-permute-done.20.refs_13_), channel_id=1, source_target_pairs={{0,4},{4,12},{8,0},{12,20},{16,8},{20,28},{24,16},{28,24},{1,5},{5... | collective-permute-start | bytes 491528 | tf_op jit(solution)/shard_map/ppermute | solution.py:273
  172.0 29.8 %collective-permute-start.31 = (bf16[1088,256]{1,0:T(8,128)(2,1)}, bf16[1088,256]{1,0:T(8,128)(2,1)}, u32[]{:S(2)}, u32[]{:S(2)}) collective-permute-start(bf16[1088,256]{1,0:T(8,128)(2,1)} %collective-permute-done.25.refs_10_), channel_id=1, source_target_pairs={{0,8},{4,0},{8,16},{12,4},{16,24},{20,12},{24,28},{28,20},{1,9},{5... | collective-permute-start | bytes 1671176 | tf_op jit(solution)/shard_map/ppermute | solution.py:273
  173.8 28.0 %collective-permute-start.32 = (bf16[1088,256]{1,0:T(8,128)(2,1)}, bf16[1088,256]{1,0:T(8,128)(2,1)}, u32[]{:S(2)}, u32[]{:S(2)}) collective-permute-start(bf16[1088,256]{1,0:T(8,128)(2,1)} %collective-permute-done.26.refs_6_), channel_id=1, source_target_pairs={{0,4},{4,12},{8,0},{12,20},{16,8},{20,28},{24,16},{28,24},{1,5},{5... | collective-permute-start | bytes 1671176 | tf_op jit(solution)/shard_map/ppermute | solution.py:273
  231.9 21.9 %collective-permute-start.44 = (bf16[768,512]{1,0:T(8,128)(2,1)S(1)}, bf16[768,512]{1,0:T(8,128)(2,1)}, u32[]{:S(2)}, u32[]{:S(2)}) collective-permute-start(bf16[768,512]{1,0:T(8,128)(2,1)S(1)} %bitcast.58), channel_id=1, source_target_pairs={{0,2},{1,3},{2,0},{3,1},{4,6},{5,7},{6,4},{7,5},{8,10},{9,11},{10,... | collective-permute-start | bytes 2359304 | tf_op jit(solution)/shard_map/ppermute | solution.py:329
  234.4 32.7 %collective-permute-start.35 = (bf16[256,1408]{1,0:T(8,128)(2,1)}, bf16[256,1408]{1,0:T(8,128)(2,1)}, u32[]{:S(2)}, u32[]{:S(2)}) collective-permute-start(bf16[256,1408]{1,0:T(8,128)(2,1)} %refs_15_.3), channel_id=1, source_target_pairs={{0,8},{4,0},{8,16},{12,4},{16,24},{20,12},{24,28},{28,20},{1,9},{5... | collective-permute-start | bytes 2162696 | tf_op jit(solution)/shard_map/ppermute | solution.py:273
  236.5 32.7 %collective-permute-start.36 = (bf16[256,1408]{1,0:T(8,128)(2,1)}, bf16[256,1408]{1,0:T(8,128)(2,1)}, u32[]{:S(2)}, u32[]{:S(2)}) collective-permute-start(bf16[256,1408]{1,0:T(8,128)(2,1)} %refs_15_.3), channel_id=1, source_target_pairs={{0,4},{4,12},{8,0},{12,20},{16,8},{20,28},{24,16},{28,24},{1,5},{5... | collective-permute-start | bytes 2162696 | tf_op jit(solution)/shard_map/ppermute | solution.py:273
  278.3 32.7 %collective-permute-start.49 = (bf16[256,1408]{1,0:T(8,128)(2,1)}, bf16[256,1408]{1,0:T(8,128)(2,1)}, u32[]{:S(2)}, u32[]{:S(2)}) collective-permute-start(bf16[256,1408]{1,0:T(8,128)(2,1)} %collective-permute-done.35.refs_22_), channel_id=1, source_target_pairs={{0,8},{4,0},{8,16},{12,4},{16,24},{20,12},{24,28},{28,20},{1,9},{5... | collective-permute-start | bytes 2162696 | tf_op jit(solution)/shard_map/ppermute | solution.py:273
  279.3 32.7 %collective-permute-start.50 = (bf16[256,1408]{1,0:T(8,128)(2,1)}, bf16[256,1408]{1,0:T(8,128)(2,1)}, u32[]{:S(2)}, u32[]{:S(2)}) collective-permute-start(bf16[256,1408]{1,0:T(8,128)(2,1)} %collective-permute-done.36.refs_16_), channel_id=1, source_target_pairs={{0,4},{4,12},{8,0},{12,20},{16,8},{20,28},{24,16},{28,24},{1,5},{5... | collective-permute-start | bytes 2162696 | tf_op jit(solution)/shard_map/ppermute | solution.py:273
  281.3 38.3 %collective-permute-start.45 = (bf16[704,256]{1,0:T(8,128)(2,1)}, bf16[704,256]{1,0:T(8,128)(2,1)}, u32[]{:S(2)}, u32[]{:S(2)}) collective-permute-start(bf16[704,256]{1,0:T(8,128)(2,1)} %get-tuple-element.600.refs_11_.refs_12_), channel_id=1, source_target_pairs={{0,8},{4,0},{8,16},{12,4},{16,24},{20,12},{24,28},{28,20},{1,9},{5... | collective-permute-start | bytes 1081352 | tf_op jit(solution)/shard_map/ppermute | solution.py:273
  297.1 22.5 %collective-permute-start.46 = (bf16[704,256]{1,0:T(8,128)(2,1)S(1)}, bf16[704,256]{1,0:T(8,128)(2,1)}, u32[]{:S(2)}, u32[]{:S(2)}) collective-permute-start(bf16[704,256]{1,0:T(8,128)(2,1)S(1)} %copy-done.22), channel_id=1, source_target_pairs={{0,4},{4,12},{8,0},{12,20},{16,8},{20,28},{24,16},{28,24},{1,5},{5... | collective-permute-start | bytes 1081352 | tf_op jit(solution)/shard_map/ppermute | solution.py:273
  332.5 21.6 %collective-permute-start.66 = (bf16[768,512]{1,0:T(8,128)(2,1)S(1)}, bf16[768,512]{1,0:T(8,128)(2,1)}, u32[]{:S(2)}, u32[]{:S(2)}) collective-permute-start(bf16[768,512]{1,0:T(8,128)(2,1)S(1)} %bitcast.59), channel_id=1, source_target_pairs={{0,2},{1,3},{2,0},{3,1},{4,6},{5,7},{6,4},{7,5},{8,10},{9,11},{10,... | collective-permute-start | bytes 2359304 | tf_op jit(solution)/shard_map/ppermute | solution.py:329
  335.9 32.7 %collective-permute-start.60 = (bf16[256,1408]{1,0:T(8,128)(2,1)}, bf16[256,1408]{1,0:T(8,128)(2,1)}, u32[]{:S(2)}, u32[]{:S(2)}) collective-permute-start(bf16[256,1408]{1,0:T(8,128)(2,1)} %collective-permute-done.49.refs_21_), channel_id=1, source_target_pairs={{0,8},{4,0},{8,16},{12,4},{16,24},{20,12},{24,28},{28,20},{1,9},{5... | collective-permute-start | bytes 2162696 | tf_op jit(solution)/shard_map/ppermute | solution.py:273
  336.8 32.7 %collective-permute-start.61 = (bf16[256,1408]{1,0:T(8,128)(2,1)}, bf16[256,1408]{1,0:T(8,128)(2,1)}, u32[]{:S(2)}, u32[]{:S(2)}) collective-permute-start(bf16[256,1408]{1,0:T(8,128)(2,1)} %collective-permute-done.50.refs_17_), channel_id=1, source_target_pairs={{0,4},{4,12},{8,0},{12,20},{16,8},{20,28},{24,16},{28,24},{1,5},{5... | collective-permute-start | bytes 2162696 | tf_op jit(solution)/shard_map/ppermute | solution.py:273
  355.6 29.0 %collective-permute-start.74 = (bf16[768,512]{1,0:T(8,128)(2,1)S(1)}, bf16[768,512]{1,0:T(8,128)(2,1)S(1)}, u32[]{:S(2)}, u32[]{:S(2)}) collective-permute-start(bf16[768,512]{1,0:T(8,128)(2,1)S(1)} %fusion.5.refs_3_), channel_id=1, source_target_pairs={{0,2},{1,3},{2,0},{3,1},{4,6},{5,7},{6,4},{7,5},{8,10},{9,11},{10,... | collective-permute-start | bytes 2359304 | tf_op jit(solution)/shard_map/ppermute | solution.py:329
  385.6 21.5 %collective-permute-start.71 = (bf16[256,1408]{1,0:T(8,128)(2,1)}, bf16[256,1408]{1,0:T(8,128)(2,1)}, u32[]{:S(2)}, u32[]{:S(2)}) collective-permute-start(bf16[256,1408]{1,0:T(8,128)(2,1)} %collective-permute-done.61.refs_18_), channel_id=1, source_target_pairs={{0,4},{4,12},{8,0},{12,20},{16,8},{20,28},{24,16},{28,24},{1,5},{5... | collective-permute-start | bytes 2162696 | tf_op jit(solution)/shard_map/ppermute | solution.py:273
  386.8 36.8 %collective-permute-start.69 = (bf16[704,256]{1,0:T(8,128)(2,1)}, bf16[704,256]{1,0:T(8,128)(2,1)S(1)}, u32[]{:S(2)}, u32[]{:S(2)}) collective-permute-start(bf16[704,256]{1,0:T(8,128)(2,1)} %copy-done.38), channel_id=1, source_target_pairs={{0,8},{4,0},{8,16},{12,4},{16,24},{20,12},{24,28},{28,20},{1,9},{5... | collective-permute-start | bytes 1081352 | tf_op jit(solution)/shard_map/ppermute | solution.py:273
  (98 other events, 2243.4 us)
